TPU v7x, 512 devices: a whole 4x4x16 slice. The times are simulated.
512 devices in a mesh: sp: 16 (over y, x), tp: 32 (over z, core).
Axes of the slice: x: 4, y: 4, z: 16, core: 2. Of those that a mesh axis runs over, the one named last changes fastest.
Arguments:
- tokens: bfloat16 [32, 6144, 2048], P('tp', 'sp'), may hold values from -12 to 12
- norm_gain: float32 [2, 2048], replicated, may hold values from 0.1 to 1.9
- in_weight: bfloat16 [2, 2048, 512], P(None, 'sp', 'tp'), may hold values from -0.125 to 0.125
- down_weight: bfloat16 [2, 512, 2048], P(None, 'sp', 'tp'), may hold values from -0.25 to 0.25
- pool_gain: float32 [2, 512], replicated, may hold values from 0.1 to 1.9
Outputs:
- mixed: bfloat16 [32, 6144, 2048], P('tp', 'sp')
All inputs are finite; a program needn't handle non-finite values.
Results may differ from a plain program's by a relative error of at most 0.0061.
Values may be sent and summed in bfloat16 or wider, within the bound.
No kernel may reach another device: no remote copies, remote signals or barrier semaphores. Data moves between devices by JAX's collectives and lax.ppermute only.
A program may use at most 64 MiB of HBM per device.

v0:
```python
import jax
import jax.numpy as jnp
from jax import lax
from jax.sharding import PartitionSpec as P

GROUP = 64


EPS = 1e-06
WINDOWS = (2, 4, 8, 16)


def joined_along(blocks, dim):
    lengths = list(blocks.shape[1:])
    lengths[dim] *= blocks.shape[0]
    return jnp.moveaxis(blocks, 0, dim).reshape(lengths)


def gather_together(arrays, axis, dims):
    ravelled = jnp.concatenate([a.reshape(-1) for a in arrays])
    lines, at, finished = (lax.all_gather(ravelled, axis), 0, [])
    for a, dim in zip(arrays, dims):
        blocks = lines[:, at : at + a.size].reshape(-1, *a.shape)
        finished.append(joined_along(blocks, dim))
        at += a.size
    return tuple(finished)


def from_behind(block, axis, distance):
    devices = range(lax.axis_size(axis))
    route = [(i - distance, i) for i in devices if i - distance in devices]
    return lax.ppermute(block, axis, route)


def pool_rows(extended, first_pos, channel):
    sum_two = extended[1:] + extended[:-1]
    sum_four = sum_two[2:] + sum_two[:-2]
    sum_eight = sum_four[4:] + sum_four[:-4]
    sum_sixteen = sum_eight[8:] + sum_eight[:-8]
    count = extended.shape[0] - 15
    sums = (sum_two[-count:], sum_four[-count:], sum_eight[-count:], sum_sixteen)
    position = (first_pos + lax.iota(jnp.int32, count) + 1).astype(jnp.float32)
    which_one = channel // GROUP % 4
    result = jnp.zeros((count, extended.shape[1]), jnp.float32)
    for index, window in enumerate(WINDOWS):
        average = sums[index] / jnp.minimum(position, float(window))[:, None]
        result = jnp.where(which_one[None, :] == index, average, result)
    return result - extended[15:]


def local(tokens, norm_gain, in_weight, down_weight, pool_gain):
    stream = tokens[0]
    tok_rows = stream.shape[0]
    pool_cols = pool_gain.shape[1]
    first_pos = lax.axis_index("sp") * tok_rows
    channel = lax.iota(jnp.int32, pool_cols)
    col_in, col_down = gather_together((in_weight, down_weight), "tp", (2, 2))
    whole_in, whole_down = gather_together((col_in, col_down), "sp", (1, 1))
    for layer_index in range(in_weight.shape[0]):
        residual = stream.astype(jnp.float32)
        inverse_rms = lax.rsqrt(jnp.mean(residual * residual, axis=1, keepdims=True) + EPS)
        normed = (residual * inverse_rms * norm_gain[layer_index]).astype(jnp.bfloat16)
        pool_acc = jnp.dot(normed, whole_in[layer_index], preferred_element_type=jnp.float32)
        pool_in = pool_acc.astype(jnp.bfloat16)
        before = from_behind(pool_in[tok_rows - 15 :], "sp", 1)
        extended = jnp.concatenate([before, pool_in], axis=0).astype(jnp.float32)
        trailing = pool_rows(extended, first_pos, channel)
        pooled = (trailing * pool_gain[layer_index]).astype(jnp.bfloat16)
        down = jnp.dot(pooled, whole_down[layer_index], preferred_element_type=jnp.float32)
        stream = (residual + down).astype(jnp.bfloat16)
    return stream[None]


def solution(mesh):
    in_specs = (P("tp", "sp", None), P(), P(None, "sp", "tp"), P(None, "sp", "tp"), P())
    out_specs = P("tp", "sp", None)
    return jax.shard_map(local, mesh=mesh, in_specs=in_specs, out_specs=out_specs, check_vma=False)
```

profile of v0, /device:TPU:8, one launch (start us, length us, event | category | flops | bytes accessed | tf_op | source)
XLA Modules:
  0.0 176.0 jit_solution(5681192595661167546)
XLA Ops:
  6.5 0.0 all-gather.4.cloned.1.call-start
  6.5 0.8 copy.12
  7.4 0.1 reshape.114
  7.5 0.8 reshape.115
  8.3 37.7 %all-gather = bf16[262144]{0:T(1024)(128)(2,1)S(1)} all-gather(bf16[8192]{0:T(1024)(128)(2,1)S(1)} %pad_maximum_fusion.1), channel_id=2, replica_groups=mesh['sp'=16,'tp'=32] {'tp'}, dimensions={0}, use_global_device_ids=true | all-gather | bytes 540672 | tf_op jit(solution)/shard_map/all_gather | solution.py:21
  45.9 0.2 reshape.121
  46.2 0.5 copy.13
  46.7 1.0 copy.14
  47.7 1.3 reshape_reshape.6
  49.1 0.0 copy-start
  49.1 0.5 reshape.117
  49.6 0.3 copy.15
  50.0 0.0 copy-start.2
  50.0 0.0 copy-start.1
  50.0 0.2 reshape_reshape.7
  50.2 0.8 pad_maximum_fusion
  51.1 0.0 all-gather.4.cloned.1.call-update
  51.2 0.0 copy-done
  51.2 0.4 fusion.2
  51.6 0.0 copy-done.2
  51.6 0.0 copy-done.1
  51.6 81.6 %all-gather.4.cloned.1.call-done = bf16[4194304]{0:T(1024)(128)(2,1)} async-done(((bf16[262144]{0:T(1024)(128)(2,1)}), bf16[4194304]{0:T(1024)(128)(2,1)}) %all-gather.4.cloned.1.call-update) | async-done | bytes 8388624 | tf_op jit(solution)/shard_map/all_gather | solution.py:21
  133.2 7.6 %reshape.122 = bf16[16,262144]{1,0:T(8,128)(2,1)} reshape(bf16[4194304]{0:T(1024)(128)(2,1)} %all-gather.4.cloned.1.call-done) | data formatting | bytes 16777216 | tf_op jit(solution)/shard_map/all_gather | solution.py:21
  140.8 3.8 %fusion.68 = (bf16[16,131072]{1,0:T(8,128)(2,1)S(1)}, bf16[16,131072]{1,0:T(8,128)(2,1)S(1)}) fusion(bf16[16,262144]{1,0:T(8,128)(2,1)} %reshape.122), kind=kLoop, calls=%fused_computation.101 | loop fusion | bytes 16777216 | tf_op jit(solution)/shard_map/slice | solution.py:23
  144.6 1.4 copy.16
  146.1 0.3 fusion.69
  146.4 1.0 fusion.20
  147.4 2.3 %collective-permute-start = (bf16[15,512]{1,0:T(8,128)(2,1)S(1)}, bf16[15,512]{1,0:T(8,128)(2,1)S(1)}, u32[]{:S(2)}, u32[]{:S(2)}) collective-permute-start(bf16[15,512]{1,0:T(8,128)(2,1)S(1)} %slice.154), channel_id=1, source_target_pairs={{0,32},{32,64},{64,96},{96,128},{128,160},{160,192},{192,224},{224... | collective-permute-start | bytes 46088 | tf_op jit(solution)/shard_map/ppermute | solution.py:32
  149.8 2.3 %copy.17 = bf16[2,8,64,2048]{3,2,1,0:T(8,128)(2,1)S(1)} copy(bf16[2,8,64,2048]{3,1,2,0:T(8,128)(2,1)S(1)} %bitcast.49) | data formatting | bytes 8388608
  152.1 0.5 fusion.70
  152.7 2.5 %collective-permute-done = bf16[15,512]{1,0:T(8,128)(2,1)S(1)} collective-permute-done((bf16[15,512]{1,0:T(8,128)(2,1)S(1)}, bf16[15,512]{1,0:T(8,128)(2,1)S(1)}, u32[]{:S(2)}, u32[]{:S(2)}) %collective-permute-start) | collective-permute-done | bytes 15392 | tf_op jit(solution)/shard_map/ppermute | solution.py:32
  155.2 0.1 maximum_convert_fusion
  155.3 0.1 slice_add_fusion.3
  155.4 0.1 slice_add_fusion.2
  155.5 0.1 slice_add_fusion.5
  155.7 1.6 fusion.6
  157.3 1.0 fusion.23
  158.3 1.9 %collective-permute-start.1 = (bf16[15,512]{1,0:T(8,128)(2,1)S(1)}, bf16[15,512]{1,0:T(8,128)(2,1)S(1)}, u32[]{:S(2)}, u32[]{:S(2)}) collective-permute-start(bf16[15,512]{1,0:T(8,128)(2,1)S(1)} %slice.169), channel_id=1, source_target_pairs={{0,32},{32,64},{64,96},{96,128},{128,160},{160,192},{192,224},{224... | collective-permute-start | bytes 46088 | tf_op jit(solution)/shard_map/ppermute | solution.py:32
  160.3 5.8 %collective-permute-done.1 = bf16[15,512]{1,0:T(8,128)(2,1)S(1)} collective-permute-done((bf16[15,512]{1,0:T(8,128)(2,1)S(1)}, bf16[15,512]{1,0:T(8,128)(2,1)S(1)}, u32[]{:S(2)}, u32[]{:S(2)}) %collective-permute-start.1) | collective-permute-done | bytes 15392 | tf_op jit(solution)/shard_map/ppermute | solution.py:32
  166.1 0.1 maximum_convert_fusion.1
  166.2 0.1 slice_add_fusion.1
  166.3 0.1 slice_add_fusion
  166.4 0.1 slice_add_fusion.4
  166.6 2.6 %fusion.10 = bf16[1,384,2048]{2,1,0:T(8,128)(2,1)} fusion(bf16[512,2048]{1,0:T(8,128)(2,1)S(1)} %bitcast.53, bf16[384,2048]{1,0:T(8,128)(2,1)S(1)} %get-tuple-element.18, f32[399,512]{1,0:T(8,128)S(1)} %maximum_convert_fusion.1, f32[398,512]{1,0:T(8,128)S(1)} %slice_add_fusion.1, f32[396,512]{1,0:T(8,128)S(1)} %slice_add_fusion, ...), kind=kOutput, calls=%fused_computation.15 | convolution fusion | flops 810024960 | bytes 9187328 | tf_op jit(solution)/shard_map/dot_general | solution.py:69
  (12 shorter events, 0.1 us)
Async XLA Ops:
  6.5 126.7 %all-gather.4.cloned.1.call-start = ((), (), s32[]{:S(2)}) async-start(), calls=%async_computation | async-start | bytes 8912896 | tf_op jit(solution)/shard_map/all_gather | solution.py:21
  49.1 2.1 %copy-start = (bf16[1,384,2048]{2,1,0:T(8,128)(2,1)S(1)}, bf16[1,384,2048]{2,1,0:T(8,128)(2,1)}, u32[]{:S(2)}) copy-start(bf16[1,384,2048]{2,1,0:T(8,128)(2,1)} %param.5) | copy-start | bytes 4718596
  50.0 1.6 copy-start.2
  50.0 1.6 copy-start.1
  147.4 7.7 %collective-permute-start = (bf16[15,512]{1,0:T(8,128)(2,1)S(1)}, bf16[15,512]{1,0:T(8,128)(2,1)S(1)}, u32[]{:S(2)}, u32[]{:S(2)}) collective-permute-start(bf16[15,512]{1,0:T(8,128)(2,1)S(1)} %slice.154), channel_id=1, source_target_pairs={{0,32},{32,64},{64,96},{96,128},{128,160},{160,192},{192,224},{224... | collective-permute-start | bytes 46088 | tf_op jit(solution)/shard_map/ppermute | solution.py:32
  158.3 7.7 %collective-permute-start.1 = (bf16[15,512]{1,0:T(8,128)(2,1)S(1)}, bf16[15,512]{1,0:T(8,128)(2,1)S(1)}, u32[]{:S(2)}, u32[]{:S(2)}) collective-permute-start(bf16[15,512]{1,0:T(8,128)(2,1)S(1)} %slice.169), channel_id=1, source_target_pairs={{0,32},{32,64},{64,96},{96,128},{128,160},{160,192},{192,224},{224... | collective-permute-start | bytes 46088 | tf_op jit(solution)/shard_map/ppermute | solution.py:32
Sparse Core Ops, SparseCore 0:
  51.2 81.9 all-gather.3
where the time goes:
time: 176 us
  waiting for transfers between devices  90 us (51%)
  blocking collectives  37.7 us (21%)
  local copies, waits for them, and re-layouts  22 us (12%)
  between operations  13.7 us (8%)
  matrix products  6.26 us (4%)
  starting transfers between devices  4.27 us (2%)
  other arithmetic  2.14 us (1%)
    all_gather x1, waiting for transfers between devices, gather_together(): lines, at, finished = (lax.all_gather(ravelled, axis), 0, [])  81.6 us
    all_gather x1, blocking collectives, gather_together(): lines, at, finished = (lax.all_gather(ravelled, axis), 0, [])  37.7 us
    ppermute x2, waiting for transfers between devices, from_behind(): return lax.ppermute(block, axis, route)  8.34 us
    all_gather x2, local copies, waits for them, and re-layouts, gather_together(): lines, at, finished = (lax.all_gather(ravelled, axis), 0, [])  7.86 us
    unnamed x9, local copies, waits for them, and re-layouts  4.57 us
    slice x3, local copies, waits for them, and re-layouts, gather_together(): blocks = lines[:, at:at + a.size].reshape(-1, *a.shape)  4.27 us
    ppermute x2, starting transfers between devices, from_behind(): return lax.ppermute(block, axis, route)  4.27 us
    dot_general x2, matrix products, local(): jnp.dot(pooled, whole_down[layer_index], preferred_element_type=jnp.float32)  4.2 us
  transfers between devices with their start and end apart: 3, of which 3 were waited for; matrix products, arithmetic and copies ran while one was open for 2% of the time, Pallas kernels for 0%

commit v1 on v0

v1 whole, which is shorter than its diff:
```python
import jax
import jax.numpy as jnp
from jax import lax
from jax.experimental import pallas as pl
from jax.experimental.pallas import tpu as pltpu
from jax.sharding import PartitionSpec as P

EPS = 1e-06
HALO = 32
PAD = 16
SEEN = (0, -1, 1, 2)
AXES = ("sp", "tp")


def number(y, x, z, c):
    return (((y % 4) * 4 + x % 4) * 16 + z % 16) * 2 + c


def places():
    for i in range(512):
        yield i, (i // 128, i // 32 % 4, i // 2 % 16, i % 2)


def send(block, target):
    route = [(i, number(*target(*place))) for i, place in places()]
    return lax.ppermute(block, AXES, route)


def shared(block, count, key):
    groups = {}
    for i, place in places():
        groups.setdefault(key(*place), []).append(i)
    copies = jnp.broadcast_to(block[None], (count, *block.shape))
    return lax.all_to_all(
        copies, AXES, 0, 0, axis_index_groups=list(groups.values()), tiled=True
    )


def second_hop(d):
    return lambda y, x, z, c: (y + d, x, z, c) if c == 0 else (y, x + d, z, c)


def other_core(y, x, z, c):
    return y, x, z, 1 - c


def mixer_kernel(place, halo, tokens, norm_gain, pool_gain, *refs):
    mine, theirs, out = refs[:4], refs[4:8], refs[8]
    whole_in, whole_down, stream, normed, extended, pooled = refs[9:]
    sp, c = place[0], place[1]
    y, x = sp // 4, sp % 4
    s_mine = jnp.where(c == 0, y, x)
    s_theirs = jnp.where(c == 0, x, y)
    left = (lax.broadcasted_iota(jnp.int32, (32, 128), 1) < 64) ^ (c == 1)

    for pieces, core, second in ((mine, c, s_mine), (theirs, 1 - c, s_theirs)):
        for k in range(4):
            s = (second + SEEN[k] + 4) % 4

            def put_in(f, carry, pieces=pieces, core=core, k=k, s=s):
                at = jnp.where(core == 0, s * 4 + f, f * 4 + s)
                lanes = pl.ds(pl.multiple_of(at * 128, 128), 128)
                for l in range(2):
                    whole_in[l, :, core, :, lanes] = pieces[k][
                        f, :, l * 16 : (l + 1) * 16
                    ]
                return carry

            lax.fori_loop(0, 4, put_in, 0)

    for k in range(4):
        a = (s_mine + SEEN[k] + 4) % 4
        for j in range(4):
            b = (s_theirs + SEEN[j] + 4) % 4
            at = jnp.where(c == 0, a * 4 + b, b * 4 + a)
            rows = pl.ds(pl.multiple_of(at * 32, 32), 32)
            for z in range(16):
                m = mine[k][b, z, 32:64]
                t = theirs[j][a, z, 32:64]
                lanes = slice(z * 128, (z + 1) * 128)
                whole_down[0, rows, lanes] = jnp.where(left, m, t)
                v = jnp.where(left, t, m)
                whole_down[1, rows, lanes] = jnp.concatenate(
                    [v[:, 64:], v[:, :64]], axis=1
                )

    stream[:HALO] = halo[...]
    stream[HALO:] = tokens[...]
    extended[:PAD] = jnp.zeros((PAD, 512), jnp.float32)
    count = extended.shape[0] - PAD
    row = lax.broadcasted_iota(jnp.int32, (count, 128), 0)
    lane = lax.broadcasted_iota(jnp.int32, (count, 128), 1)
    position = jnp.maximum(sp * 384 - HALO + row + 1, 1).astype(jnp.float32)

    def layer(l, carry):
        gain_in = jnp.where(l == 0, norm_gain[0:1], norm_gain[1:2])

        def norm(i, carry):
            rows = pl.ds(pl.multiple_of(i * 32, 32), 32)
            residual = stream[rows].astype(jnp.float32)
            mean = jnp.mean(residual * residual, axis=1, keepdims=True)
            scaled = residual * lax.rsqrt(mean + EPS) * gain_in
            normed[rows] = scaled.astype(jnp.bfloat16)
            return carry

        lax.fori_loop(0, count // 32, norm, 0)
        pool_in = lax.dot_general(
            normed[...],
            whole_in[l].reshape(512, 2048),
            (((1,), (1,)), ((), ())),
            preferred_element_type=jnp.float32,
        )
        extended[PAD:] = pool_in.astype(jnp.bfloat16).astype(jnp.float32)
        for j in range(4):
            lanes = slice(j * 128, (j + 1) * 128)
            own = extended[:, lanes]
            two = own + pltpu.roll(own, 1, 0)
            four = two + pltpu.roll(two, 2, 0)
            short, long, window = two, four, 2.0
            if j % 2:
                eight = four + pltpu.roll(four, 4, 0)
                short, long, window = eight, eight + pltpu.roll(eight, 8, 0), 8.0
            total = jnp.where(lane < 64, short[PAD:], long[PAD:])
            width = jnp.where(lane < 64, window, 2 * window)
            trailing = total / jnp.minimum(position, width) - own[PAD:]
            gain = jnp.where(l == 0, pool_gain[0:1, lanes], pool_gain[1:2, lanes])
            pooled[:, lanes] = (trailing * gain).astype(jnp.bfloat16)
        for j in range(4):
            lanes = slice(j * 512, (j + 1) * 512)
            down = jnp.dot(
                pooled[...],
                whole_down[l, :, lanes],
                preferred_element_type=jnp.float32,
            )
            total = stream[:, lanes].astype(jnp.float32) + down
            stream[:, lanes] = total.astype(jnp.bfloat16)
        return carry

    lax.fori_loop(0, 2, layer, 0)
    out[...] = stream[HALO:]


def mixer(halo, tokens, norm_gain, pool_gain, mine, theirs):
    place = jnp.stack([lax.axis_index("sp"), lax.axis_index("tp") % 2])
    vmem = pl.BlockSpec(memory_space=pltpu.VMEM)
    rows = HALO + tokens.shape[0]
    return pl.pallas_call(
        mixer_kernel,
        out_shape=jax.ShapeDtypeStruct(tokens.shape, tokens.dtype),
        in_specs=[pl.BlockSpec(memory_space=pltpu.SMEM)] + [vmem] * 12,
        out_specs=vmem,
        scratch_shapes=[
            pltpu.VMEM((2, 16, 2, 16, 2048), jnp.bfloat16),
            pltpu.VMEM((2, 512, 2048), jnp.bfloat16),
            pltpu.VMEM((rows, 2048), jnp.bfloat16),
            pltpu.VMEM((rows, 2048), jnp.bfloat16),
            pltpu.VMEM((PAD + rows, 512), jnp.float32),
            pltpu.VMEM((rows, 512), jnp.bfloat16),
        ],
        compiler_params=pltpu.CompilerParams(vmem_limit_bytes=26 << 20),
        cost_estimate=pl.CostEstimate(
            flops=4 << 30, bytes_accessed=16 << 20, transcendentals=0
        ),
        name="mixer",
    )(place.astype(jnp.int32), halo, tokens, norm_gain, pool_gain, *mine, *theirs)


def gathered(in_weight, down_weight):
    core = lax.axis_index("tp") % 2
    turned = jnp.swapaxes(in_weight, 1, 2).reshape(32, 128)
    first = jnp.where(core == 0, down_weight[0], down_weight[1])
    last = jnp.where(core == 0, down_weight[1], down_weight[0])
    folded = jnp.concatenate([first, last], axis=1)
    block = jnp.concatenate([turned, folded], axis=0)
    column = shared(block, 16, lambda y, x, z, c: (y, x, c))
    line = shared(
        column.reshape(16, 64, 128),
        4,
        lambda y, x, z, c: (y, z, c) if c == 0 else (x, z, c),
    )
    line = line.reshape(4, 16, 64, 128)
    mine = [line]
    for d in (1, -1, 2):
        mine.append(send(line, second_hop(d)))
    theirs = []
    for piece in mine:
        theirs.append(send(piece, other_core))
    return mine, theirs


def mixed(tokens, norm_gain, in_weight, down_weight, pool_gain):
    rows = tokens.shape[1]
    halo = lax.ppermute(
        tokens[0, rows - HALO :], AXES, [(i, i + 32) for i in range(480)]
    )
    mine, theirs = gathered(in_weight, down_weight)
    return mixer(halo, tokens[0], norm_gain, pool_gain, mine, theirs)[None]


def solution(mesh):
    in_specs = (P("tp", "sp", None), P(), P(None, "sp", "tp"), P(None, "sp", "tp"), P())
    out_specs = P("tp", "sp", None)
    return jax.shard_map(
        mixed, mesh=mesh, in_specs=in_specs, out_specs=out_specs, check_vma=False
    )
```

time: 176 us -> 114 us (0.65)
  the two profiles are of different devices: /device:TPU:8 before, /device:TPU:12 now
where the time goes in v1:
time: 114 us
  blocking collectives  46.4 us (41%)
  starting transfers between devices  30.2 us (26%)
  waiting for transfers between devices  19.8 us (17%)
  Pallas kernels  15.4 us (14%)
  other arithmetic  1.57 us (1%)
    all_to_all x2, blocking collectives, shared(): lax.all_to_all(copies, AXES, 0, 0, axis_index_groups=list(groups.values()...  46.4 us
    ppermute x7, starting transfers between devices, send(): return lax.ppermute(block, AXES, route)  28.3 us
    pallas_call x1, Pallas kernels, mixer(): pl.pallas_call(mixer_kernel, out_shape=jax.ShapeDtypeStruct(tokens.shape,...  15.4 us
    ppermute x7, waiting for transfers between devices, send(): return lax.ppermute(block, AXES, route)  14 us
    ppermute x1, waiting for transfers between devices, mixed(): lax.ppermute(tokens[0, rows - HALO:], AXES, [(i, i + 32) for i in range(4...  5.78 us
  transfers between devices with their start and end apart: 8, of which 3 were waited for; matrix products, arithmetic and copies ran while one was open for 0% of the time, Pallas kernels for 0%

profile of v1, /device:TPU:12, one launch (start us, length us, event | category | flops | bytes accessed | tf_op | source)
XLA Modules:
  0.0 113.7 jit_solution(743774244360713266)
XLA Ops:
  0.0 0.7 select_bitcast_fusion.1
  0.7 0.8 maximum_maximum_fusion
  1.5 33.4 %all_to_all.10 = bf16[16,64,128]{2,1,0:T(8,128)(2,1)S(1)} all-to-all(bf16[16,64,128]{2,1,0:T(8,128)(2,1)S(1)} %broadcast_in_dim.6), channel_id=1, replica_groups={{0,2,4,6,8,10,12,14,16,18,20,22,24,26,28,30},{1,3,5,7,9,11,13,15,17,19,..., dimensions={0} | all-to-all | bytes 524288 | tf_op jit(solution)/shard_map/all_to_all | solution.py:34
  34.9 0.0 copy-start
  34.9 0.0 copy-start.1
  34.9 0.0 copy-start.2
  34.9 0.2 broadcast_in_dim.7
  35.2 13.0 %all_to_all.11.refs_0_ = bf16[4,16,64,128]{3,2,1,0:T(8,128)(2,1)S(1)} all-to-all(bf16[4,16,64,128]{3,2,1,0:T(8,128)(2,1)S(1)} %broadcast_in_dim.7), channel_id=1, replica_groups={{0,32,64,96},{1,129,257,385},{2,34,66,98},{3,131,259,387},{4,36,68,100}..., dimensions={0} | all-to-all | bytes 2097152 | tf_op jit(solution)/shard_map/all_to_all | solution.py:34
  48.2 5.0 %collective-permute-start.3 = (bf16[4,16,64,128]{3,2,1,0:T(8,128)(2,1)S(1)}, bf16[4,16,64,128]{3,2,1,0:T(8,128)(2,1)}, u32[]{:S(2)}, u32[]{:S(2)}) collective-permute-start(bf16[4,16,64,128]{3,2,1,0:T(8,128)(2,1)S(1)} %all_to_all.11.refs_0_), channel_id=1, source_target_pairs={{0,256},{1,65},{2,258},{3,67},{4,260},{5,69},{6,262},{7,71},{8,264... | collective-permute-start | bytes 3145736 | tf_op jit(solution)/shard_map/ppermute | solution.py:26
  53.2 13.2 %collective-permute-start.2 = (bf16[4,16,64,128]{3,2,1,0:T(8,128)(2,1)S(1)}, bf16[4,16,64,128]{3,2,1,0:T(8,128)(2,1)}, u32[]{:S(2)}, u32[]{:S(2)}) collective-permute-start(bf16[4,16,64,128]{3,2,1,0:T(8,128)(2,1)S(1)} %all_to_all.11.refs_0_), channel_id=1, source_target_pairs={{0,384},{1,97},{2,386},{3,99},{4,388},{5,101},{6,390},{7,103},{8,3... | collective-permute-start | bytes 3145736 | tf_op jit(solution)/shard_map/ppermute | solution.py:26
  66.4 1.9 %collective-permute-start.1 = (bf16[4,16,64,128]{3,2,1,0:T(8,128)(2,1)S(1)}, bf16[4,16,64,128]{3,2,1,0:T(8,128)(2,1)}, u32[]{:S(2)}, u32[]{:S(2)}) collective-permute-start(bf16[4,16,64,128]{3,2,1,0:T(8,128)(2,1)S(1)} %all_to_all.11.refs_0_), channel_id=1, source_target_pairs={{0,128},{1,33},{2,130},{3,35},{4,132},{5,37},{6,134},{7,39},{8,136... | collective-permute-start | bytes 3145736 | tf_op jit(solution)/shard_map/ppermute | solution.py:26
  68.3 1.9 %collective-permute-start.4 = (bf16[4,16,64,128]{3,2,1,0:T(8,128)(2,1)S(1)}, bf16[4,16,64,128]{3,2,1,0:T(8,128)(2,1)}, u32[]{:S(2)}, u32[]{:S(2)}) collective-permute-start(bf16[4,16,64,128]{3,2,1,0:T(8,128)(2,1)S(1)} %all_to_all.11.refs_0_), channel_id=1, source_target_pairs={{0,1},{1,0},{2,3},{3,2},{4,5},{5,4},{6,7},{7,6},{8,9},{9,8},{10,11... | collective-permute-start | bytes 3145736 | tf_op jit(solution)/shard_map/ppermute | solution.py:26
  70.2 0.0 collective-permute-done.3.refs_3_
  70.2 2.4 %collective-permute-start.7 = (bf16[4,16,64,128]{3,2,1,0:T(8,128)(2,1)}, bf16[4,16,64,128]{3,2,1,0:T(8,128)(2,1)}, u32[]{:S(2)}, u32[]{:S(2)}) collective-permute-start(bf16[4,16,64,128]{3,2,1,0:T(8,128)(2,1)} %collective-permute-done.3.refs_3_), channel_id=1, source_target_pairs={{0,1},{1,0},{2,3},{3,2},{4,5},{5,4},{6,7},{7,6},{8,9},{9,8},{10,11... | collective-permute-start | bytes 3145736 | tf_op jit(solution)/shard_map/ppermute | solution.py:26
  72.7 6.0 %collective-permute-done.2.refs_2_ = bf16[4,16,64,128]{3,2,1,0:T(8,128)(2,1)} collective-permute-done((bf16[4,16,64,128]{3,2,1,0:T(8,128)(2,1)S(1)}, bf16[4,16,64,128]{3,2,1,0:T(8,128)(2,1)}, u32[]{:S(2)}, u32[]{:S(2)}) %collective-permute-start.2) | collective-permute-done | bytes 1048608 | tf_op jit(solution)/shard_map/ppermute | solution.py:26
  78.7 1.9 %collective-permute-start.6 = (bf16[4,16,64,128]{3,2,1,0:T(8,128)(2,1)}, bf16[4,16,64,128]{3,2,1,0:T(8,128)(2,1)}, u32[]{:S(2)}, u32[]{:S(2)}) collective-permute-start(bf16[4,16,64,128]{3,2,1,0:T(8,128)(2,1)} %collective-permute-done.2.refs_2_), channel_id=1, source_target_pairs={{0,1},{1,0},{2,3},{3,2},{4,5},{5,4},{6,7},{7,6},{8,9},{9,8},{10,11... | collective-permute-start | bytes 3145736 | tf_op jit(solution)/shard_map/ppermute | solution.py:26
  80.6 8.0 %collective-permute-done.1.refs_1_ = bf16[4,16,64,128]{3,2,1,0:T(8,128)(2,1)} collective-permute-done((bf16[4,16,64,128]{3,2,1,0:T(8,128)(2,1)S(1)}, bf16[4,16,64,128]{3,2,1,0:T(8,128)(2,1)}, u32[]{:S(2)}, u32[]{:S(2)}) %collective-permute-start.1) | collective-permute-done | bytes 1048608 | tf_op jit(solution)/shard_map/ppermute | solution.py:26
  88.6 1.9 %collective-permute-start.5 = (bf16[4,16,64,128]{3,2,1,0:T(8,128)(2,1)}, bf16[4,16,64,128]{3,2,1,0:T(8,128)(2,1)}, u32[]{:S(2)}, u32[]{:S(2)}) collective-permute-start(bf16[4,16,64,128]{3,2,1,0:T(8,128)(2,1)} %collective-permute-done.1.refs_1_), channel_id=1, source_target_pairs={{0,1},{1,0},{2,3},{3,2},{4,5},{5,4},{6,7},{7,6},{8,9},{9,8},{10,11... | collective-permute-start | bytes 3145736 | tf_op jit(solution)/shard_map/ppermute | solution.py:26
  90.5 0.0 copy-done
  90.5 1.9 %collective-permute-start = (bf16[32,2048]{1,0:T(8,128)(2,1)S(1)}, bf16[32,2048]{1,0:T(8,128)(2,1)S(1)}, u32[]{:S(2)}, u32[]{:S(2)}) collective-permute-start(bf16[32,2048]{1,0:T(8,128)(2,1)S(1)} %slice_bitcast_fusion), channel_id=1, source_target_pairs={{0,32},{1,33},{2,34},{3,35},{4,36},{5,37},{6,38},{7,39},{8,40},{9,... | collective-permute-start | bytes 393224 | tf_op jit(solution)/shard_map/ppermute | solution.py:193
  92.5 0.1 pad_add_fusion.place
  92.5 5.8 %collective-permute-done.halo = bf16[32,2048]{1,0:T(8,128)(2,1)S(1)} collective-permute-done((bf16[32,2048]{1,0:T(8,128)(2,1)S(1)}, bf16[32,2048]{1,0:T(8,128)(2,1)S(1)}, u32[]{:S(2)}, u32[]{:S(2)}) %collective-permute-start) | collective-permute-done | bytes 131104 | tf_op jit(solution)/shard_map/ppermute | solution.py:193
  98.3 0.0 collective-permute-done.4.refs_4_
  98.3 0.0 collective-permute-done.7.refs_7_
  98.3 0.0 collective-permute-done.6.refs_6_
  98.3 0.0 collective-permute-done.5.refs_5_
  98.3 0.0 copy-done.1
  98.4 0.0 copy-done.2
  98.4 15.4 %mixer.1 = bf16[384,2048]{1,0:T(8,128)(2,1)} custom-call(s32[2]{0:T(128)S(1)} %pad_add_fusion.place, bf16[32,2048]{1,0:T(8,128)(2,1)S(1)} %collective-permute-done.halo, bf16[384,2048]{1,0:T(8,128)(2,1)S(1)} %bitcast.13, f32[2,2048]{1,0:T(2,128)S(1)} %copy-done.1, f32[2,512]{1,0:T(2,128)S(1)} %copy-done.2, bf16[4,16,64,128]{3,2,1,0:T(8,128)(2,1)S(1)} %all_to_all.11.refs_0_, ...), custom_call_target="tpu_custom_call" | custom-call | flops 4294967296 | bytes 16777216 | tf_op jit(solution)/shard_map/mixer/pallas_call | solution.py:147
  (2 shorter events, 0.1 us)
Async XLA Ops:
  34.9 55.6 %copy-start = (bf16[1,384,2048]{2,1,0:T(8,128)(2,1)S(1)}, bf16[1,384,2048]{2,1,0:T(8,128)(2,1)}, u32[]{:S(2)}) copy-start(bf16[1,384,2048]{2,1,0:T(8,128)(2,1)} %param.5) | copy-start | bytes 4718596
  34.9 63.4 %copy-start.1 = (f32[2,2048]{1,0:T(2,128)S(1)}, f32[2,2048]{1,0:T(2,128)}, u32[]{:S(2)}) copy-start(f32[2,2048]{1,0:T(2,128)} %norm_gain.1) | copy-start | bytes 49156
  34.9 63.4 %copy-start.2 = (f32[2,512]{1,0:T(2,128)S(1)}, f32[2,512]{1,0:T(2,128)}, u32[]{:S(2)}) copy-start(f32[2,512]{1,0:T(2,128)} %pool_gain.1) | copy-start | bytes 12292
  48.2 22.1 %collective-permute-start.3 = (bf16[4,16,64,128]{3,2,1,0:T(8,128)(2,1)S(1)}, bf16[4,16,64,128]{3,2,1,0:T(8,128)(2,1)}, u32[]{:S(2)}, u32[]{:S(2)}) collective-permute-start(bf16[4,16,64,128]{3,2,1,0:T(8,128)(2,1)S(1)} %all_to_all.11.refs_0_), channel_id=1, source_target_pairs={{0,256},{1,65},{2,258},{3,67},{4,260},{5,69},{6,262},{7,71},{8,264... | collective-permute-start | bytes 3145736 | tf_op jit(solution)/shard_map/ppermute | solution.py:26
  53.2 25.5 %collective-permute-start.2 = (bf16[4,16,64,128]{3,2,1,0:T(8,128)(2,1)S(1)}, bf16[4,16,64,128]{3,2,1,0:T(8,128)(2,1)}, u32[]{:S(2)}, u32[]{:S(2)}) collective-permute-start(bf16[4,16,64,128]{3,2,1,0:T(8,128)(2,1)S(1)} %all_to_all.11.refs_0_), channel_id=1, source_target_pairs={{0,384},{1,97},{2,386},{3,99},{4,388},{5,101},{6,390},{7,103},{8,3... | collective-permute-start | bytes 3145736 | tf_op jit(solution)/shard_map/ppermute | solution.py:26
  66.4 22.2 %collective-permute-start.1 = (bf16[4,16,64,128]{3,2,1,0:T(8,128)(2,1)S(1)}, bf16[4,16,64,128]{3,2,1,0:T(8,128)(2,1)}, u32[]{:S(2)}, u32[]{:S(2)}) collective-permute-start(bf16[4,16,64,128]{3,2,1,0:T(8,128)(2,1)S(1)} %all_to_all.11.refs_0_), channel_id=1, source_target_pairs={{0,128},{1,33},{2,130},{3,35},{4,132},{5,37},{6,134},{7,39},{8,136... | collective-permute-start | bytes 3145736 | tf_op jit(solution)/shard_map/ppermute | solution.py:26
  68.3 30.0 %collective-permute-start.4 = (bf16[4,16,64,128]{3,2,1,0:T(8,128)(2,1)S(1)}, bf16[4,16,64,128]{3,2,1,0:T(8,128)(2,1)}, u32[]{:S(2)}, u32[]{:S(2)}) collective-permute-start(bf16[4,16,64,128]{3,2,1,0:T(8,128)(2,1)S(1)} %all_to_all.11.refs_0_), channel_id=1, source_target_pairs={{0,1},{1,0},{2,3},{3,2},{4,5},{5,4},{6,7},{7,6},{8,9},{9,8},{10,11... | collective-permute-start | bytes 3145736 | tf_op jit(solution)/shard_map/ppermute | solution.py:26
  70.2 28.1 %collective-permute-start.7 = (bf16[4,16,64,128]{3,2,1,0:T(8,128)(2,1)}, bf16[4,16,64,128]{3,2,1,0:T(8,128)(2,1)}, u32[]{:S(2)}, u32[]{:S(2)}) collective-permute-start(bf16[4,16,64,128]{3,2,1,0:T(8,128)(2,1)} %collective-permute-done.3.refs_3_), channel_id=1, source_target_pairs={{0,1},{1,0},{2,3},{3,2},{4,5},{5,4},{6,7},{7,6},{8,9},{9,8},{10,11... | collective-permute-start | bytes 3145736 | tf_op jit(solution)/shard_map/ppermute | solution.py:26
  78.7 19.7 %collective-permute-start.6 = (bf16[4,16,64,128]{3,2,1,0:T(8,128)(2,1)}, bf16[4,16,64,128]{3,2,1,0:T(8,128)(2,1)}, u32[]{:S(2)}, u32[]{:S(2)}) collective-permute-start(bf16[4,16,64,128]{3,2,1,0:T(8,128)(2,1)} %collective-permute-done.2.refs_2_), channel_id=1, source_target_pairs={{0,1},{1,0},{2,3},{3,2},{4,5},{5,4},{6,7},{7,6},{8,9},{9,8},{10,11... | collective-permute-start | bytes 3145736 | tf_op jit(solution)/shard_map/ppermute | solution.py:26
  88.6 9.8 %collective-permute-start.5 = (bf16[4,16,64,128]{3,2,1,0:T(8,128)(2,1)}, bf16[4,16,64,128]{3,2,1,0:T(8,128)(2,1)}, u32[]{:S(2)}, u32[]{:S(2)}) collective-permute-start(bf16[4,16,64,128]{3,2,1,0:T(8,128)(2,1)} %collective-permute-done.1.refs_1_), channel_id=1, source_target_pairs={{0,1},{1,0},{2,3},{3,2},{4,5},{5,4},{6,7},{7,6},{8,9},{9,8},{10,11... | collective-permute-start | bytes 3145736 | tf_op jit(solution)/shard_map/ppermute | solution.py:26
  90.5 7.8 %collective-permute-start = (bf16[32,2048]{1,0:T(8,128)(2,1)S(1)}, bf16[32,2048]{1,0:T(8,128)(2,1)S(1)}, u32[]{:S(2)}, u32[]{:S(2)}) collective-permute-start(bf16[32,2048]{1,0:T(8,128)(2,1)S(1)} %slice_bitcast_fusion), channel_id=1, source_target_pairs={{0,32},{1,33},{2,34},{3,35},{4,36},{5,37},{6,38},{7,39},{8,40},{9,... | collective-permute-start | bytes 393224 | tf_op jit(solution)/shard_map/ppermute | solution.py:193

commit v2 on v1

v2 whole, which is shorter than its diff:
```python
import jax
import jax.numpy as jnp
from jax import lax
from jax.experimental import pallas as pl
from jax.experimental.pallas import tpu as pltpu
from jax.sharding import PartitionSpec as P

EPS = 1e-06
HALO = 32
PAD = 16
AXES = ("sp", "tp")
PIECES = ((0, 0, 4), (-1, 0, 4), (1, 0, 4), (2, 0, 2), (2, 2, 4))
HEAD_MIB, PUT_MIB, MIX_MIB = 5, 10, 16
VMEM = pl.BlockSpec(memory_space=pltpu.VMEM)
SMEM = pl.BlockSpec(memory_space=pltpu.SMEM)


def number(y, x, z, c):
    return (((y % 4) * 4 + x % 4) * 16 + z % 16) * 2 + c


def places():
    for i in range(512):
        yield i, (i // 128, i // 32 % 4, i // 2 % 16, i % 2)


def send(block, target):
    route = [(i, number(*target(*place))) for i, place in places()]
    return lax.ppermute(block, AXES, route)


def shared(block, count, key):
    groups = {}
    for i, place in places():
        groups.setdefault(key(*place), []).append(i)
    copies = jnp.broadcast_to(block[None], (count, *block.shape))
    return lax.all_to_all(
        copies, AXES, 0, 0, axis_index_groups=list(groups.values()), tiled=True
    )


def second_hop(d):
    return lambda y, x, z, c: (y + d, x, z, c) if c == 0 else (y, x + d, z, c)


def other_core(y, x, z, c):
    return y, x, z, 1 - c


def seconds(place):
    sp, c = place[0], place[1]
    y, x = sp // 4, sp % 4
    return c, jnp.where(c == 0, y, x), jnp.where(c == 0, x, y)


def put(place, mine, theirs, new, whole_in, whole_down):
    c, s_mine, s_theirs = seconds(place)
    left = (lax.broadcasted_iota(jnp.int32, (32, 128), 1) < 64) ^ (c == 1)

    for pieces, core, second in ((mine, c, s_mine), (theirs, 1 - c, s_theirs)):
        for k in new:
            d, low, high = PIECES[k]
            s = (second + d + 4) % 4

            def put_in(i, carry, pieces=pieces, core=core, k=k, s=s, low=low):
                f = i + low
                at = jnp.where(core == 0, s * 4 + f, f * 4 + s)
                lanes = pl.ds(pl.multiple_of(at * 128, 128), 128)
                for l in range(2):
                    whole_in[l, :, core, :, lanes] = pieces[k][
                        i, :, l * 16 : (l + 1) * 16
                    ]
                return carry

            lax.fori_loop(0, high - low, put_in, 0)

    for k in range(max(new) + 1):
        for j in range(max(new) + 1):
            if k not in new and j not in new:
                continue
            a = (s_mine + PIECES[k][0] + 4) % 4
            b = (s_theirs + PIECES[j][0] + 4) % 4
            (_, k_low, k_high), (_, j_low, j_high) = PIECES[k], PIECES[j]

            def put_down(k=k, j=j, a=a, b=b, k_low=k_low, j_low=j_low):
                at = jnp.where(c == 0, a * 4 + b, b * 4 + a)
                rows = pl.ds(pl.multiple_of(at * 32, 32), 32)
                for z in range(16):
                    m = mine[k][b - k_low, z, 32:64]
                    t = theirs[j][a - j_low, z, 32:64]
                    lanes = slice(z * 128, (z + 1) * 128)
                    whole_down[0, rows, lanes] = jnp.where(left, m, t)
                    v = jnp.where(left, t, m)
                    whole_down[1, rows, lanes] = jnp.concatenate(
                        [v[:, 64:], v[:, :64]], axis=1
                    )

            if k > 2 or j > 2:
                here = (b >= k_low) & (b < k_high) & (a >= j_low) & (a < j_high)
                pl.when(here)(put_down)
            else:
                put_down()


def wholes():
    return (
        jax.ShapeDtypeStruct((2, 16, 2, 16, 2048), jnp.bfloat16),
        jax.ShapeDtypeStruct((2, 512, 2048), jnp.bfloat16),
    )


def params(mib):
    return pltpu.CompilerParams(vmem_limit_bytes=mib << 20)


def cost(flops):
    return pl.CostEstimate(flops=flops, bytes_accessed=1 << 20, transcendentals=0)


def placed(place, mine, theirs, new, wholes_before=()):
    count = max(new) + 1

    def kernel(place, *refs):
        put(place, refs[:count], refs[count : 2 * count], new, refs[-2], refs[-1])

    at = 1 + 2 * count
    return pl.pallas_call(
        kernel,
        out_shape=wholes(),
        in_specs=[SMEM] + [VMEM] * (2 * count + len(wholes_before)),
        out_specs=(VMEM, VMEM),
        input_output_aliases={at: 0, at + 1: 1} if wholes_before else {},
        compiler_params=params(PUT_MIB),
        cost_estimate=cost(1 << 29),
    )(place, *mine[:count], *theirs[:count], *wholes_before)


def norm_rows(block, gain):
    residual = block.astype(jnp.float32)
    mean = jnp.mean(residual * residual, axis=1, keepdims=True)
    return (residual * lax.rsqrt(mean + EPS) * gain).astype(jnp.bfloat16)


def head_kernel(tokens, norm_gain, normed):
    def norm(i, carry):
        rows = pl.multiple_of(i * 32, 32)
        normed[pl.ds(HALO + rows, 32)] = norm_rows(
            tokens[pl.ds(rows, 32)], norm_gain[0:1]
        )
        return carry

    lax.fori_loop(0, tokens.shape[0] // 32, norm, 0)


def head(tokens, norm_gain):
    return pl.pallas_call(
        head_kernel,
        out_shape=jax.ShapeDtypeStruct((HALO + tokens.shape[0], 2048), jnp.bfloat16),
        in_specs=[VMEM] * 2,
        out_specs=VMEM,
        compiler_params=params(HEAD_MIB),
        cost_estimate=cost(1 << 30),
        name="head",
    )(tokens, norm_gain)


def mixer_kernel(place, halo, tokens, normed, norm_gain, pool_gain, *refs):
    count = len(PIECES)
    mine, theirs = refs[:count], refs[count : 2 * count]
    out, whole_in, whole_down, left, extended, pooled, middle = refs[-7:]
    put(place, mine, theirs, (3, 4), whole_in, whole_down)
    rows = left.shape[0]
    left[:HALO] = norm_rows(halo[...], norm_gain[0:1])
    extended[:PAD] = jnp.zeros((PAD, 512), jnp.float32)
    row = lax.broadcasted_iota(jnp.int32, (rows, 128), 0)
    lane = lax.broadcasted_iota(jnp.int32, (rows, 128), 1)
    position = place[0] * 384 - HALO + row + 1
    position = jnp.maximum(position, 1).astype(jnp.float32)

    def pool(l, row_scale):
        pool_in = lax.dot_general(
            left[...],
            whole_in[l].reshape(512, 2048),
            (((1,), (1,)), ((), ())),
            preferred_element_type=jnp.float32,
        )
        if row_scale is not None:
            pool_in = pool_in * row_scale
        extended[PAD:] = pool_in.astype(jnp.bfloat16).astype(jnp.float32)
        for j in range(4):
            lanes = slice(j * 128, (j + 1) * 128)
            own = extended[:, lanes]
            two = own + pltpu.roll(own, 1, 0)
            four = two + pltpu.roll(two, 2, 0)
            short, long, window = two, four, 2.0
            if j % 2:
                eight = four + pltpu.roll(four, 4, 0)
                short, long, window = eight, eight + pltpu.roll(eight, 8, 0), 8.0
            total = jnp.where(lane < 64, short[PAD:], long[PAD:])
            width = jnp.where(lane < 64, window, 2 * window)
            trailing = total / jnp.minimum(position, width) - own[PAD:]
            gain = pool_gain[l : l + 1, lanes]
            pooled[:, lanes] = (trailing * gain).astype(jnp.bfloat16)

    pool(0, None)
    squares = jnp.zeros((rows, 128), jnp.float32)
    for j in range(4):
        lanes = slice(j * 512, (j + 1) * 512)
        down = jnp.dot(
            pooled[...], whole_down[0, :, lanes], preferred_element_type=jnp.float32
        )
        before = jnp.concatenate([halo[:, lanes], tokens[:, lanes]], axis=0)
        total = before.astype(jnp.float32) + down
        middle[:, lanes] = total.astype(jnp.bfloat16)
        total = middle[:, lanes].astype(jnp.float32)
        left[:, lanes] = (total * norm_gain[1:2, lanes]).astype(jnp.bfloat16)
        total = total * total
        squares += (total[:, :128] + total[:, 128:256]) + (
            total[:, 256:384] + total[:, 384:]
        )
    mean = jnp.sum(squares, axis=1, keepdims=True) / 2048.0
    pool(1, lax.rsqrt(mean + EPS))
    for j in range(4):
        lanes = slice(j * 512, (j + 1) * 512)
        down = jnp.dot(
            pooled[HALO:], whole_down[1, :, lanes], preferred_element_type=jnp.float32
        )
        total = middle[HALO:, lanes].astype(jnp.float32) + down
        out[:, lanes] = total.astype(jnp.bfloat16)


def mixer(place, halo, tokens, normed, norm_gain, pool_gain, mine, theirs, whole):
    rows = normed.shape[0]
    at = 6 + 2 * len(PIECES)
    return pl.pallas_call(
        mixer_kernel,
        out_shape=(
            jax.ShapeDtypeStruct(tokens.shape, tokens.dtype),
            *wholes(),
            jax.ShapeDtypeStruct(normed.shape, normed.dtype),
        ),
        in_specs=[SMEM] + [VMEM] * (at + 1),
        out_specs=(VMEM,) * 4,
        input_output_aliases={at: 1, at + 1: 2, 3: 3},
        scratch_shapes=[
            pltpu.VMEM((PAD + rows, 512), jnp.float32),
            pltpu.VMEM((rows, 512), jnp.bfloat16),
            pltpu.VMEM((rows, 2048), jnp.bfloat16),
        ],
        compiler_params=params(MIX_MIB),
        cost_estimate=cost(4 << 30),
        name="mixer",
    )(place, halo, tokens, normed, norm_gain, pool_gain, *mine, *theirs, *whole)[0]


def packed(in_weight, down_weight):
    core = lax.axis_index("tp") % 2
    turned = jnp.swapaxes(in_weight, 1, 2).reshape(32, 128)
    first = jnp.where(core == 0, down_weight[0], down_weight[1])
    last = jnp.where(core == 0, down_weight[1], down_weight[0])
    return jnp.concatenate([turned, jnp.concatenate([first, last], axis=1)], axis=0)


def mixed(tokens, norm_gain, in_weight, down_weight, pool_gain):
    rows = tokens.shape[1]
    place = jnp.stack([lax.axis_index("sp"), lax.axis_index("tp") % 2])
    place = place.astype(jnp.int32)
    halo = lax.ppermute(
        tokens[0, rows - HALO :], AXES, [(i, i + 32) for i in range(480)]
    )
    normed = head(tokens[0], norm_gain)
    column = shared(packed(in_weight, down_weight), 16, lambda y, x, z, c: (y, x, c))
    line = shared(
        column.reshape(16, 64, 128),
        4,
        lambda y, x, z, c: (y, z, c) if c == 0 else (x, z, c),
    )
    line = line.reshape(4, 16, 64, 128)
    up = send(line, second_hop(1))
    down = send(line, second_hop(-1))
    up_on = send(up[:2], second_hop(1))
    down_on = send(down[2:], second_hop(-1))
    mine = [line, up, down, up_on, down_on]
    theirs = [send(piece, other_core) for piece in mine]
    whole = placed(place, mine, theirs, (0,))
    whole = placed(place, mine, theirs, (1, 2), whole)
    return mixer(
        place, halo, tokens[0], normed, norm_gain, pool_gain, mine, theirs, whole
    )[None]


def solution(mesh):
    in_specs = (P("tp", "sp", None), P(), P(None, "sp", "tp"), P(None, "sp", "tp"), P())
    out_specs = P("tp", "sp", None)
    return jax.shard_map(
        mixed, mesh=mesh, in_specs=in_specs, out_specs=out_specs, check_vma=False
    )
```

time: 114 us -> 114 us (level)
  the two profiles are of different devices: /device:TPU:12 before, /device:TPU:1 now
where the time goes in v2:
time: 114 us
  starting transfers between devices  47.2 us (41%)
  blocking collectives  43 us (38%)
  Pallas kernels  15.4 us (14%)
  local copies, waits for them, and re-layouts  5.32 us (5%)
  other arithmetic  1.58 us (1%)
    ppermute x9, starting transfers between devices, send(): return lax.ppermute(block, AXES, route)  43.2 us
    all_to_all x2, blocking collectives, shared(): lax.all_to_all(copies, AXES, 0, 0, axis_index_groups=list(groups.values()...  43 us
    pallas_call x1, Pallas kernels, mixer(): pl.pallas_call(mixer_kernel, out_shape=(jax.ShapeDtypeStruct(tokens.shape...  9.58 us
    pallas_call x2, Pallas kernels, placed(): pl.pallas_call(kernel, out_shape=wholes(), in_specs=[SMEM] + [VMEM] * (2...  4.27 us
    ppermute x1, starting transfers between devices, mixed(): lax.ppermute(tokens[0, rows - HALO:], AXES, [(i, i + 32) for i in range(4...  4.03 us
  transfers between devices with their start and end apart: 10, of which 1 were waited for; matrix products, arithmetic and copies ran while one was open for 3% of the time, Pallas kernels for 5%

profile of v2, /device:TPU:1, one launch (start us, length us, event | category | flops | bytes accessed | tf_op | source)
XLA Modules:
  0.0 113.6 jit_solution(14815181923384485239)
XLA Ops:
  0.0 0.0 copy-start.2
  0.0 0.7 select_bitcast_fusion.1
  0.7 0.8 maximum_maximum_fusion
  1.6 29.3 %all_to_all.10 = bf16[16,64,128]{2,1,0:T(8,128)(2,1)S(1)} all-to-all(bf16[16,64,128]{2,1,0:T(8,128)(2,1)S(1)} %broadcast_in_dim.6), channel_id=1, replica_groups={{0,2,4,6,8,10,12,14,16,18,20,22,24,26,28,30},{1,3,5,7,9,11,13,15,17,19,..., dimensions={0} | all-to-all | bytes 524288 | tf_op jit(solution)/shard_map/all_to_all | solution.py:37
  30.9 0.2 broadcast_in_dim.7
  31.1 13.7 %all_to_all.11.refs_0_ = bf16[4,16,64,128]{3,2,1,0:T(8,128)(2,1)S(1)} all-to-all(bf16[4,16,64,128]{3,2,1,0:T(8,128)(2,1)S(1)} %broadcast_in_dim.7), channel_id=1, replica_groups={{0,32,64,96},{1,129,257,385},{2,34,66,98},{3,131,259,387},{4,36,68,100}..., dimensions={0} | all-to-all | bytes 2097152 | tf_op jit(solution)/shard_map/all_to_all | solution.py:37
  44.8 4.7 %collective-permute-start.2 = (bf16[4,16,64,128]{3,2,1,0:T(8,128)(2,1)S(1)}, bf16[4,16,64,128]{3,2,1,0:T(8,128)(2,1)S(1)}, u32[]{:S(2)}, u32[]{:S(2)}) collective-permute-start(bf16[4,16,64,128]{3,2,1,0:T(8,128)(2,1)S(1)} %all_to_all.11.refs_0_), channel_id=1, source_target_pairs={{0,384},{1,97},{2,386},{3,99},{4,388},{5,101},{6,390},{7,103},{8,3... | collective-permute-start | bytes 3145736 | tf_op jit(solution)/shard_map/ppermute | solution.py:29
  49.5 1.9 %collective-permute-start.1 = (bf16[4,16,64,128]{3,2,1,0:T(8,128)(2,1)S(1)}, bf16[4,16,64,128]{3,2,1,0:T(8,128)(2,1)}, u32[]{:S(2)}, u32[]{:S(2)}) collective-permute-start(bf16[4,16,64,128]{3,2,1,0:T(8,128)(2,1)S(1)} %all_to_all.11.refs_0_), channel_id=1, source_target_pairs={{0,128},{1,33},{2,130},{3,35},{4,132},{5,37},{6,134},{7,39},{8,136... | collective-permute-start | bytes 3145736 | tf_op jit(solution)/shard_map/ppermute | solution.py:29
  51.5 9.0 %collective-permute-start.5 = (bf16[4,16,64,128]{3,2,1,0:T(8,128)(2,1)S(1)}, bf16[4,16,64,128]{3,2,1,0:T(8,128)(2,1)S(1)}, u32[]{:S(2)}, u32[]{:S(2)}) collective-permute-start(bf16[4,16,64,128]{3,2,1,0:T(8,128)(2,1)S(1)} %all_to_all.11.refs_0_), channel_id=1, source_target_pairs={{0,1},{1,0},{2,3},{3,2},{4,5},{5,4},{6,7},{7,6},{8,9},{9,8},{10,11... | collective-permute-start | bytes 3145736 | tf_op jit(solution)/shard_map/ppermute | solution.py:29
  60.4 0.8 collective-permute-done.2.refs_2_
  61.2 0.8 slice.23
  62.1 5.0 %collective-permute-start.4 = (bf16[2,16,64,128]{3,2,1,0:T(8,128)(2,1)}, bf16[2,16,64,128]{3,2,1,0:T(8,128)(2,1)}, u32[]{:S(2)}, u32[]{:S(2)}) collective-permute-start(bf16[2,16,64,128]{3,2,1,0:T(8,128)(2,1)} %slice.23), channel_id=1, source_target_pairs={{0,384},{1,97},{2,386},{3,99},{4,388},{5,101},{6,390},{7,103},{8,3... | collective-permute-start | bytes 1572872 | tf_op jit(solution)/shard_map/ppermute | solution.py:29
  67.1 0.0 collective-permute-done.1.refs_1_
  67.1 1.9 %slice.22 = bf16[2,16,64,128]{3,2,1,0:T(8,128)(2,1)} slice(bf16[4,16,64,128]{3,2,1,0:T(8,128)(2,1)} %collective-permute-done.1.refs_1_), slice={[0:2], [0:16], [0:64], [0:128]} | slice | bytes 1048576 | tf_op jit(solution)/shard_map/slice | solution.py:281
  69.0 1.9 %collective-permute-start.3 = (bf16[2,16,64,128]{3,2,1,0:T(8,128)(2,1)}, bf16[2,16,64,128]{3,2,1,0:T(8,128)(2,1)}, u32[]{:S(2)}, u32[]{:S(2)}) collective-permute-start(bf16[2,16,64,128]{3,2,1,0:T(8,128)(2,1)} %slice.22), channel_id=1, source_target_pairs={{0,128},{1,33},{2,130},{3,35},{4,132},{5,37},{6,134},{7,39},{8,136... | collective-permute-start | bytes 1572872 | tf_op jit(solution)/shard_map/ppermute | solution.py:29
  70.9 10.1 %collective-permute-start.7 = (bf16[4,16,64,128]{3,2,1,0:T(8,128)(2,1)S(1)}, bf16[4,16,64,128]{3,2,1,0:T(8,128)(2,1)}, u32[]{:S(2)}, u32[]{:S(2)}) collective-permute-start(bf16[4,16,64,128]{3,2,1,0:T(8,128)(2,1)S(1)} %collective-permute-done.2.refs_2_), channel_id=1, source_target_pairs={{0,1},{1,0},{2,3},{3,2},{4,5},{5,4},{6,7},{7,6},{8,9},{9,8},{10,11... | collective-permute-start | bytes 3145736 | tf_op jit(solution)/shard_map/ppermute | solution.py:29
  81.0 1.9 %collective-permute-start.6 = (bf16[4,16,64,128]{3,2,1,0:T(8,128)(2,1)}, bf16[4,16,64,128]{3,2,1,0:T(8,128)(2,1)}, u32[]{:S(2)}, u32[]{:S(2)}) collective-permute-start(bf16[4,16,64,128]{3,2,1,0:T(8,128)(2,1)} %collective-permute-done.1.refs_1_), channel_id=1, source_target_pairs={{0,1},{1,0},{2,3},{3,2},{4,5},{5,4},{6,7},{7,6},{8,9},{9,8},{10,11... | collective-permute-start | bytes 3145736 | tf_op jit(solution)/shard_map/ppermute | solution.py:29
  83.0 0.1 pad_add_fusion.place
  83.0 0.0 collective-permute-done.4.refs_4_
  83.0 2.4 %collective-permute-start.9 = (bf16[2,16,64,128]{3,2,1,0:T(8,128)(2,1)}, bf16[2,16,64,128]{3,2,1,0:T(8,128)(2,1)S(1)}, u32[]{:S(2)}, u32[]{:S(2)}) collective-permute-start(bf16[2,16,64,128]{3,2,1,0:T(8,128)(2,1)} %collective-permute-done.4.refs_4_), channel_id=1, source_target_pairs={{0,1},{1,0},{2,3},{3,2},{4,5},{5,4},{6,7},{7,6},{8,9},{9,8},{10,11... | collective-permute-start | bytes 1572872 | tf_op jit(solution)/shard_map/ppermute | solution.py:29
  85.4 0.0 collective-permute-done.3.refs_3_
  85.5 6.2 %collective-permute-start.8 = (bf16[2,16,64,128]{3,2,1,0:T(8,128)(2,1)}, bf16[2,16,64,128]{3,2,1,0:T(8,128)(2,1)S(1)}, u32[]{:S(2)}, u32[]{:S(2)}) collective-permute-start(bf16[2,16,64,128]{3,2,1,0:T(8,128)(2,1)} %collective-permute-done.3.refs_3_), channel_id=1, source_target_pairs={{0,1},{1,0},{2,3},{3,2},{4,5},{5,4},{6,7},{7,6},{8,9},{9,8},{10,11... | collective-permute-start | bytes 1572872 | tf_op jit(solution)/shard_map/ppermute | solution.py:29
  91.7 0.9 slice_bitcast_fusion
  92.6 0.0 collective-permute-done.5.refs_1_.refs_3_.refs_5_
  92.6 4.0 %collective-permute-start = (bf16[32,2048]{1,0:T(8,128)(2,1)S(1)}, bf16[32,2048]{1,0:T(8,128)(2,1)S(1)}, u32[]{:S(2)}, u32[]{:S(2)}) collective-permute-start(bf16[32,2048]{1,0:T(8,128)(2,1)S(1)} %slice_bitcast_fusion), channel_id=1, source_target_pairs={{0,32},{1,33},{2,34},{3,35},{4,36},{5,37},{6,38},{7,39},{8,40},{9,... | collective-permute-start | bytes 393224 | tf_op jit(solution)/shard_map/ppermute | solution.py:268
  96.7 0.0 copy-done.2
  96.7 0.0 copy-start
  96.7 1.4 %copy-done = bf16[1,384,2048]{2,1,0:T(8,128)(2,1)S(1)} copy-done((bf16[1,384,2048]{2,1,0:T(8,128)(2,1)S(1)}, bf16[1,384,2048]{2,1,0:T(8,128)(2,1)}, u32[]{:S(2)}) %copy-start) | copy-done | bytes 1572888
  98.1 1.6 %head.1.normed = bf16[416,2048]{1,0:T(8,128)(2,1)S(1)} custom-call(bf16[384,2048]{1,0:T(8,128)(2,1)S(1)} %bitcast.13, f32[2,2048]{1,0:T(2,128)S(1)} %copy-done.2), custom_call_target="tpu_custom_call" | custom-call | flops 1073741824 | bytes 1048576 | tf_op jit(solution)/shard_map/head/pallas_call | solution.py:156
  99.7 1.0 shard_map.55
  100.6 0.0 collective-permute-done.7.refs_5_.refs_7_
  100.6 0.0 collective-permute-done.6.refs_4_.refs_6_
  100.7 0.0 copy-start.1
  100.7 0.0 copy-start.3
  100.7 3.3 %shard_map.56 = (bf16[2,16,2,16,2048]{4,3,2,1,0:T(8,128)(2,1)S(1)}, bf16[2,512,2048]{2,1,0:T(8,128)(2,1)S(1)}) custom-call(s32[2]{0:T(128)S(1)} %pad_add_fusion.place, bf16[4,16,64,128]{3,2,1,0:T(8,128)(2,1)S(1)} %all_to_all.11.refs_0_, bf16[4,16,64,128]{3,2,1,0:T(8,128)(2,1)} %collective-permute-done.1.refs_1_, ...), custom_call_target="tpu_custom_call", output_to_operand_aliasing={{0}: (7, {}), {1}: (8, {})} | custom-call | flops 536870912 | bytes 1048576 | tf_op jit(solution)/shard_map/pallas_call | solution.py:127
  104.0 0.0 collective-permute-done.halo
  104.0 0.0 collective-permute-done.9.refs_9_
  104.0 0.0 collective-permute-done.8.refs_8_
  104.0 0.0 copy-done.1
  104.0 0.0 copy-done.3
  104.0 9.6 %mixer.1 = (bf16[384,2048]{1,0:T(8,128)(2,1)}, bf16[2,16,2,16,2048]{4,3,2,1,0:T(8,128)(2,1)S(1)}, bf16[2,512,2048]{2,1,0:T(8,128)(2,1)S(1)}, bf16[416,2048]{1,0:T(8,128)(2,1)S(1)}) custom-call(s32[2]{0:T(128)S(1)} %pad_add_fusion.place, bf16[32,2048]{1,0:T(8,128)(2,1)S(1)} %collective-permute-done.halo, ...), custom_call_target="tpu_custom_call", output_to_operand_aliasing={{1}: (16, {}), {2}: (17, {}), {3}: (3, {})} | custom-call | flops 4294967296 | bytes 1048576 | tf_op jit(solution)/shard_map/mixer/pallas_call | solution.py:235
  (1 shorter events, 0.0 us)
Async XLA Ops:
  0.0 96.7 %copy-start.2 = (f32[2,2048]{1,0:T(2,128)S(1)}, f32[2,2048]{1,0:T(2,128)}, u32[]{:S(2)}) copy-start(f32[2,2048]{1,0:T(2,128)} %norm_gain.3) | copy-start | bytes 49156
  44.8 16.4 %collective-permute-start.2 = (bf16[4,16,64,128]{3,2,1,0:T(8,128)(2,1)S(1)}, bf16[4,16,64,128]{3,2,1,0:T(8,128)(2,1)S(1)}, u32[]{:S(2)}, u32[]{:S(2)}) collective-permute-start(bf16[4,16,64,128]{3,2,1,0:T(8,128)(2,1)S(1)} %all_to_all.11.refs_0_), channel_id=1, source_target_pairs={{0,384},{1,97},{2,386},{3,99},{4,388},{5,101},{6,390},{7,103},{8,3... | collective-permute-start | bytes 3145736 | tf_op jit(solution)/shard_map/ppermute | solution.py:29
  49.5 17.6 %collective-permute-start.1 = (bf16[4,16,64,128]{3,2,1,0:T(8,128)(2,1)S(1)}, bf16[4,16,64,128]{3,2,1,0:T(8,128)(2,1)}, u32[]{:S(2)}, u32[]{:S(2)}) collective-permute-start(bf16[4,16,64,128]{3,2,1,0:T(8,128)(2,1)S(1)} %all_to_all.11.refs_0_), channel_id=1, source_target_pairs={{0,128},{1,33},{2,130},{3,35},{4,132},{5,37},{6,134},{7,39},{8,136... | collective-permute-start | bytes 3145736 | tf_op jit(solution)/shard_map/ppermute | solution.py:29
  51.5 41.2 %collective-permute-start.5 = (bf16[4,16,64,128]{3,2,1,0:T(8,128)(2,1)S(1)}, bf16[4,16,64,128]{3,2,1,0:T(8,128)(2,1)S(1)}, u32[]{:S(2)}, u32[]{:S(2)}) collective-permute-start(bf16[4,16,64,128]{3,2,1,0:T(8,128)(2,1)S(1)} %all_to_all.11.refs_0_), channel_id=1, source_target_pairs={{0,1},{1,0},{2,3},{3,2},{4,5},{5,4},{6,7},{7,6},{8,9},{9,8},{10,11... | collective-permute-start | bytes 3145736 | tf_op jit(solution)/shard_map/ppermute | solution.py:29
  62.1 21.0 %collective-permute-start.4 = (bf16[2,16,64,128]{3,2,1,0:T(8,128)(2,1)}, bf16[2,16,64,128]{3,2,1,0:T(8,128)(2,1)}, u32[]{:S(2)}, u32[]{:S(2)}) collective-permute-start(bf16[2,16,64,128]{3,2,1,0:T(8,128)(2,1)} %slice.23), channel_id=1, source_target_pairs={{0,384},{1,97},{2,386},{3,99},{4,388},{5,101},{6,390},{7,103},{8,3... | collective-permute-start | bytes 1572872 | tf_op jit(solution)/shard_map/ppermute | solution.py:29
  69.0 16.5 %collective-permute-start.3 = (bf16[2,16,64,128]{3,2,1,0:T(8,128)(2,1)}, bf16[2,16,64,128]{3,2,1,0:T(8,128)(2,1)}, u32[]{:S(2)}, u32[]{:S(2)}) collective-permute-start(bf16[2,16,64,128]{3,2,1,0:T(8,128)(2,1)} %slice.22), channel_id=1, source_target_pairs={{0,128},{1,33},{2,130},{3,35},{4,132},{5,37},{6,134},{7,39},{8,136... | collective-permute-start | bytes 1572872 | tf_op jit(solution)/shard_map/ppermute | solution.py:29
  70.9 29.7 %collective-permute-start.7 = (bf16[4,16,64,128]{3,2,1,0:T(8,128)(2,1)S(1)}, bf16[4,16,64,128]{3,2,1,0:T(8,128)(2,1)}, u32[]{:S(2)}, u32[]{:S(2)}) collective-permute-start(bf16[4,16,64,128]{3,2,1,0:T(8,128)(2,1)S(1)} %collective-permute-done.2.refs_2_), channel_id=1, source_target_pairs={{0,1},{1,0},{2,3},{3,2},{4,5},{5,4},{6,7},{7,6},{8,9},{9,8},{10,11... | collective-permute-start | bytes 3145736 | tf_op jit(solution)/shard_map/ppermute | solution.py:29
  81.0 19.6 %collective-permute-start.6 = (bf16[4,16,64,128]{3,2,1,0:T(8,128)(2,1)}, bf16[4,16,64,128]{3,2,1,0:T(8,128)(2,1)}, u32[]{:S(2)}, u32[]{:S(2)}) collective-permute-start(bf16[4,16,64,128]{3,2,1,0:T(8,128)(2,1)} %collective-permute-done.1.refs_1_), channel_id=1, source_target_pairs={{0,1},{1,0},{2,3},{3,2},{4,5},{5,4},{6,7},{7,6},{8,9},{9,8},{10,11... | collective-permute-start | bytes 3145736 | tf_op jit(solution)/shard_map/ppermute | solution.py:29
  83.0 21.0 %collective-permute-start.9 = (bf16[2,16,64,128]{3,2,1,0:T(8,128)(2,1)}, bf16[2,16,64,128]{3,2,1,0:T(8,128)(2,1)S(1)}, u32[]{:S(2)}, u32[]{:S(2)}) collective-permute-start(bf16[2,16,64,128]{3,2,1,0:T(8,128)(2,1)} %collective-permute-done.4.refs_4_), channel_id=1, source_target_pairs={{0,1},{1,0},{2,3},{3,2},{4,5},{5,4},{6,7},{7,6},{8,9},{9,8},{10,11... | collective-permute-start | bytes 1572872 | tf_op jit(solution)/shard_map/ppermute | solution.py:29
  85.5 18.6 %collective-permute-start.8 = (bf16[2,16,64,128]{3,2,1,0:T(8,128)(2,1)}, bf16[2,16,64,128]{3,2,1,0:T(8,128)(2,1)S(1)}, u32[]{:S(2)}, u32[]{:S(2)}) collective-permute-start(bf16[2,16,64,128]{3,2,1,0:T(8,128)(2,1)} %collective-permute-done.3.refs_3_), channel_id=1, source_target_pairs={{0,1},{1,0},{2,3},{3,2},{4,5},{5,4},{6,7},{7,6},{8,9},{9,8},{10,11... | collective-permute-start | bytes 1572872 | tf_op jit(solution)/shard_map/ppermute | solution.py:29
  92.6 11.4 %collective-permute-start = (bf16[32,2048]{1,0:T(8,128)(2,1)S(1)}, bf16[32,2048]{1,0:T(8,128)(2,1)S(1)}, u32[]{:S(2)}, u32[]{:S(2)}) collective-permute-start(bf16[32,2048]{1,0:T(8,128)(2,1)S(1)} %slice_bitcast_fusion), channel_id=1, source_target_pairs={{0,32},{1,33},{2,34},{3,35},{4,36},{5,37},{6,38},{7,39},{8,40},{9,... | collective-permute-start | bytes 393224 | tf_op jit(solution)/shard_map/ppermute | solution.py:268
  96.7 1.4 %copy-start = (bf16[1,384,2048]{2,1,0:T(8,128)(2,1)S(1)}, bf16[1,384,2048]{2,1,0:T(8,128)(2,1)}, u32[]{:S(2)}) copy-start(bf16[1,384,2048]{2,1,0:T(8,128)(2,1)} %param.5) | copy-start | bytes 4718596
  100.7 3.4 %copy-start.1 = (bf16[1,384,2048]{2,1,0:T(8,128)(2,1)S(1)}, bf16[1,384,2048]{2,1,0:T(8,128)(2,1)}, u32[]{:S(2)}) copy-start(bf16[1,384,2048]{2,1,0:T(8,128)(2,1)} %param.5) | copy-start | bytes 4718596
  100.7 3.4 %copy-start.3 = (f32[2,512]{1,0:T(2,128)S(1)}, f32[2,512]{1,0:T(2,128)}, u32[]{:S(2)}) copy-start(f32[2,512]{1,0:T(2,128)} %pool_gain.1) | copy-start | bytes 12292

commit v3 on v2

--- a/solution.py
+++ b/solution.py
@@ -9,7 +9,7 @@
 HALO = 32
 PAD = 16
 AXES = ("sp", "tp")
-PIECES = ((0, 0, 4), (-1, 0, 4), (1, 0, 4), (2, 0, 2), (2, 2, 4))
+PIECES = (0, 2, 1, -1)
 HEAD_MIB, PUT_MIB, MIX_MIB = 5, 10, 16
 VMEM = pl.BlockSpec(memory_space=pltpu.VMEM)
 SMEM = pl.BlockSpec(memory_space=pltpu.SMEM)
@@ -59,47 +59,36 @@
 
     for pieces, core, second in ((mine, c, s_mine), (theirs, 1 - c, s_theirs)):
         for k in new:
-            d, low, high = PIECES[k]
-            s = (second + d + 4) % 4
-
-            def put_in(i, carry, pieces=pieces, core=core, k=k, s=s, low=low):
-                f = i + low
+            s = (second + PIECES[k] + 4) % 4
+
+            def put_in(f, carry, pieces=pieces, core=core, k=k, s=s):
                 at = jnp.where(core == 0, s * 4 + f, f * 4 + s)
                 lanes = pl.ds(pl.multiple_of(at * 128, 128), 128)
                 for l in range(2):
                     whole_in[l, :, core, :, lanes] = pieces[k][
-                        i, :, l * 16 : (l + 1) * 16
+                        f, :, l * 16 : (l + 1) * 16
                     ]
                 return carry
 
-            lax.fori_loop(0, high - low, put_in, 0)
+            lax.fori_loop(0, 4, put_in, 0)
 
     for k in range(max(new) + 1):
         for j in range(max(new) + 1):
             if k not in new and j not in new:
                 continue
-            a = (s_mine + PIECES[k][0] + 4) % 4
-            b = (s_theirs + PIECES[j][0] + 4) % 4
-            (_, k_low, k_high), (_, j_low, j_high) = PIECES[k], PIECES[j]
-
-            def put_down(k=k, j=j, a=a, b=b, k_low=k_low, j_low=j_low):
-                at = jnp.where(c == 0, a * 4 + b, b * 4 + a)
-                rows = pl.ds(pl.multiple_of(at * 32, 32), 32)
-                for z in range(16):
-                    m = mine[k][b - k_low, z, 32:64]
-                    t = theirs[j][a - j_low, z, 32:64]
-                    lanes = slice(z * 128, (z + 1) * 128)
-                    whole_down[0, rows, lanes] = jnp.where(left, m, t)
-                    v = jnp.where(left, t, m)
-                    whole_down[1, rows, lanes] = jnp.concatenate(
-                        [v[:, 64:], v[:, :64]], axis=1
-                    )
-
-            if k > 2 or j > 2:
-                here = (b >= k_low) & (b < k_high) & (a >= j_low) & (a < j_high)
-                pl.when(here)(put_down)
-            else:
-                put_down()
+            a = (s_mine + PIECES[k] + 4) % 4
+            b = (s_theirs + PIECES[j] + 4) % 4
+            at = jnp.where(c == 0, a * 4 + b, b * 4 + a)
+            rows = pl.ds(pl.multiple_of(at * 32, 32), 32)
+            for z in range(16):
+                m = mine[k][b, z, 32:64]
+                t = theirs[j][a, z, 32:64]
+                lanes = slice(z * 128, (z + 1) * 128)
+                whole_down[0, rows, lanes] = jnp.where(left, m, t)
+                v = jnp.where(left, t, m)
+                whole_down[1, rows, lanes] = jnp.concatenate(
+                    [v[:, 64:], v[:, :64]], axis=1
+                )
 
 
 def wholes():
@@ -167,8 +156,8 @@
 def mixer_kernel(place, halo, tokens, normed, norm_gain, pool_gain, *refs):
     count = len(PIECES)
     mine, theirs = refs[:count], refs[count : 2 * count]
-    out, whole_in, whole_down, left, extended, pooled, middle = refs[-7:]
-    put(place, mine, theirs, (3, 4), whole_in, whole_down)
+    out, whole_in, whole_down, left, extended, pooled, middle, last, sems = refs[-9:]
+    put(place, mine, theirs, (2, 3), whole_in, whole_down)
     rows = left.shape[0]
     left[:HALO] = norm_rows(halo[...], norm_gain[0:1])
     extended[:PAD] = jnp.zeros((PAD, 512), jnp.float32)
@@ -220,13 +209,18 @@
         )
     mean = jnp.sum(squares, axis=1, keepdims=True) / 2048.0
     pool(1, lax.rsqrt(mean + EPS))
+    copies = []
     for j in range(4):
         lanes = slice(j * 512, (j + 1) * 512)
         down = jnp.dot(
             pooled[HALO:], whole_down[1, :, lanes], preferred_element_type=jnp.float32
         )
         total = middle[HALO:, lanes].astype(jnp.float32) + down
-        out[:, lanes] = total.astype(jnp.bfloat16)
+        last[:, lanes] = total.astype(jnp.bfloat16)
+        copies.append(pltpu.make_async_copy(last.at[:, lanes], out.at[:, lanes], sems.at[j]))
+        copies[-1].start()
+    for copy in copies:
+        copy.wait()
 
 
 def mixer(place, halo, tokens, normed, norm_gain, pool_gain, mine, theirs, whole):
@@ -240,12 +234,14 @@
             jax.ShapeDtypeStruct(normed.shape, normed.dtype),
         ),
         in_specs=[SMEM] + [VMEM] * (at + 1),
-        out_specs=(VMEM,) * 4,
+        out_specs=(pl.BlockSpec(memory_space=pl.ANY),) + (VMEM,) * 3,
         input_output_aliases={at: 1, at + 1: 2, 3: 3},
         scratch_shapes=[
             pltpu.VMEM((PAD + rows, 512), jnp.float32),
             pltpu.VMEM((rows, 512), jnp.bfloat16),
             pltpu.VMEM((rows, 2048), jnp.bfloat16),
+            pltpu.VMEM(tokens.shape, jnp.bfloat16),
+            pltpu.SemaphoreType.DMA((4,)),
         ],
         compiler_params=params(MIX_MIB),
         cost_estimate=cost(4 << 30),
@@ -276,14 +272,11 @@
         lambda y, x, z, c: (y, z, c) if c == 0 else (x, z, c),
     )
     line = line.reshape(4, 16, 64, 128)
-    up = send(line, second_hop(1))
-    down = send(line, second_hop(-1))
-    up_on = send(up[:2], second_hop(1))
-    down_on = send(down[2:], second_hop(-1))
-    mine = [line, up, down, up_on, down_on]
+    names = (2, -1, 1)
+    mine = [line] + [send(line, second_hop(d)) for d in names]
     theirs = [send(piece, other_core) for piece in mine]
     whole = placed(place, mine, theirs, (0,))
-    whole = placed(place, mine, theirs, (1, 2), whole)
+    whole = placed(place, mine, theirs, (1,), whole)
     return mixer(
         place, halo, tokens[0], normed, norm_gain, pool_gain, mine, theirs, whole
     )[None]

time: 114 us -> 113 us (level)
  the two profiles are of different devices: /device:TPU:1 before, /device:TPU:10 now
where the time goes in v3:
time: 113 us
  blocking collectives  47.9 us (42%)
  starting transfers between devices  30.5 us (27%)
  waiting for transfers between devices  16 us (14%)
  Pallas kernels  14.1 us (12%)
  local copies, waits for them, and re-layouts  2.63 us (2%)
  other arithmetic  1.58 us (1%)
    all_to_all x2, blocking collectives, shared(): lax.all_to_all(copies, AXES, 0, 0, axis_index_groups=list(groups.values()...  47.9 us
    ppermute x7, starting transfers between devices, send(): return lax.ppermute(block, AXES, route)  19 us
    ppermute x7, waiting for transfers between devices, send(): return lax.ppermute(block, AXES, route)  16 us
    ppermute x1, starting transfers between devices, mixed(): lax.ppermute(tokens[0, rows - HALO:], AXES, [(i, i + 32) for i in range(4...  11.4 us
    pallas_call x1, Pallas kernels, mixer(): pl.pallas_call(mixer_kernel, out_shape=(jax.ShapeDtypeStruct(tokens.shape...  9.69 us
    pallas_call x2, Pallas kernels, placed(): pl.pallas_call(kernel, out_shape=wholes(), in_specs=[SMEM] + [VMEM] * (2...  2.88 us
  transfers between devices with their start and end apart: 8, of which 2 were waited for; matrix products, arithmetic and copies ran while one was open for 1% of the time, Pallas kernels for 4%

profile of v3, /device:TPU:10, one launch (start us, length us, event | category | flops | bytes accessed | tf_op | source)
XLA Modules:
  0.0 112.9 jit_solution(3090282026809195528)
XLA Ops:
  0.0 0.0 copy-start.2
  0.0 0.7 select_bitcast_fusion.1
  0.7 0.8 maximum_maximum_fusion
  1.6 33.4 %all_to_all.10 = bf16[16,64,128]{2,1,0:T(8,128)(2,1)S(1)} all-to-all(bf16[16,64,128]{2,1,0:T(8,128)(2,1)S(1)} %broadcast_in_dim.6), channel_id=1, replica_groups={{0,2,4,6,8,10,12,14,16,18,20,22,24,26,28,30},{1,3,5,7,9,11,13,15,17,19,..., dimensions={0} | all-to-all | bytes 524288 | tf_op jit(solution)/shard_map/all_to_all | solution.py:37
  34.9 0.2 broadcast_in_dim.7
  35.2 14.5 %all_to_all.11.refs_0_ = bf16[4,16,64,128]{3,2,1,0:T(8,128)(2,1)S(1)} all-to-all(bf16[4,16,64,128]{3,2,1,0:T(8,128)(2,1)S(1)} %broadcast_in_dim.7), channel_id=1, replica_groups={{0,32,64,96},{1,129,257,385},{2,34,66,98},{3,131,259,387},{4,36,68,100}..., dimensions={0} | all-to-all | bytes 2097152 | tf_op jit(solution)/shard_map/all_to_all | solution.py:37
  49.7 5.0 %collective-permute-start.1 = (bf16[4,16,64,128]{3,2,1,0:T(8,128)(2,1)S(1)}, bf16[4,16,64,128]{3,2,1,0:T(8,128)(2,1)S(1)}, u32[]{:S(2)}, u32[]{:S(2)}) collective-permute-start(bf16[4,16,64,128]{3,2,1,0:T(8,128)(2,1)S(1)} %all_to_all.11.refs_0_), channel_id=1, source_target_pairs={{0,256},{1,65},{2,258},{3,67},{4,260},{5,69},{6,262},{7,71},{8,264... | collective-permute-start | bytes 3145736 | tf_op jit(solution)/shard_map/ppermute | solution.py:29
  54.7 1.9 %collective-permute-start.3 = (bf16[4,16,64,128]{3,2,1,0:T(8,128)(2,1)S(1)}, bf16[4,16,64,128]{3,2,1,0:T(8,128)(2,1)}, u32[]{:S(2)}, u32[]{:S(2)}) collective-permute-start(bf16[4,16,64,128]{3,2,1,0:T(8,128)(2,1)S(1)} %all_to_all.11.refs_0_), channel_id=1, source_target_pairs={{0,128},{1,33},{2,130},{3,35},{4,132},{5,37},{6,134},{7,39},{8,136... | collective-permute-start | bytes 3145736 | tf_op jit(solution)/shard_map/ppermute | solution.py:29
  56.6 3.9 %collective-permute-start.2 = (bf16[4,16,64,128]{3,2,1,0:T(8,128)(2,1)S(1)}, bf16[4,16,64,128]{3,2,1,0:T(8,128)(2,1)}, u32[]{:S(2)}, u32[]{:S(2)}) collective-permute-start(bf16[4,16,64,128]{3,2,1,0:T(8,128)(2,1)S(1)} %all_to_all.11.refs_0_), channel_id=1, source_target_pairs={{0,384},{1,97},{2,386},{3,99},{4,388},{5,101},{6,390},{7,103},{8,3... | collective-permute-start | bytes 3145736 | tf_op jit(solution)/shard_map/ppermute | solution.py:29
  60.6 1.9 %collective-permute-start.4 = (bf16[4,16,64,128]{3,2,1,0:T(8,128)(2,1)S(1)}, bf16[4,16,64,128]{3,2,1,0:T(8,128)(2,1)S(1)}, u32[]{:S(2)}, u32[]{:S(2)}) collective-permute-start(bf16[4,16,64,128]{3,2,1,0:T(8,128)(2,1)S(1)} %all_to_all.11.refs_0_), channel_id=1, source_target_pairs={{0,1},{1,0},{2,3},{3,2},{4,5},{5,4},{6,7},{7,6},{8,9},{9,8},{10,11... | collective-permute-start | bytes 3145736 | tf_op jit(solution)/shard_map/ppermute | solution.py:29
  62.5 5.5 %collective-permute-done.1.refs_1_ = bf16[4,16,64,128]{3,2,1,0:T(8,128)(2,1)S(1)} collective-permute-done((bf16[4,16,64,128]{3,2,1,0:T(8,128)(2,1)S(1)}, bf16[4,16,64,128]{3,2,1,0:T(8,128)(2,1)S(1)}, u32[]{:S(2)}, u32[]{:S(2)}) %collective-permute-start.1) | collective-permute-done | bytes 1048608 | tf_op jit(solution)/shard_map/ppermute | solution.py:29
  68.0 1.9 %collective-permute-start.5 = (bf16[4,16,64,128]{3,2,1,0:T(8,128)(2,1)S(1)}, bf16[4,16,64,128]{3,2,1,0:T(8,128)(2,1)}, u32[]{:S(2)}, u32[]{:S(2)}) collective-permute-start(bf16[4,16,64,128]{3,2,1,0:T(8,128)(2,1)S(1)} %collective-permute-done.1.refs_1_), channel_id=1, source_target_pairs={{0,1},{1,0},{2,3},{3,2},{4,5},{5,4},{6,7},{7,6},{8,9},{9,8},{10,11... | collective-permute-start | bytes 3145736 | tf_op jit(solution)/shard_map/ppermute | solution.py:29
  69.9 10.6 %collective-permute-done.3.refs_3_ = bf16[4,16,64,128]{3,2,1,0:T(8,128)(2,1)} collective-permute-done((bf16[4,16,64,128]{3,2,1,0:T(8,128)(2,1)S(1)}, bf16[4,16,64,128]{3,2,1,0:T(8,128)(2,1)}, u32[]{:S(2)}, u32[]{:S(2)}) %collective-permute-start.3) | collective-permute-done | bytes 1048608 | tf_op jit(solution)/shard_map/ppermute | solution.py:29
  80.4 1.9 %collective-permute-start.7 = (bf16[4,16,64,128]{3,2,1,0:T(8,128)(2,1)}, bf16[4,16,64,128]{3,2,1,0:T(8,128)(2,1)}, u32[]{:S(2)}, u32[]{:S(2)}) collective-permute-start(bf16[4,16,64,128]{3,2,1,0:T(8,128)(2,1)} %collective-permute-done.3.refs_3_), channel_id=1, source_target_pairs={{0,1},{1,0},{2,3},{3,2},{4,5},{5,4},{6,7},{7,6},{8,9},{9,8},{10,11... | collective-permute-start | bytes 3145736 | tf_op jit(solution)/shard_map/ppermute | solution.py:29
  82.3 0.0 collective-permute-done.2.refs_2_
  82.3 2.4 %collective-permute-start.6 = (bf16[4,16,64,128]{3,2,1,0:T(8,128)(2,1)}, bf16[4,16,64,128]{3,2,1,0:T(8,128)(2,1)}, u32[]{:S(2)}, u32[]{:S(2)}) collective-permute-start(bf16[4,16,64,128]{3,2,1,0:T(8,128)(2,1)} %collective-permute-done.2.refs_2_), channel_id=1, source_target_pairs={{0,1},{1,0},{2,3},{3,2},{4,5},{5,4},{6,7},{7,6},{8,9},{9,8},{10,11... | collective-permute-start | bytes 3145736 | tf_op jit(solution)/shard_map/ppermute | solution.py:29
  84.8 0.9 slice_bitcast_fusion
  85.7 11.4 %collective-permute-start = (bf16[32,2048]{1,0:T(8,128)(2,1)S(1)}, bf16[32,2048]{1,0:T(8,128)(2,1)S(1)}, u32[]{:S(2)}, u32[]{:S(2)}) collective-permute-start(bf16[32,2048]{1,0:T(8,128)(2,1)S(1)} %slice_bitcast_fusion), channel_id=1, source_target_pairs={{0,32},{1,33},{2,34},{3,35},{4,36},{5,37},{6,38},{7,39},{8,40},{9,... | collective-permute-start | bytes 393224 | tf_op jit(solution)/shard_map/ppermute | solution.py:264
  97.1 0.1 pad_add_fusion.place
  97.2 0.0 copy-done.2
  97.2 0.0 copy-start
  97.2 1.4 %copy-done = bf16[1,384,2048]{2,1,0:T(8,128)(2,1)S(1)} copy-done((bf16[1,384,2048]{2,1,0:T(8,128)(2,1)S(1)}, bf16[1,384,2048]{2,1,0:T(8,128)(2,1)}, u32[]{:S(2)}) %copy-start) | copy-done | bytes 1572888
  98.6 1.6 %head.1.normed = bf16[416,2048]{1,0:T(8,128)(2,1)S(1)} custom-call(bf16[384,2048]{1,0:T(8,128)(2,1)S(1)} %bitcast.13, f32[2,2048]{1,0:T(2,128)S(1)} %copy-done.2), custom_call_target="tpu_custom_call" | custom-call | flops 1073741824 | bytes 1048576 | tf_op jit(solution)/shard_map/head/pallas_call | solution.py:145
  100.2 0.0 collective-permute-done.4.refs_1_.refs_2_.refs_4_
  100.2 1.0 shard_map.55
  101.2 0.0 collective-permute-done.5.refs_3_.refs_5_
  101.2 0.0 copy-start.1
  101.2 0.0 copy-start.3
  101.2 1.9 %shard_map.56 = (bf16[2,16,2,16,2048]{4,3,2,1,0:T(8,128)(2,1)S(1)}, bf16[2,512,2048]{2,1,0:T(8,128)(2,1)S(1)}) custom-call(s32[2]{0:T(128)S(1)} %pad_add_fusion.place, bf16[4,16,64,128]{3,2,1,0:T(8,128)(2,1)S(1)} %all_to_all.11.refs_0_, bf16[4,16,64,128]{3,2,1,0:T(8,128)(2,1)S(1)} %collective-permute-done.1.refs_1_, ...), custom_call_target="tpu_custom_call", output_to_operand_aliasing={{0}: (5, {}), {1}: (6, {})} | custom-call | flops 536870912 | bytes 1048576 | tf_op jit(solution)/shard_map/pallas_call | solution.py:116
  103.1 0.0 collective-permute-done.halo
  103.1 0.0 collective-permute-done.7.refs_7_
  103.2 0.0 collective-permute-done.6.refs_6_
  103.2 0.0 copy-done.1
  103.2 0.0 copy-done.3
  103.2 9.7 %mixer.1 = (bf16[384,2048]{1,0:T(8,128)(2,1)}, bf16[2,16,2,16,2048]{4,3,2,1,0:T(8,128)(2,1)S(1)}, bf16[2,512,2048]{2,1,0:T(8,128)(2,1)S(1)}, bf16[416,2048]{1,0:T(8,128)(2,1)S(1)}) custom-call(s32[2]{0:T(128)S(1)} %pad_add_fusion.place, bf16[32,2048]{1,0:T(8,128)(2,1)S(1)} %collective-permute-done.halo, ...), custom_call_target="tpu_custom_call", output_to_operand_aliasing={{1}: (14, {}), {2}: (15, {}), {3}: (3, {})} | custom-call | flops 4294967296 | bytes 1048576 | tf_op jit(solution)/shard_map/mixer/pallas_call | solution.py:229
  (1 shorter events, 0.0 us)
Async XLA Ops:
  0.0 97.2 %copy-start.2 = (f32[2,2048]{1,0:T(2,128)S(1)}, f32[2,2048]{1,0:T(2,128)}, u32[]{:S(2)}) copy-start(f32[2,2048]{1,0:T(2,128)} %norm_gain.3) | copy-start | bytes 49156
  49.7 18.3 %collective-permute-start.1 = (bf16[4,16,64,128]{3,2,1,0:T(8,128)(2,1)S(1)}, bf16[4,16,64,128]{3,2,1,0:T(8,128)(2,1)S(1)}, u32[]{:S(2)}, u32[]{:S(2)}) collective-permute-start(bf16[4,16,64,128]{3,2,1,0:T(8,128)(2,1)S(1)} %all_to_all.11.refs_0_), channel_id=1, source_target_pairs={{0,256},{1,65},{2,258},{3,67},{4,260},{5,69},{6,262},{7,71},{8,264... | collective-permute-start | bytes 3145736 | tf_op jit(solution)/shard_map/ppermute | solution.py:29
  54.7 25.7 %collective-permute-start.3 = (bf16[4,16,64,128]{3,2,1,0:T(8,128)(2,1)S(1)}, bf16[4,16,64,128]{3,2,1,0:T(8,128)(2,1)}, u32[]{:S(2)}, u32[]{:S(2)}) collective-permute-start(bf16[4,16,64,128]{3,2,1,0:T(8,128)(2,1)S(1)} %all_to_all.11.refs_0_), channel_id=1, source_target_pairs={{0,128},{1,33},{2,130},{3,35},{4,132},{5,37},{6,134},{7,39},{8,136... | collective-permute-start | bytes 3145736 | tf_op jit(solution)/shard_map/ppermute | solution.py:29
  56.6 25.7 %collective-permute-start.2 = (bf16[4,16,64,128]{3,2,1,0:T(8,128)(2,1)S(1)}, bf16[4,16,64,128]{3,2,1,0:T(8,128)(2,1)}, u32[]{:S(2)}, u32[]{:S(2)}) collective-permute-start(bf16[4,16,64,128]{3,2,1,0:T(8,128)(2,1)S(1)} %all_to_all.11.refs_0_), channel_id=1, source_target_pairs={{0,384},{1,97},{2,386},{3,99},{4,388},{5,101},{6,390},{7,103},{8,3... | collective-permute-start | bytes 3145736 | tf_op jit(solution)/shard_map/ppermute | solution.py:29
  60.6 39.6 %collective-permute-start.4 = (bf16[4,16,64,128]{3,2,1,0:T(8,128)(2,1)S(1)}, bf16[4,16,64,128]{3,2,1,0:T(8,128)(2,1)S(1)}, u32[]{:S(2)}, u32[]{:S(2)}) collective-permute-start(bf16[4,16,64,128]{3,2,1,0:T(8,128)(2,1)S(1)} %all_to_all.11.refs_0_), channel_id=1, source_target_pairs={{0,1},{1,0},{2,3},{3,2},{4,5},{5,4},{6,7},{7,6},{8,9},{9,8},{10,11... | collective-permute-start | bytes 3145736 | tf_op jit(solution)/shard_map/ppermute | solution.py:29
  68.0 33.2 %collective-permute-start.5 = (bf16[4,16,64,128]{3,2,1,0:T(8,128)(2,1)S(1)}, bf16[4,16,64,128]{3,2,1,0:T(8,128)(2,1)}, u32[]{:S(2)}, u32[]{:S(2)}) collective-permute-start(bf16[4,16,64,128]{3,2,1,0:T(8,128)(2,1)S(1)} %collective-permute-done.1.refs_1_), channel_id=1, source_target_pairs={{0,1},{1,0},{2,3},{3,2},{4,5},{5,4},{6,7},{7,6},{8,9},{9,8},{10,11... | collective-permute-start | bytes 3145736 | tf_op jit(solution)/shard_map/ppermute | solution.py:29
  80.4 22.7 %collective-permute-start.7 = (bf16[4,16,64,128]{3,2,1,0:T(8,128)(2,1)}, bf16[4,16,64,128]{3,2,1,0:T(8,128)(2,1)}, u32[]{:S(2)}, u32[]{:S(2)}) collective-permute-start(bf16[4,16,64,128]{3,2,1,0:T(8,128)(2,1)} %collective-permute-done.3.refs_3_), channel_id=1, source_target_pairs={{0,1},{1,0},{2,3},{3,2},{4,5},{5,4},{6,7},{7,6},{8,9},{9,8},{10,11... | collective-permute-start | bytes 3145736 | tf_op jit(solution)/shard_map/ppermute | solution.py:29
  82.3 20.8 %collective-permute-start.6 = (bf16[4,16,64,128]{3,2,1,0:T(8,128)(2,1)}, bf16[4,16,64,128]{3,2,1,0:T(8,128)(2,1)}, u32[]{:S(2)}, u32[]{:S(2)}) collective-permute-start(bf16[4,16,64,128]{3,2,1,0:T(8,128)(2,1)} %collective-permute-done.2.refs_2_), channel_id=1, source_target_pairs={{0,1},{1,0},{2,3},{3,2},{4,5},{5,4},{6,7},{7,6},{8,9},{9,8},{10,11... | collective-permute-start | bytes 3145736 | tf_op jit(solution)/shard_map/ppermute | solution.py:29
  85.7 17.5 %collective-permute-start = (bf16[32,2048]{1,0:T(8,128)(2,1)S(1)}, bf16[32,2048]{1,0:T(8,128)(2,1)S(1)}, u32[]{:S(2)}, u32[]{:S(2)}) collective-permute-start(bf16[32,2048]{1,0:T(8,128)(2,1)S(1)} %slice_bitcast_fusion), channel_id=1, source_target_pairs={{0,32},{1,33},{2,34},{3,35},{4,36},{5,37},{6,38},{7,39},{8,40},{9,... | collective-permute-start | bytes 393224 | tf_op jit(solution)/shard_map/ppermute | solution.py:264
  97.2 1.4 %copy-start = (bf16[1,384,2048]{2,1,0:T(8,128)(2,1)S(1)}, bf16[1,384,2048]{2,1,0:T(8,128)(2,1)}, u32[]{:S(2)}) copy-start(bf16[1,384,2048]{2,1,0:T(8,128)(2,1)} %param.5) | copy-start | bytes 4718596
  101.2 2.0 %copy-start.1 = (bf16[1,384,2048]{2,1,0:T(8,128)(2,1)S(1)}, bf16[1,384,2048]{2,1,0:T(8,128)(2,1)}, u32[]{:S(2)}) copy-start(bf16[1,384,2048]{2,1,0:T(8,128)(2,1)} %param.5) | copy-start | bytes 4718596
  101.2 2.0 %copy-start.3 = (f32[2,512]{1,0:T(2,128)S(1)}, f32[2,512]{1,0:T(2,128)}, u32[]{:S(2)}) copy-start(f32[2,512]{1,0:T(2,128)} %pool_gain.1) | copy-start | bytes 12292

commit v4 on v3

v4 whole, which is shorter than its diff:
```python
import jax
import jax.numpy as jnp
from jax import lax
from jax.experimental import pallas as pl
from jax.experimental.pallas import tpu as pltpu
from jax.sharding import PartitionSpec as P

EPS = 1e-06
HALO = 32
PAD = 16
AXES = ("sp", "tp")
PIECES = (0, 2, 1, -1)
VMEM = pl.BlockSpec(memory_space=pltpu.VMEM)
BF16, F32 = jnp.bfloat16, jnp.float32


def number(y, x, z, c):
    return (((y % 4) * 4 + x % 4) * 16 + z % 16) * 2 + c


def places():
    for i in range(512):
        yield i, (i // 128, i // 32 % 4, i // 2 % 16, i % 2)


def send(block, target):
    route = [(i, number(*target(*place))) for i, place in places()]
    return lax.ppermute(block, AXES, route)


def shared(copies, key):
    groups = {}
    for i, place in places():
        groups.setdefault(key(*place), []).append(i)
    return lax.all_to_all(
        copies, AXES, 0, 0, axis_index_groups=list(groups.values()), tiled=True
    )


def second_hop(d):
    return lambda y, x, z, c: (y + d, x, z, c) if c == 0 else (y, x + d, z, c)


def other_core(y, x, z, c):
    return y, x, z, 1 - c


def seconds():
    sp, c = lax.axis_index("sp"), lax.axis_index("tp") % 2
    y, x = sp // 4, sp % 4
    return c, jnp.where(c == 0, y, x), jnp.where(c == 0, x, y)


def lanes_of(core, s, f):
    at = jnp.where(core == 0, s * 4 + f, f * 4 + s)
    return pl.ds(pl.multiple_of(at * 128, 128), 128)


def along(second, k):
    return (second + PIECES[k] + 4) % 4


def part(left, piece, core, s):
    lhs = jnp.concatenate([left[:, lanes_of(core, s, f)] for f in range(4)], axis=1)
    rhs = jnp.concatenate(
        [piece[f, :, 0:16].reshape(256, 128) for f in range(4)], axis=1
    )
    return lax.dot_general(
        lhs, rhs, (((1,), (1,)), ((), ())), preferred_element_type=F32
    )


def put_in(piece, core, s, whole_in):
    def step(f, carry):
        whole_in[core, :, :, lanes_of(core, s, f)] = piece[f, :, 16:32]
        return carry

    lax.fori_loop(0, 4, step, 0)


def put_down(mine, theirs, pairs, whole_down):
    c, s_mine, s_theirs = seconds()
    left = (lax.broadcasted_iota(jnp.int32, (32, 128), 1) < 64) ^ (c == 1)
    for k, j in pairs:
        a, b = along(s_mine, k), along(s_theirs, j)
        at = jnp.where(c == 0, a * 4 + b, b * 4 + a)
        rows = pl.ds(pl.multiple_of(at * 16, 16), 16)
        for z in range(16):
            m = mine[k][b, z, 32:64]
            t = theirs[j][a, z, 32:64]
            lanes = slice(z * 128, (z + 1) * 128)
            first = jnp.where(left, m, t)
            last = jnp.where(left, t, m)
            last = jnp.concatenate([last[:, 64:], last[:, :64]], axis=1)
            for l, tile in enumerate((first, last)):
                whole_down[l, 0, rows, lanes] = tile[:16]
                whole_down[l, 1, rows, lanes] = tile[16:]


def params(mib):
    return pltpu.CompilerParams(vmem_limit_bytes=mib << 20)


def cost(flops):
    return pl.CostEstimate(flops=flops, bytes_accessed=1 << 20, transcendentals=0)


def packed(in_weight, down_weight):
    core = lax.axis_index("tp") % 2
    turned = jnp.swapaxes(in_weight, 1, 2).reshape(32, 128)
    first = jnp.where(core == 0, down_weight[0], down_weight[1])
    last = jnp.where(core == 0, down_weight[1], down_weight[0])
    folded = jnp.concatenate([first, last], axis=1)
    block = jnp.concatenate([turned, folded], axis=0)
    return jnp.broadcast_to(block[None], (16, 64, 128))


def head_kernel(halo, tokens, norm_gain, pool_gain, normed, gain_out):
    gain = norm_gain[0:1]

    def norm_rows(block):
        residual = block.astype(F32)
        mean = jnp.mean(residual * residual, axis=1, keepdims=True)
        return (residual * lax.rsqrt(mean + EPS) * gain).astype(BF16)

    def norm(i, carry):
        rows = pl.multiple_of(i * 32, 32)
        normed[pl.ds(HALO + rows, 32)] = norm_rows(tokens[pl.ds(rows, 32)])
        return carry

    lax.fori_loop(0, tokens.shape[0] // 32, norm, 0)
    normed[:HALO] = norm_rows(halo[...])
    old = lax.broadcasted_iota(jnp.int32, (512, 512), 0)
    new = lax.broadcasted_iota(jnp.int32, (512, 512), 1)
    source = new % 256 // 16 * 32 + new // 256 * 16 + new % 16
    gain_out[...] = jnp.dot(
        pool_gain[...],
        (old == source).astype(F32),
        precision=lax.Precision.HIGHEST,
        preferred_element_type=F32,
    )


def head(halo, tokens, norm_gain, pool_gain):
    return pl.pallas_call(
        head_kernel,
        out_shape=(
            jax.ShapeDtypeStruct((HALO + tokens.shape[0], 2048), BF16),
            jax.ShapeDtypeStruct(pool_gain.shape, F32),
        ),
        in_specs=[VMEM] * 4,
        out_specs=(VMEM, VMEM),
        compiler_params=params(5),
        cost_estimate=cost(1 << 30),
        name="head",
    )(halo, tokens, norm_gain, pool_gain)


def wholes():
    return (
        jax.ShapeDtypeStruct((2, 16, 16, 2048), BF16),
        jax.ShapeDtypeStruct((2, 2, 256, 2048), BF16),
    )


def placed(body, mib, normed, pieces, so_far):
    rows = normed.shape[0]
    count = 1 + len(pieces)

    def kernel(*refs):
        body(refs[0], refs[1:count], refs[count:-3], *refs[-3:])

    return pl.pallas_call(
        kernel,
        out_shape=(jax.ShapeDtypeStruct((2, rows, 256), F32), *wholes()),
        in_specs=[VMEM] * (count + len(so_far)),
        out_specs=(VMEM,) * 3,
        input_output_aliases={count + i: i for i in range(len(so_far))},
        compiler_params=params(mib),
        cost_estimate=cost(1 << 29),
    )(normed, *pieces, *so_far)


def place_a(normed, pieces, so_far, total, whole_in, whole_down):
    mine, theirs = pieces
    c, s_mine, s_theirs = seconds()
    for slot, piece, core, second in ((0, mine, c, s_mine), (1, theirs, 1 - c, s_theirs)):
        s = along(second, 0)
        total[slot] = part(normed, piece, core, s)
        put_in(piece, core, s, whole_in)
    put_down((mine,), (theirs,), ((0, 0),), whole_down)


def place_b(normed, pieces, so_far, total, whole_in, whole_down):
    mine, theirs = pieces[:2], pieces[2:]
    c, s_mine, s_theirs = seconds()
    for slot, piece, core, second in (
        (0, mine[1], c, s_mine),
        (1, theirs[1], 1 - c, s_theirs),
    ):
        s = along(second, 1)
        total[slot] += part(normed, piece, core, s)
        put_in(piece, core, s, whole_in)
    put_down(mine, theirs, ((0, 1), (1, 0), (1, 1)), whole_down)


def place_c(normed, pieces, so_far, total, whole_in, whole_down):
    mine, theirs = pieces[:4], pieces[4:]
    c, s_mine, s_theirs = seconds()
    for slot, piece, core, s in (
        (0, mine[2], c, along(s_mine, 2)),
        (0, mine[3], c, along(s_mine, 3)),
        (1, theirs[2], 1 - c, along(s_theirs, 2)),
    ):
        total[slot] += part(normed, piece, core, s)
        put_in(piece, core, s, whole_in)
    pairs = [(k, j) for k in range(4) for j in range(3) if k > 1 or j > 1]
    put_down(mine, theirs, pairs, whole_down)


def mixer_kernel(tokens, halo, norm_gain, pool_gain, left, *refs):
    mine, theirs = refs[:4], (None, None, None, refs[4])
    out, total, whole_in, whole_down = refs[-10:-6]
    extended, pooled, middle, scaled, last, sems = refs[-6:]
    c, _, s_theirs = seconds()
    s = along(s_theirs, 3)
    put_in(theirs[3], 1 - c, s, whole_in)
    put_down(mine, theirs, [(k, 3) for k in range(4)], whole_down)
    rows = left.shape[0]
    extended[:PAD] = jnp.zeros((PAD, 512), F32)
    row = lax.broadcasted_iota(jnp.int32, (rows, 128), 0)
    lane = lax.broadcasted_iota(jnp.int32, (rows, 128), 1)
    position = lax.axis_index("sp") * 384 - HALO + row + 1
    position = jnp.maximum(position, 1).astype(F32)
    width = jnp.where(
        lane < 64, jnp.where(lane < 32, 2.0, 4.0), jnp.where(lane < 96, 8.0, 16.0)
    )
    count = jnp.minimum(position, width)

    def rounded(block):
        return block.astype(BF16).astype(F32)

    def pool(l):
        for j in range(4):
            lanes = slice(j * 128, (j + 1) * 128)
            own = extended[:, lanes]
            two = own + pltpu.roll(own, 1, 0)
            four = two + pltpu.roll(two, 2, 0)
            eight = four + pltpu.roll(four, 4, 0)
            sixteen = eight + pltpu.roll(eight, 8, 0)
            sums = jnp.where(
                lane < 64,
                jnp.where(lane < 32, two[PAD:], four[PAD:]),
                jnp.where(lane < 96, eight[PAD:], sixteen[PAD:]),
            )
            trailing = sums / count - own[PAD:]
            pooled[:, lanes] = (trailing * pool_gain[l : l + 1, lanes]).astype(BF16)

    extended[PAD:, pl.ds(pl.multiple_of(c * 256, 256), 256)] = rounded(total[0])
    extended[PAD:, pl.ds(pl.multiple_of((1 - c) * 256, 256), 256)] = rounded(
        total[1] + part(left, theirs[3], 1 - c, s)
    )
    pool(0)
    squares = jnp.zeros((rows, 128), F32)
    for j in range(4):
        lanes = slice(j * 512, (j + 1) * 512)
        down = jnp.dot(
            pooled[...],
            whole_down[0, :, :, lanes].reshape(512, 512),
            preferred_element_type=F32,
        )
        before = jnp.concatenate([halo[:, lanes], tokens[:, lanes]], axis=0)
        middle[:, lanes] = (before.astype(F32) + down).astype(BF16)
        block = middle[:, lanes].astype(F32)
        scaled[:, lanes] = (block * norm_gain[1:2, lanes]).astype(BF16)
        block = block * block
        squares += (block[:, :128] + block[:, 128:256]) + (
            block[:, 256:384] + block[:, 384:]
        )
    mean = jnp.sum(squares, axis=1, keepdims=True) / 2048.0
    pool_in = lax.dot_general(
        scaled[...],
        whole_in[...].reshape(512, 2048),
        (((1,), (1,)), ((), ())),
        preferred_element_type=F32,
    )
    extended[PAD:] = rounded(pool_in * lax.rsqrt(mean + EPS))
    pool(1)
    copies = []
    for j in range(4):
        lanes = slice(j * 512, (j + 1) * 512)
        down = jnp.dot(
            pooled[HALO:],
            whole_down[1, :, :, lanes].reshape(512, 512),
            preferred_element_type=F32,
        )
        last[:, lanes] = (middle[HALO:, lanes].astype(F32) + down).astype(BF16)
        copies.append(
            pltpu.make_async_copy(last.at[:, lanes], out.at[:, lanes], sems.at[j])
        )
        copies[-1].start()
    for copy in copies:
        copy.wait()


def mixer(tokens, halo, norm_gain, pool_gain, normed, pieces, so_far):
    rows = normed.shape[0]
    at = 5 + len(pieces)
    return pl.pallas_call(
        mixer_kernel,
        out_shape=(
            jax.ShapeDtypeStruct(tokens.shape, tokens.dtype),
            jax.ShapeDtypeStruct((2, rows, 256), F32),
            *wholes(),
        ),
        in_specs=[VMEM] * (at + 3),
        out_specs=(pl.BlockSpec(memory_space=pl.ANY),) + (VMEM,) * 3,
        input_output_aliases={at: 1, at + 1: 2, at + 2: 3},
        scratch_shapes=[
            pltpu.VMEM((PAD + rows, 512), F32),
            pltpu.VMEM((rows, 512), BF16),
            pltpu.VMEM((rows, 2048), BF16),
            pltpu.VMEM((rows, 2048), BF16),
            pltpu.VMEM(tokens.shape, BF16),
            pltpu.SemaphoreType.DMA((4,)),
        ],
        compiler_params=params(16),
        cost_estimate=cost(4 << 30),
        name="mixer",
    )(tokens, halo, norm_gain, pool_gain, normed, *pieces, *so_far)[0]


def mixed(tokens, norm_gain, in_weight, down_weight, pool_gain):
    rows = tokens.shape[1]
    halo = lax.ppermute(
        tokens[0, rows - HALO :], AXES, [(i, i + 32) for i in range(480)]
    )
    normed, pool_gain = head(halo, tokens[0], norm_gain, pool_gain)
    column = shared(packed(in_weight, down_weight), lambda y, x, z, c: (y, x, c))
    line = shared(
        jnp.broadcast_to(column[None], (4, 16, 64, 128)),
        lambda y, x, z, c: (y, z, c) if c == 0 else (x, z, c),
    )
    names = (2, -1, 1)
    mine = [line] + [send(line, second_hop(d)) for d in names]
    theirs = [send(piece, other_core) for piece in mine]
    so_far = placed(place_a, 10, normed, mine[:1] + theirs[:1], ())
    so_far = placed(place_b, 10, normed, mine[:2] + theirs[:2], so_far)
    so_far = placed(place_c, 12, normed, mine + theirs[:3], so_far)
    return mixer(
        tokens[0], halo, norm_gain, pool_gain, normed, mine + theirs[3:], so_far
    )[None]


def solution(mesh):
    in_specs = (P("tp", "sp", None), P(), P(None, "sp", "tp"), P(None, "sp", "tp"), P())
    out_specs = P("tp", "sp", None)
    return jax.shard_map(
        mixed, mesh=mesh, in_specs=in_specs, out_specs=out_specs, check_vma=False
    )
```

time: 113 us -> 111 us (0.982)
  the two profiles are of different devices: /device:TPU:10 before, /device:TPU:12 now
where the time goes in v4:
time: 111 us; the launch traced here: 110 us
  blocking collectives  46.4 us (42%)
  starting transfers between devices  30.2 us (27%)
  waiting for transfers between devices  19.8 us (18%)
  Pallas kernels  12.1 us (11%)
  other arithmetic  1.49 us (1%)
    all_to_all x2, blocking collectives, shared(): lax.all_to_all(copies, AXES, 0, 0, axis_index_groups=list(groups.values()...  46.4 us
    ppermute x7, starting transfers between devices, send(): return lax.ppermute(block, AXES, route)  28.2 us
    ppermute x7, waiting for transfers between devices, send(): return lax.ppermute(block, AXES, route)  13.9 us
    ppermute x1, waiting for transfers between devices, mixed(): lax.ppermute(tokens[0, rows - HALO:], AXES, [(i, i + 32) for i in range(4...  5.87 us
    pallas_call x1, Pallas kernels, mixer(): pl.pallas_call(mixer_kernel, out_shape=(jax.ShapeDtypeStruct(tokens.shape...  5.58 us
    pallas_call x3, Pallas kernels, placed(): pl.pallas_call(kernel, out_shape=(jax.ShapeDtypeStruct((2, rows, 256), F3...  4.24 us
    pallas_call x1, Pallas kernels, head(): pl.pallas_call(head_kernel, out_shape=(jax.ShapeDtypeStruct((HALO + token...  2.28 us
  transfers between devices with their start and end apart: 8, of which 3 were waited for; matrix products, arithmetic and copies ran while one was open for 0% of the time, Pallas kernels for 6%

profile of v4, /device:TPU:12, one launch (start us, length us, event | category | flops | bytes accessed | tf_op | source)
XLA Modules:
  0.0 110.4 jit_solution(18189190540860683789)
XLA Ops:
  0.0 0.7 select_bitcast_fusion.1
  0.7 0.8 maximum_maximum_fusion
  1.5 0.0 copy-start
  1.5 0.0 copy-start.1
  1.6 0.0 copy-start.2
  1.6 33.5 %all_to_all.10 = bf16[16,64,128]{2,1,0:T(8,128)(2,1)S(1)} all-to-all(bf16[16,64,128]{2,1,0:T(8,128)(2,1)S(1)} %broadcast_in_dim.6), channel_id=1, replica_groups={{0,2,4,6,8,10,12,14,16,18,20,22,24,26,28,30},{1,3,5,7,9,11,13,15,17,19,..., dimensions={0} | all-to-all | bytes 524288 | tf_op jit(solution)/shard_map/all_to_all | solution.py:35
  35.1 0.2 broadcast_in_dim.7
  35.3 12.9 %all_to_all.11.refs_1_.refs_0_ = bf16[4,16,64,128]{3,2,1,0:T(8,128)(2,1)S(1)} all-to-all(bf16[4,16,64,128]{3,2,1,0:T(8,128)(2,1)S(1)} %broadcast_in_dim.7), channel_id=1, replica_groups={{0,32,64,96},{1,129,257,385},{2,34,66,98},{3,131,259,387},{4,36,68,100}..., dimensions={0} | all-to-all | bytes 2097152 | tf_op jit(solution)/shard_map/all_to_all | solution.py:35
  48.2 5.0 %collective-permute-start.1 = (bf16[4,16,64,128]{3,2,1,0:T(8,128)(2,1)S(1)}, bf16[4,16,64,128]{3,2,1,0:T(8,128)(2,1)S(1)}, u32[]{:S(2)}, u32[]{:S(2)}) collective-permute-start(bf16[4,16,64,128]{3,2,1,0:T(8,128)(2,1)S(1)} %all_to_all.11.refs_1_.refs_0_), channel_id=1, source_target_pairs={{0,256},{1,65},{2,258},{3,67},{4,260},{5,69},{6,262},{7,71},{8,264... | collective-permute-start | bytes 3145736 | tf_op jit(solution)/shard_map/ppermute | solution.py:28
  53.2 13.2 %collective-permute-start.2 = (bf16[4,16,64,128]{3,2,1,0:T(8,128)(2,1)S(1)}, bf16[4,16,64,128]{3,2,1,0:T(8,128)(2,1)S(1)}, u32[]{:S(2)}, u32[]{:S(2)}) collective-permute-start(bf16[4,16,64,128]{3,2,1,0:T(8,128)(2,1)S(1)} %all_to_all.11.refs_1_.refs_0_), channel_id=1, source_target_pairs={{0,384},{1,97},{2,386},{3,99},{4,388},{5,101},{6,390},{7,103},{8,3... | collective-permute-start | bytes 3145736 | tf_op jit(solution)/shard_map/ppermute | solution.py:28
  66.4 1.9 %collective-permute-start.3 = (bf16[4,16,64,128]{3,2,1,0:T(8,128)(2,1)S(1)}, bf16[4,16,64,128]{3,2,1,0:T(8,128)(2,1)S(1)}, u32[]{:S(2)}, u32[]{:S(2)}) collective-permute-start(bf16[4,16,64,128]{3,2,1,0:T(8,128)(2,1)S(1)} %all_to_all.11.refs_1_.refs_0_), channel_id=1, source_target_pairs={{0,128},{1,33},{2,130},{3,35},{4,132},{5,37},{6,134},{7,39},{8,136... | collective-permute-start | bytes 3145736 | tf_op jit(solution)/shard_map/ppermute | solution.py:28
  68.3 1.9 %collective-permute-start.5 = (bf16[4,16,64,128]{3,2,1,0:T(8,128)(2,1)S(1)}, bf16[4,16,64,128]{3,2,1,0:T(8,128)(2,1)S(1)}, u32[]{:S(2)}, u32[]{:S(2)}) collective-permute-start(bf16[4,16,64,128]{3,2,1,0:T(8,128)(2,1)S(1)} %all_to_all.11.refs_1_.refs_0_), channel_id=1, source_target_pairs={{0,1},{1,0},{2,3},{3,2},{4,5},{5,4},{6,7},{7,6},{8,9},{9,8},{10,11... | collective-permute-start | bytes 3145736 | tf_op jit(solution)/shard_map/ppermute | solution.py:28
  70.2 0.0 collective-permute-done.1.refs_2_.refs_1_
  70.3 2.4 %collective-permute-start.6 = (bf16[4,16,64,128]{3,2,1,0:T(8,128)(2,1)S(1)}, bf16[4,16,64,128]{3,2,1,0:T(8,128)(2,1)S(1)}, u32[]{:S(2)}, u32[]{:S(2)}) collective-permute-start(bf16[4,16,64,128]{3,2,1,0:T(8,128)(2,1)S(1)} %collective-permute-done.1.refs_2_.refs_1_), channel_id=1, source_target_pairs={{0,1},{1,0},{2,3},{3,2},{4,5},{5,4},{6,7},{7,6},{8,9},{9,8},{10,11... | collective-permute-start | bytes 3145736 | tf_op jit(solution)/shard_map/ppermute | solution.py:28
  72.7 6.0 %collective-permute-done.2.refs_3_.refs_2_ = bf16[4,16,64,128]{3,2,1,0:T(8,128)(2,1)S(1)} collective-permute-done((bf16[4,16,64,128]{3,2,1,0:T(8,128)(2,1)S(1)}, bf16[4,16,64,128]{3,2,1,0:T(8,128)(2,1)S(1)}, u32[]{:S(2)}, u32[]{:S(2)}) %collective-permute-start.2) | collective-permute-done | bytes 1048608 | tf_op jit(solution)/shard_map/ppermute | solution.py:28
  78.7 1.9 %collective-permute-start.7 = (bf16[4,16,64,128]{3,2,1,0:T(8,128)(2,1)S(1)}, bf16[4,16,64,128]{3,2,1,0:T(8,128)(2,1)S(1)}, u32[]{:S(2)}, u32[]{:S(2)}) collective-permute-start(bf16[4,16,64,128]{3,2,1,0:T(8,128)(2,1)S(1)} %collective-permute-done.2.refs_3_.refs_2_), channel_id=1, source_target_pairs={{0,1},{1,0},{2,3},{3,2},{4,5},{5,4},{6,7},{7,6},{8,9},{9,8},{10,11... | collective-permute-start | bytes 3145736 | tf_op jit(solution)/shard_map/ppermute | solution.py:28
  80.6 7.9 %collective-permute-done.3.refs_4_.refs_3_ = bf16[4,16,64,128]{3,2,1,0:T(8,128)(2,1)S(1)} collective-permute-done((bf16[4,16,64,128]{3,2,1,0:T(8,128)(2,1)S(1)}, bf16[4,16,64,128]{3,2,1,0:T(8,128)(2,1)S(1)}, u32[]{:S(2)}, u32[]{:S(2)}) %collective-permute-start.3) | collective-permute-done | bytes 1048608 | tf_op jit(solution)/shard_map/ppermute | solution.py:28
  88.5 1.9 %collective-permute-start.4 = (bf16[4,16,64,128]{3,2,1,0:T(8,128)(2,1)S(1)}, bf16[4,16,64,128]{3,2,1,0:T(8,128)(2,1)S(1)}, u32[]{:S(2)}, u32[]{:S(2)}) collective-permute-start(bf16[4,16,64,128]{3,2,1,0:T(8,128)(2,1)S(1)} %collective-permute-done.3.refs_4_.refs_3_), channel_id=1, source_target_pairs={{0,1},{1,0},{2,3},{3,2},{4,5},{5,4},{6,7},{7,6},{8,9},{9,8},{10,11... | collective-permute-start | bytes 3145736 | tf_op jit(solution)/shard_map/ppermute | solution.py:28
  90.4 0.0 copy-done
  90.4 1.9 %collective-permute-start = (bf16[32,2048]{1,0:T(8,128)(2,1)S(1)}, bf16[32,2048]{1,0:T(8,128)(2,1)S(1)}, u32[]{:S(2)}, u32[]{:S(2)}) collective-permute-start(bf16[32,2048]{1,0:T(8,128)(2,1)S(1)} %slice_bitcast_fusion), channel_id=1, source_target_pairs={{0,32},{1,33},{2,34},{3,35},{4,36},{5,37},{6,38},{7,39},{8,40},{9,... | collective-permute-start | bytes 393224 | tf_op jit(solution)/shard_map/ppermute | solution.py:335
  92.4 5.9 %collective-permute-done.halo = bf16[32,2048]{1,0:T(8,128)(2,1)S(1)} collective-permute-done((bf16[32,2048]{1,0:T(8,128)(2,1)S(1)}, bf16[32,2048]{1,0:T(8,128)(2,1)S(1)}, u32[]{:S(2)}, u32[]{:S(2)}) %collective-permute-start) | collective-permute-done | bytes 131104 | tf_op jit(solution)/shard_map/ppermute | solution.py:335
  98.2 0.0 copy-done.1
  98.2 0.0 copy-done.2
  98.2 2.3 %head.1 = (bf16[416,2048]{1,0:T(8,128)(2,1)S(1)}, f32[2,512]{1,0:T(2,128)S(1)}) custom-call(bf16[32,2048]{1,0:T(8,128)(2,1)S(1)} %collective-permute-done.halo, bf16[384,2048]{1,0:T(8,128)(2,1)S(1)} %bitcast.11, f32[2,2048]{1,0:T(2,128)S(1)} %copy-done.1, f32[2,512]{1,0:T(2,128)S(1)} %copy-done.2), custom_call_target="tpu_custom_call" | custom-call | flops 1073741824 | bytes 1048576 | tf_op jit(solution)/shard_map/head/pallas_call | solution.py:145
  100.5 0.0 collective-permute-done.5.refs_2_.refs_3_.refs_5_
  100.5 1.1 shard_map.55
  101.6 0.0 collective-permute-done.6.refs_4_.refs_6_
  101.6 1.2 %shard_map.56 = (f32[2,416,256]{2,1,0:T(8,128)S(1)}, bf16[2,16,16,2048]{3,2,1,0:T(8,128)(2,1)S(1)}, bf16[2,2,256,2048]{3,2,1,0:T(8,128)(2,1)S(1)}) custom-call(bf16[416,2048]{1,0:T(8,128)(2,1)S(1)} %get-tuple-element.18.refs_0_.left, ...), custom_call_target="tpu_custom_call", output_to_operand_aliasing={{0}: (5, {}), {1}: (6, {}), {2}: (7, {})} | custom-call | flops 536870912 | bytes 1048576 | tf_op jit(solution)/shard_map/pallas_call | solution.py:173
  102.8 0.0 collective-permute-done.7.refs_7_
  102.8 2.0 %shard_map.57 = (f32[2,416,256]{2,1,0:T(8,128)S(1)}, bf16[2,16,16,2048]{3,2,1,0:T(8,128)(2,1)S(1)}, bf16[2,2,256,2048]{3,2,1,0:T(8,128)(2,1)S(1)}) custom-call(bf16[416,2048]{1,0:T(8,128)(2,1)S(1)} %get-tuple-element.18.refs_0_.left, ...), custom_call_target="tpu_custom_call", output_to_operand_aliasing={{0}: (8, {}), {1}: (9, {}), {2}: (10, {})} | custom-call | flops 536870912 | bytes 1048576 | tf_op jit(solution)/shard_map/pallas_call | solution.py:173
  104.8 0.0 collective-permute-done.4.refs_4_
  104.8 5.6 %mixer.1 = (bf16[384,2048]{1,0:T(8,128)(2,1)}, f32[2,416,256]{2,1,0:T(8,128)S(1)}, bf16[2,16,16,2048]{3,2,1,0:T(8,128)(2,1)S(1)}, bf16[2,2,256,2048]{3,2,1,0:T(8,128)(2,1)S(1)}) custom-call(bf16[384,2048]{1,0:T(8,128)(2,1)S(1)} %bitcast.12, ...), custom_call_target="tpu_custom_call", output_to_operand_aliasing={{1}: (10, {}), {2}: (11, {}), {3}: (12, {})} | custom-call | flops 4294967296 | bytes 1048576 | tf_op jit(solution)/shard_map/mixer/pallas_call | solution.py:309
  (2 shorter events, 0.1 us)
Async XLA Ops:
  1.5 88.9 %copy-start = (bf16[1,384,2048]{2,1,0:T(8,128)(2,1)S(1)}, bf16[1,384,2048]{2,1,0:T(8,128)(2,1)}, u32[]{:S(2)}) copy-start(bf16[1,384,2048]{2,1,0:T(8,128)(2,1)} %param.5) | copy-start | bytes 4718596
  1.5 96.7 %copy-start.1 = (f32[2,2048]{1,0:T(2,128)S(1)}, f32[2,2048]{1,0:T(2,128)}, u32[]{:S(2)}) copy-start(f32[2,2048]{1,0:T(2,128)} %norm_gain.3) | copy-start | bytes 49156
  1.6 96.7 %copy-start.2 = (f32[2,512]{1,0:T(2,128)S(1)}, f32[2,512]{1,0:T(2,128)}, u32[]{:S(2)}) copy-start(f32[2,512]{1,0:T(2,128)} %pool_gain.1) | copy-start | bytes 12292
  48.2 22.1 %collective-permute-start.1 = (bf16[4,16,64,128]{3,2,1,0:T(8,128)(2,1)S(1)}, bf16[4,16,64,128]{3,2,1,0:T(8,128)(2,1)S(1)}, u32[]{:S(2)}, u32[]{:S(2)}) collective-permute-start(bf16[4,16,64,128]{3,2,1,0:T(8,128)(2,1)S(1)} %all_to_all.11.refs_1_.refs_0_), channel_id=1, source_target_pairs={{0,256},{1,65},{2,258},{3,67},{4,260},{5,69},{6,262},{7,71},{8,264... | collective-permute-start | bytes 3145736 | tf_op jit(solution)/shard_map/ppermute | solution.py:28
  53.2 25.5 %collective-permute-start.2 = (bf16[4,16,64,128]{3,2,1,0:T(8,128)(2,1)S(1)}, bf16[4,16,64,128]{3,2,1,0:T(8,128)(2,1)S(1)}, u32[]{:S(2)}, u32[]{:S(2)}) collective-permute-start(bf16[4,16,64,128]{3,2,1,0:T(8,128)(2,1)S(1)} %all_to_all.11.refs_1_.refs_0_), channel_id=1, source_target_pairs={{0,384},{1,97},{2,386},{3,99},{4,388},{5,101},{6,390},{7,103},{8,3... | collective-permute-start | bytes 3145736 | tf_op jit(solution)/shard_map/ppermute | solution.py:28
  66.4 22.1 %collective-permute-start.3 = (bf16[4,16,64,128]{3,2,1,0:T(8,128)(2,1)S(1)}, bf16[4,16,64,128]{3,2,1,0:T(8,128)(2,1)S(1)}, u32[]{:S(2)}, u32[]{:S(2)}) collective-permute-start(bf16[4,16,64,128]{3,2,1,0:T(8,128)(2,1)S(1)} %all_to_all.11.refs_1_.refs_0_), channel_id=1, source_target_pairs={{0,128},{1,33},{2,130},{3,35},{4,132},{5,37},{6,134},{7,39},{8,136... | collective-permute-start | bytes 3145736 | tf_op jit(solution)/shard_map/ppermute | solution.py:28
  68.3 32.2 %collective-permute-start.5 = (bf16[4,16,64,128]{3,2,1,0:T(8,128)(2,1)S(1)}, bf16[4,16,64,128]{3,2,1,0:T(8,128)(2,1)S(1)}, u32[]{:S(2)}, u32[]{:S(2)}) collective-permute-start(bf16[4,16,64,128]{3,2,1,0:T(8,128)(2,1)S(1)} %all_to_all.11.refs_1_.refs_0_), channel_id=1, source_target_pairs={{0,1},{1,0},{2,3},{3,2},{4,5},{5,4},{6,7},{7,6},{8,9},{9,8},{10,11... | collective-permute-start | bytes 3145736 | tf_op jit(solution)/shard_map/ppermute | solution.py:28
  70.3 31.3 %collective-permute-start.6 = (bf16[4,16,64,128]{3,2,1,0:T(8,128)(2,1)S(1)}, bf16[4,16,64,128]{3,2,1,0:T(8,128)(2,1)S(1)}, u32[]{:S(2)}, u32[]{:S(2)}) collective-permute-start(bf16[4,16,64,128]{3,2,1,0:T(8,128)(2,1)S(1)} %collective-permute-done.1.refs_2_.refs_1_), channel_id=1, source_target_pairs={{0,1},{1,0},{2,3},{3,2},{4,5},{5,4},{6,7},{7,6},{8,9},{9,8},{10,11... | collective-permute-start | bytes 3145736 | tf_op jit(solution)/shard_map/ppermute | solution.py:28
  78.7 24.1 %collective-permute-start.7 = (bf16[4,16,64,128]{3,2,1,0:T(8,128)(2,1)S(1)}, bf16[4,16,64,128]{3,2,1,0:T(8,128)(2,1)S(1)}, u32[]{:S(2)}, u32[]{:S(2)}) collective-permute-start(bf16[4,16,64,128]{3,2,1,0:T(8,128)(2,1)S(1)} %collective-permute-done.2.refs_3_.refs_2_), channel_id=1, source_target_pairs={{0,1},{1,0},{2,3},{3,2},{4,5},{5,4},{6,7},{7,6},{8,9},{9,8},{10,11... | collective-permute-start | bytes 3145736 | tf_op jit(solution)/shard_map/ppermute | solution.py:28
  88.5 16.3 %collective-permute-start.4 = (bf16[4,16,64,128]{3,2,1,0:T(8,128)(2,1)S(1)}, bf16[4,16,64,128]{3,2,1,0:T(8,128)(2,1)S(1)}, u32[]{:S(2)}, u32[]{:S(2)}) collective-permute-start(bf16[4,16,64,128]{3,2,1,0:T(8,128)(2,1)S(1)} %collective-permute-done.3.refs_4_.refs_3_), channel_id=1, source_target_pairs={{0,1},{1,0},{2,3},{3,2},{4,5},{5,4},{6,7},{7,6},{8,9},{9,8},{10,11... | collective-permute-start | bytes 3145736 | tf_op jit(solution)/shard_map/ppermute | solution.py:28
  90.4 7.8 %collective-permute-start = (bf16[32,2048]{1,0:T(8,128)(2,1)S(1)}, bf16[32,2048]{1,0:T(8,128)(2,1)S(1)}, u32[]{:S(2)}, u32[]{:S(2)}) collective-permute-start(bf16[32,2048]{1,0:T(8,128)(2,1)S(1)} %slice_bitcast_fusion), channel_id=1, source_target_pairs={{0,32},{1,33},{2,34},{3,35},{4,36},{5,37},{6,38},{7,39},{8,40},{9,... | collective-permute-start | bytes 393224 | tf_op jit(solution)/shard_map/ppermute | solution.py:335

commit v5 on v4

--- a/solution.py
+++ b/solution.py
@@ -113,6 +113,22 @@
     folded = jnp.concatenate([first, last], axis=1)
     block = jnp.concatenate([turned, folded], axis=0)
     return jnp.broadcast_to(block[None], (16, 64, 128))
+
+
+def end_kernel(tokens, end):
+    end[...] = tokens[tokens.shape[0] - HALO :]
+
+
+def end_of(tokens):
+    return pl.pallas_call(
+        end_kernel,
+        out_shape=jax.ShapeDtypeStruct((HALO, tokens.shape[1]), BF16),
+        in_specs=[VMEM],
+        out_specs=VMEM,
+        compiler_params=params(3),
+        cost_estimate=cost(1 << 20),
+        name="end",
+    )(tokens)
 
 
 def head_kernel(halo, tokens, norm_gain, pool_gain, normed, gain_out):
@@ -331,10 +347,8 @@
 
 
 def mixed(tokens, norm_gain, in_weight, down_weight, pool_gain):
-    rows = tokens.shape[1]
-    halo = lax.ppermute(
-        tokens[0, rows - HALO :], AXES, [(i, i + 32) for i in range(480)]
-    )
+    end = end_of(tokens[0])
+    halo = lax.ppermute(end, AXES, [(i, i + 32) for i in range(480)])
     normed, pool_gain = head(halo, tokens[0], norm_gain, pool_gain)
     column = shared(packed(in_weight, down_weight), lambda y, x, z, c: (y, x, c))
     line = shared(

time: 111 us -> 111 us (level)
  no operation moved by 1% of the time
where the time goes in v5:
time: 111 us
  blocking collectives  46.5 us (42%)
  starting transfers between devices  30.2 us (27%)
  waiting for transfers between devices  19.8 us (18%)
  Pallas kernels  12.1 us (11%)
  other arithmetic  1.49 us (1%)
    all_to_all x2, blocking collectives, shared(): lax.all_to_all(copies, AXES, 0, 0, axis_index_groups=list(groups.values()...  46.5 us
    ppermute x7, starting transfers between devices, send(): return lax.ppermute(block, AXES, route)  28.2 us
    ppermute x7, waiting for transfers between devices, send(): return lax.ppermute(block, AXES, route)  13.9 us
    ppermute x1, waiting for transfers between devices, mixed(): halo = lax.ppermute(end, AXES, [(i, i + 32) for i in range(480)])  5.87 us
    pallas_call x1, Pallas kernels, mixer(): pl.pallas_call(mixer_kernel, out_shape=(jax.ShapeDtypeStruct(tokens.shape...  5.58 us
    pallas_call x3, Pallas kernels, placed(): pl.pallas_call(kernel, out_shape=(jax.ShapeDtypeStruct((2, rows, 256), F3...  4.24 us
    pallas_call x1, Pallas kernels, head(): pl.pallas_call(head_kernel, out_shape=(jax.ShapeDtypeStruct((HALO + token...  2.28 us
  transfers between devices with their start and end apart: 8, of which 3 were waited for; matrix products, arithmetic and copies ran while one was open for 0% of the time, Pallas kernels for 6%

profile of v5, /device:TPU:12, one launch (start us, length us, event | category | flops | bytes accessed | tf_op | source)
XLA Modules:
  0.0 110.5 jit_solution(11979658049231721512)
XLA Ops:
  0.0 0.7 select_bitcast_fusion.1
  0.7 0.8 maximum_maximum_fusion
  1.5 0.0 copy-start
  1.5 33.5 %all_to_all.10 = bf16[16,64,128]{2,1,0:T(8,128)(2,1)S(1)} all-to-all(bf16[16,64,128]{2,1,0:T(8,128)(2,1)S(1)} %broadcast_in_dim.6), channel_id=1, replica_groups={{0,2,4,6,8,10,12,14,16,18,20,22,24,26,28,30},{1,3,5,7,9,11,13,15,17,19,..., dimensions={0} | all-to-all | bytes 524288 | tf_op jit(solution)/shard_map/all_to_all | solution.py:35
  35.1 0.2 broadcast_in_dim.7
  35.3 0.0 copy-start.1
  35.3 0.0 copy-start.2
  35.3 13.0 %all_to_all.11.refs_1_.refs_0_ = bf16[4,16,64,128]{3,2,1,0:T(8,128)(2,1)S(1)} all-to-all(bf16[4,16,64,128]{3,2,1,0:T(8,128)(2,1)S(1)} %broadcast_in_dim.7), channel_id=1, replica_groups={{0,32,64,96},{1,129,257,385},{2,34,66,98},{3,131,259,387},{4,36,68,100}..., dimensions={0} | all-to-all | bytes 2097152 | tf_op jit(solution)/shard_map/all_to_all | solution.py:35
  48.3 5.0 %collective-permute-start.1 = (bf16[4,16,64,128]{3,2,1,0:T(8,128)(2,1)S(1)}, bf16[4,16,64,128]{3,2,1,0:T(8,128)(2,1)S(1)}, u32[]{:S(2)}, u32[]{:S(2)}) collective-permute-start(bf16[4,16,64,128]{3,2,1,0:T(8,128)(2,1)S(1)} %all_to_all.11.refs_1_.refs_0_), channel_id=1, source_target_pairs={{0,256},{1,65},{2,258},{3,67},{4,260},{5,69},{6,262},{7,71},{8,264... | collective-permute-start | bytes 3145736 | tf_op jit(solution)/shard_map/ppermute | solution.py:28
  53.3 13.2 %collective-permute-start.2 = (bf16[4,16,64,128]{3,2,1,0:T(8,128)(2,1)S(1)}, bf16[4,16,64,128]{3,2,1,0:T(8,128)(2,1)S(1)}, u32[]{:S(2)}, u32[]{:S(2)}) collective-permute-start(bf16[4,16,64,128]{3,2,1,0:T(8,128)(2,1)S(1)} %all_to_all.11.refs_1_.refs_0_), channel_id=1, source_target_pairs={{0,384},{1,97},{2,386},{3,99},{4,388},{5,101},{6,390},{7,103},{8,3... | collective-permute-start | bytes 3145736 | tf_op jit(solution)/shard_map/ppermute | solution.py:28
  66.5 1.9 %collective-permute-start.3 = (bf16[4,16,64,128]{3,2,1,0:T(8,128)(2,1)S(1)}, bf16[4,16,64,128]{3,2,1,0:T(8,128)(2,1)S(1)}, u32[]{:S(2)}, u32[]{:S(2)}) collective-permute-start(bf16[4,16,64,128]{3,2,1,0:T(8,128)(2,1)S(1)} %all_to_all.11.refs_1_.refs_0_), channel_id=1, source_target_pairs={{0,128},{1,33},{2,130},{3,35},{4,132},{5,37},{6,134},{7,39},{8,136... | collective-permute-start | bytes 3145736 | tf_op jit(solution)/shard_map/ppermute | solution.py:28
  68.4 1.9 %collective-permute-start.5 = (bf16[4,16,64,128]{3,2,1,0:T(8,128)(2,1)S(1)}, bf16[4,16,64,128]{3,2,1,0:T(8,128)(2,1)S(1)}, u32[]{:S(2)}, u32[]{:S(2)}) collective-permute-start(bf16[4,16,64,128]{3,2,1,0:T(8,128)(2,1)S(1)} %all_to_all.11.refs_1_.refs_0_), channel_id=1, source_target_pairs={{0,1},{1,0},{2,3},{3,2},{4,5},{5,4},{6,7},{7,6},{8,9},{9,8},{10,11... | collective-permute-start | bytes 3145736 | tf_op jit(solution)/shard_map/ppermute | solution.py:28
  70.4 0.0 collective-permute-done.1.refs_2_.refs_1_
  70.4 2.4 %collective-permute-start.6 = (bf16[4,16,64,128]{3,2,1,0:T(8,128)(2,1)S(1)}, bf16[4,16,64,128]{3,2,1,0:T(8,128)(2,1)S(1)}, u32[]{:S(2)}, u32[]{:S(2)}) collective-permute-start(bf16[4,16,64,128]{3,2,1,0:T(8,128)(2,1)S(1)} %collective-permute-done.1.refs_2_.refs_1_), channel_id=1, source_target_pairs={{0,1},{1,0},{2,3},{3,2},{4,5},{5,4},{6,7},{7,6},{8,9},{9,8},{10,11... | collective-permute-start | bytes 3145736 | tf_op jit(solution)/shard_map/ppermute | solution.py:28
  72.8 6.0 %collective-permute-done.2.refs_3_.refs_2_ = bf16[4,16,64,128]{3,2,1,0:T(8,128)(2,1)S(1)} collective-permute-done((bf16[4,16,64,128]{3,2,1,0:T(8,128)(2,1)S(1)}, bf16[4,16,64,128]{3,2,1,0:T(8,128)(2,1)S(1)}, u32[]{:S(2)}, u32[]{:S(2)}) %collective-permute-start.2) | collective-permute-done | bytes 1048608 | tf_op jit(solution)/shard_map/ppermute | solution.py:28
  78.8 1.9 %collective-permute-start.7 = (bf16[4,16,64,128]{3,2,1,0:T(8,128)(2,1)S(1)}, bf16[4,16,64,128]{3,2,1,0:T(8,128)(2,1)S(1)}, u32[]{:S(2)}, u32[]{:S(2)}) collective-permute-start(bf16[4,16,64,128]{3,2,1,0:T(8,128)(2,1)S(1)} %collective-permute-done.2.refs_3_.refs_2_), channel_id=1, source_target_pairs={{0,1},{1,0},{2,3},{3,2},{4,5},{5,4},{6,7},{7,6},{8,9},{9,8},{10,11... | collective-permute-start | bytes 3145736 | tf_op jit(solution)/shard_map/ppermute | solution.py:28
  80.7 7.9 %collective-permute-done.3.refs_4_.refs_3_ = bf16[4,16,64,128]{3,2,1,0:T(8,128)(2,1)S(1)} collective-permute-done((bf16[4,16,64,128]{3,2,1,0:T(8,128)(2,1)S(1)}, bf16[4,16,64,128]{3,2,1,0:T(8,128)(2,1)S(1)}, u32[]{:S(2)}, u32[]{:S(2)}) %collective-permute-start.3) | collective-permute-done | bytes 1048608 | tf_op jit(solution)/shard_map/ppermute | solution.py:28
  88.6 1.9 %collective-permute-start.4 = (bf16[4,16,64,128]{3,2,1,0:T(8,128)(2,1)S(1)}, bf16[4,16,64,128]{3,2,1,0:T(8,128)(2,1)S(1)}, u32[]{:S(2)}, u32[]{:S(2)}) collective-permute-start(bf16[4,16,64,128]{3,2,1,0:T(8,128)(2,1)S(1)} %collective-permute-done.3.refs_4_.refs_3_), channel_id=1, source_target_pairs={{0,1},{1,0},{2,3},{3,2},{4,5},{5,4},{6,7},{7,6},{8,9},{9,8},{10,11... | collective-permute-start | bytes 3145736 | tf_op jit(solution)/shard_map/ppermute | solution.py:28
  90.5 0.0 copy-done
  90.6 1.9 %collective-permute-start = (bf16[32,2048]{1,0:T(8,128)(2,1)S(1)}, bf16[32,2048]{1,0:T(8,128)(2,1)S(1)}, u32[]{:S(2)}, u32[]{:S(2)}) collective-permute-start(bf16[32,2048]{1,0:T(8,128)(2,1)S(1)} %end.1), channel_id=1, source_target_pairs={{0,32},{1,33},{2,34},{3,35},{4,36},{5,37},{6,38},{7,39},{8,40},{9,... | collective-permute-start | bytes 393224 | tf_op jit(solution)/shard_map/ppermute | solution.py:351
  92.5 5.9 %collective-permute-done.halo = bf16[32,2048]{1,0:T(8,128)(2,1)S(1)} collective-permute-done((bf16[32,2048]{1,0:T(8,128)(2,1)S(1)}, bf16[32,2048]{1,0:T(8,128)(2,1)S(1)}, u32[]{:S(2)}, u32[]{:S(2)}) %collective-permute-start) | collective-permute-done | bytes 131104 | tf_op jit(solution)/shard_map/ppermute | solution.py:351
  98.4 0.0 copy-done.1
  98.4 0.0 copy-done.2
  98.4 2.3 %head.1 = (bf16[416,2048]{1,0:T(8,128)(2,1)S(1)}, f32[2,512]{1,0:T(2,128)S(1)}) custom-call(bf16[32,2048]{1,0:T(8,128)(2,1)S(1)} %collective-permute-done.halo, bf16[384,2048]{1,0:T(8,128)(2,1)S(1)} %bitcast.10, f32[2,2048]{1,0:T(2,128)S(1)} %copy-done.1, f32[2,512]{1,0:T(2,128)S(1)} %copy-done.2), custom_call_target="tpu_custom_call" | custom-call | flops 1073741824 | bytes 1048576 | tf_op jit(solution)/shard_map/head/pallas_call | solution.py:161
  100.7 0.0 collective-permute-done.5.refs_2_.refs_3_.refs_5_
  100.7 1.1 shard_map.55
  101.7 0.0 collective-permute-done.6.refs_4_.refs_6_
  101.7 1.2 %shard_map.56 = (f32[2,416,256]{2,1,0:T(8,128)S(1)}, bf16[2,16,16,2048]{3,2,1,0:T(8,128)(2,1)S(1)}, bf16[2,2,256,2048]{3,2,1,0:T(8,128)(2,1)S(1)}) custom-call(bf16[416,2048]{1,0:T(8,128)(2,1)S(1)} %get-tuple-element.18.refs_0_.left, ...), custom_call_target="tpu_custom_call", output_to_operand_aliasing={{0}: (5, {}), {1}: (6, {}), {2}: (7, {})} | custom-call | flops 536870912 | bytes 1048576 | tf_op jit(solution)/shard_map/pallas_call | solution.py:189
  102.9 0.0 collective-permute-done.7.refs_7_
  102.9 2.0 %shard_map.57 = (f32[2,416,256]{2,1,0:T(8,128)S(1)}, bf16[2,16,16,2048]{3,2,1,0:T(8,128)(2,1)S(1)}, bf16[2,2,256,2048]{3,2,1,0:T(8,128)(2,1)S(1)}) custom-call(bf16[416,2048]{1,0:T(8,128)(2,1)S(1)} %get-tuple-element.18.refs_0_.left, ...), custom_call_target="tpu_custom_call", output_to_operand_aliasing={{0}: (8, {}), {1}: (9, {}), {2}: (10, {})} | custom-call | flops 536870912 | bytes 1048576 | tf_op jit(solution)/shard_map/pallas_call | solution.py:189
  104.9 0.0 collective-permute-done.4.refs_4_
  105.0 5.6 %mixer.1 = (bf16[384,2048]{1,0:T(8,128)(2,1)}, f32[2,416,256]{2,1,0:T(8,128)S(1)}, bf16[2,16,16,2048]{3,2,1,0:T(8,128)(2,1)S(1)}, bf16[2,2,256,2048]{3,2,1,0:T(8,128)(2,1)S(1)}) custom-call(bf16[384,2048]{1,0:T(8,128)(2,1)S(1)} %bitcast.11, ...), custom_call_target="tpu_custom_call", output_to_operand_aliasing={{1}: (10, {}), {2}: (11, {}), {3}: (12, {})} | custom-call | flops 4294967296 | bytes 1048576 | tf_op jit(solution)/shard_map/mixer/pallas_call | solution.py:325
  (2 shorter events, 0.1 us)
Async XLA Ops:
  1.5 89.1 %copy-start = (bf16[1,384,2048]{2,1,0:T(8,128)(2,1)S(1)}, bf16[1,384,2048]{2,1,0:T(8,128)(2,1)}, u32[]{:S(2)}) copy-start(bf16[1,384,2048]{2,1,0:T(8,128)(2,1)} %param.5) | copy-start | bytes 4718596
  35.3 63.1 %copy-start.1 = (f32[2,2048]{1,0:T(2,128)S(1)}, f32[2,2048]{1,0:T(2,128)}, u32[]{:S(2)}) copy-start(f32[2,2048]{1,0:T(2,128)} %norm_gain.3) | copy-start | bytes 49156
  35.3 63.0 %copy-start.2 = (f32[2,512]{1,0:T(2,128)S(1)}, f32[2,512]{1,0:T(2,128)}, u32[]{:S(2)}) copy-start(f32[2,512]{1,0:T(2,128)} %pool_gain.1) | copy-start | bytes 12292
  48.3 22.1 %collective-permute-start.1 = (bf16[4,16,64,128]{3,2,1,0:T(8,128)(2,1)S(1)}, bf16[4,16,64,128]{3,2,1,0:T(8,128)(2,1)S(1)}, u32[]{:S(2)}, u32[]{:S(2)}) collective-permute-start(bf16[4,16,64,128]{3,2,1,0:T(8,128)(2,1)S(1)} %all_to_all.11.refs_1_.refs_0_), channel_id=1, source_target_pairs={{0,256},{1,65},{2,258},{3,67},{4,260},{5,69},{6,262},{7,71},{8,264... | collective-permute-start | bytes 3145736 | tf_op jit(solution)/shard_map/ppermute | solution.py:28
  53.3 25.5 %collective-permute-start.2 = (bf16[4,16,64,128]{3,2,1,0:T(8,128)(2,1)S(1)}, bf16[4,16,64,128]{3,2,1,0:T(8,128)(2,1)S(1)}, u32[]{:S(2)}, u32[]{:S(2)}) collective-permute-start(bf16[4,16,64,128]{3,2,1,0:T(8,128)(2,1)S(1)} %all_to_all.11.refs_1_.refs_0_), channel_id=1, source_target_pairs={{0,384},{1,97},{2,386},{3,99},{4,388},{5,101},{6,390},{7,103},{8,3... | collective-permute-start | bytes 3145736 | tf_op jit(solution)/shard_map/ppermute | solution.py:28
  66.5 22.1 %collective-permute-start.3 = (bf16[4,16,64,128]{3,2,1,0:T(8,128)(2,1)S(1)}, bf16[4,16,64,128]{3,2,1,0:T(8,128)(2,1)S(1)}, u32[]{:S(2)}, u32[]{:S(2)}) collective-permute-start(bf16[4,16,64,128]{3,2,1,0:T(8,128)(2,1)S(1)} %all_to_all.11.refs_1_.refs_0_), channel_id=1, source_target_pairs={{0,128},{1,33},{2,130},{3,35},{4,132},{5,37},{6,134},{7,39},{8,136... | collective-permute-start | bytes 3145736 | tf_op jit(solution)/shard_map/ppermute | solution.py:28
  68.4 32.2 %collective-permute-start.5 = (bf16[4,16,64,128]{3,2,1,0:T(8,128)(2,1)S(1)}, bf16[4,16,64,128]{3,2,1,0:T(8,128)(2,1)S(1)}, u32[]{:S(2)}, u32[]{:S(2)}) collective-permute-start(bf16[4,16,64,128]{3,2,1,0:T(8,128)(2,1)S(1)} %all_to_all.11.refs_1_.refs_0_), channel_id=1, source_target_pairs={{0,1},{1,0},{2,3},{3,2},{4,5},{5,4},{6,7},{7,6},{8,9},{9,8},{10,11... | collective-permute-start | bytes 3145736 | tf_op jit(solution)/shard_map/ppermute | solution.py:28
  70.4 31.3 %collective-permute-start.6 = (bf16[4,16,64,128]{3,2,1,0:T(8,128)(2,1)S(1)}, bf16[4,16,64,128]{3,2,1,0:T(8,128)(2,1)S(1)}, u32[]{:S(2)}, u32[]{:S(2)}) collective-permute-start(bf16[4,16,64,128]{3,2,1,0:T(8,128)(2,1)S(1)} %collective-permute-done.1.refs_2_.refs_1_), channel_id=1, source_target_pairs={{0,1},{1,0},{2,3},{3,2},{4,5},{5,4},{6,7},{7,6},{8,9},{9,8},{10,11... | collective-permute-start | bytes 3145736 | tf_op jit(solution)/shard_map/ppermute | solution.py:28
  78.8 24.1 %collective-permute-start.7 = (bf16[4,16,64,128]{3,2,1,0:T(8,128)(2,1)S(1)}, bf16[4,16,64,128]{3,2,1,0:T(8,128)(2,1)S(1)}, u32[]{:S(2)}, u32[]{:S(2)}) collective-permute-start(bf16[4,16,64,128]{3,2,1,0:T(8,128)(2,1)S(1)} %collective-permute-done.2.refs_3_.refs_2_), channel_id=1, source_target_pairs={{0,1},{1,0},{2,3},{3,2},{4,5},{5,4},{6,7},{7,6},{8,9},{9,8},{10,11... | collective-permute-start | bytes 3145736 | tf_op jit(solution)/shard_map/ppermute | solution.py:28
  88.6 16.3 %collective-permute-start.4 = (bf16[4,16,64,128]{3,2,1,0:T(8,128)(2,1)S(1)}, bf16[4,16,64,128]{3,2,1,0:T(8,128)(2,1)S(1)}, u32[]{:S(2)}, u32[]{:S(2)}) collective-permute-start(bf16[4,16,64,128]{3,2,1,0:T(8,128)(2,1)S(1)} %collective-permute-done.3.refs_4_.refs_3_), channel_id=1, source_target_pairs={{0,1},{1,0},{2,3},{3,2},{4,5},{5,4},{6,7},{7,6},{8,9},{9,8},{10,11... | collective-permute-start | bytes 3145736 | tf_op jit(solution)/shard_map/ppermute | solution.py:28
  90.6 7.8 %collective-permute-start = (bf16[32,2048]{1,0:T(8,128)(2,1)S(1)}, bf16[32,2048]{1,0:T(8,128)(2,1)S(1)}, u32[]{:S(2)}, u32[]{:S(2)}) collective-permute-start(bf16[32,2048]{1,0:T(8,128)(2,1)S(1)} %end.1), channel_id=1, source_target_pairs={{0,32},{1,33},{2,34},{3,35},{4,36},{5,37},{6,38},{7,39},{8,40},{9,... | collective-permute-start | bytes 393224 | tf_op jit(solution)/shard_map/ppermute | solution.py:351

commit v6 on v5

--- a/solution.py
+++ b/solution.py
@@ -9,7 +9,7 @@
 HALO = 32
 PAD = 16
 AXES = ("sp", "tp")
-PIECES = (0, 2, 1, -1)
+PIECES = (0, -1, 1, 2)
 VMEM = pl.BlockSpec(memory_space=pltpu.VMEM)
 BF16, F32 = jnp.bfloat16, jnp.float32
 
@@ -60,8 +60,8 @@
     return (second + PIECES[k] + 4) % 4
 
 
-def part(left, piece, core, s):
-    lhs = jnp.concatenate([left[:, lanes_of(core, s, f)] for f in range(4)], axis=1)
+def part(left, rows, piece, core, s):
+    lhs = jnp.concatenate([left[rows, lanes_of(core, s, f)] for f in range(4)], axis=1)
     rhs = jnp.concatenate(
         [piece[f, :, 0:16].reshape(256, 128) for f in range(4)], axis=1
     )
@@ -131,21 +131,21 @@
     )(tokens)
 
 
-def head_kernel(halo, tokens, norm_gain, pool_gain, normed, gain_out):
-    gain = norm_gain[0:1]
-
-    def norm_rows(block):
-        residual = block.astype(F32)
-        mean = jnp.mean(residual * residual, axis=1, keepdims=True)
-        return (residual * lax.rsqrt(mean + EPS) * gain).astype(BF16)
-
+def norm_rows(block, gain):
+    residual = block.astype(F32)
+    mean = jnp.mean(residual * residual, axis=1, keepdims=True)
+    return (residual * lax.rsqrt(mean + EPS) * gain).astype(BF16)
+
+
+def head_kernel(tokens, norm_gain, pool_gain, normed, gain_out):
     def norm(i, carry):
         rows = pl.multiple_of(i * 32, 32)
-        normed[pl.ds(HALO + rows, 32)] = norm_rows(tokens[pl.ds(rows, 32)])
+        normed[pl.ds(HALO + rows, 32)] = norm_rows(
+            tokens[pl.ds(rows, 32)], norm_gain[0:1]
+        )
         return carry
 
     lax.fori_loop(0, tokens.shape[0] // 32, norm, 0)
-    normed[:HALO] = norm_rows(halo[...])
     old = lax.broadcasted_iota(jnp.int32, (512, 512), 0)
     new = lax.broadcasted_iota(jnp.int32, (512, 512), 1)
     source = new % 256 // 16 * 32 + new // 256 * 16 + new % 16
@@ -157,19 +157,19 @@
     )
 
 
-def head(halo, tokens, norm_gain, pool_gain):
+def head(tokens, norm_gain, pool_gain):
     return pl.pallas_call(
         head_kernel,
         out_shape=(
             jax.ShapeDtypeStruct((HALO + tokens.shape[0], 2048), BF16),
             jax.ShapeDtypeStruct(pool_gain.shape, F32),
         ),
-        in_specs=[VMEM] * 4,
+        in_specs=[VMEM] * 3,
         out_specs=(VMEM, VMEM),
         compiler_params=params(5),
         cost_estimate=cost(1 << 30),
         name="head",
-    )(halo, tokens, norm_gain, pool_gain)
+    )(tokens, norm_gain, pool_gain)
 
 
 def wholes():
@@ -179,63 +179,66 @@
     )
 
 
-def placed(body, mib, normed, pieces, so_far):
-    rows = normed.shape[0]
-    count = 1 + len(pieces)
+def placed(body, mib, inputs, state):
+    rows = state[0].shape[0]
+    count = len(inputs)
 
     def kernel(*refs):
-        body(refs[0], refs[1:count], refs[count:-3], *refs[-3:])
+        body(refs[:count], *refs[-4:])
 
     return pl.pallas_call(
         kernel,
-        out_shape=(jax.ShapeDtypeStruct((2, rows, 256), F32), *wholes()),
-        in_specs=[VMEM] * (count + len(so_far)),
-        out_specs=(VMEM,) * 3,
-        input_output_aliases={count + i: i for i in range(len(so_far))},
+        out_shape=(
+            jax.ShapeDtypeStruct((rows, 2048), BF16),
+            jax.ShapeDtypeStruct((2, rows, 256), F32),
+            *wholes(),
+        ),
+        in_specs=[VMEM] * (count + len(state)),
+        out_specs=(VMEM,) * 4,
+        input_output_aliases={count + i: i for i in range(len(state))},
         compiler_params=params(mib),
         cost_estimate=cost(1 << 29),
-    )(normed, *pieces, *so_far)
-
-
-def place_a(normed, pieces, so_far, total, whole_in, whole_down):
-    mine, theirs = pieces
+    )(*inputs, *state)
+
+
+def place_a(inputs, normed, total, whole_in, whole_down):
+    mine, theirs = inputs
     c, s_mine, s_theirs = seconds()
     for slot, piece, core, second in ((0, mine, c, s_mine), (1, theirs, 1 - c, s_theirs)):
         s = along(second, 0)
-        total[slot] = part(normed, piece, core, s)
+        rows = slice(HALO, None)
+        total[slot, rows] = part(normed, rows, piece, core, s)
         put_in(piece, core, s, whole_in)
     put_down((mine,), (theirs,), ((0, 0),), whole_down)
 
 
-def place_b(normed, pieces, so_far, total, whole_in, whole_down):
-    mine, theirs = pieces[:2], pieces[2:]
+def place_b(inputs, normed, total, whole_in, whole_down):
+    halo, norm_gain, *pieces = inputs
+    mine, theirs = pieces[:3], pieces[3:]
+    normed[:HALO] = norm_rows(halo[...], norm_gain[0:1])
     c, s_mine, s_theirs = seconds()
-    for slot, piece, core, second in (
-        (0, mine[1], c, s_mine),
-        (1, theirs[1], 1 - c, s_theirs),
-    ):
-        s = along(second, 1)
-        total[slot] += part(normed, piece, core, s)
-        put_in(piece, core, s, whole_in)
-    put_down(mine, theirs, ((0, 1), (1, 0), (1, 1)), whole_down)
-
-
-def place_c(normed, pieces, so_far, total, whole_in, whole_down):
-    mine, theirs = pieces[:4], pieces[4:]
-    c, s_mine, s_theirs = seconds()
-    for slot, piece, core, s in (
-        (0, mine[2], c, along(s_mine, 2)),
-        (0, mine[3], c, along(s_mine, 3)),
-        (1, theirs[2], 1 - c, along(s_theirs, 2)),
-    ):
-        total[slot] += part(normed, piece, core, s)
-        put_in(piece, core, s, whole_in)
-    pairs = [(k, j) for k in range(4) for j in range(3) if k > 1 or j > 1]
+    for slot, of, core, second in ((0, mine, c, s_mine), (1, theirs, 1 - c, s_theirs)):
+        rows = slice(0, HALO)
+        total[slot, rows] = part(normed, rows, of[0], core, along(second, 0))
+        for k in (1, 2):
+            s = along(second, k)
+            total[slot] += part(normed, slice(None), of[k], core, s)
+            put_in(of[k], core, s, whole_in)
+    pairs = [(k, j) for k in range(3) for j in range(3) if k + j > 0]
     put_down(mine, theirs, pairs, whole_down)
 
 
-def mixer_kernel(tokens, halo, norm_gain, pool_gain, left, *refs):
-    mine, theirs = refs[:4], (None, None, None, refs[4])
+def place_c(inputs, normed, total, whole_in, whole_down):
+    mine, theirs = (None, None, None, inputs[0]), inputs[1:]
+    c, s_mine, _ = seconds()
+    s = along(s_mine, 3)
+    total[0] += part(normed, slice(None), mine[3], c, s)
+    put_in(mine[3], c, s, whole_in)
+    put_down(mine, theirs, [(3, j) for j in range(3)], whole_down)
+
+
+def mixer_kernel(tokens, halo, norm_gain, pool_gain, *refs):
+    mine, theirs, left = refs[:4], (None, None, None, refs[4]), refs[5]
     out, total, whole_in, whole_down = refs[-10:-6]
     extended, pooled, middle, scaled, last, sems = refs[-6:]
     c, _, s_theirs = seconds()
@@ -274,7 +277,7 @@
 
     extended[PAD:, pl.ds(pl.multiple_of(c * 256, 256), 256)] = rounded(total[0])
     extended[PAD:, pl.ds(pl.multiple_of((1 - c) * 256, 256), 256)] = rounded(
-        total[1] + part(left, theirs[3], 1 - c, s)
+        total[1] + part(left, slice(None), theirs[3], 1 - c, s)
     )
     pool(0)
     squares = jnp.zeros((rows, 128), F32)
@@ -319,8 +322,8 @@
         copy.wait()
 
 
-def mixer(tokens, halo, norm_gain, pool_gain, normed, pieces, so_far):
-    rows = normed.shape[0]
+def mixer(tokens, halo, norm_gain, pool_gain, pieces, state):
+    rows = state[0].shape[0]
     at = 5 + len(pieces)
     return pl.pallas_call(
         mixer_kernel,
@@ -343,27 +346,27 @@
         compiler_params=params(16),
         cost_estimate=cost(4 << 30),
         name="mixer",
-    )(tokens, halo, norm_gain, pool_gain, normed, *pieces, *so_far)[0]
+    )(tokens, halo, norm_gain, pool_gain, *pieces, *state)[0]
 
 
 def mixed(tokens, norm_gain, in_weight, down_weight, pool_gain):
     end = end_of(tokens[0])
     halo = lax.ppermute(end, AXES, [(i, i + 32) for i in range(480)])
-    normed, pool_gain = head(halo, tokens[0], norm_gain, pool_gain)
+    normed, pool_gain = head(tokens[0], norm_gain, pool_gain)
     column = shared(packed(in_weight, down_weight), lambda y, x, z, c: (y, x, c))
     line = shared(
         jnp.broadcast_to(column[None], (4, 16, 64, 128)),
         lambda y, x, z, c: (y, z, c) if c == 0 else (x, z, c),
     )
-    names = (2, -1, 1)
+    names = (1, -1, 2)
     mine = [line] + [send(line, second_hop(d)) for d in names]
     theirs = [send(piece, other_core) for piece in mine]
-    so_far = placed(place_a, 10, normed, mine[:1] + theirs[:1], ())
-    so_far = placed(place_b, 10, normed, mine[:2] + theirs[:2], so_far)
-    so_far = placed(place_c, 12, normed, mine + theirs[:3], so_far)
-    return mixer(
-        tokens[0], halo, norm_gain, pool_gain, normed, mine + theirs[3:], so_far
-    )[None]
+    state = placed(place_a, 10, mine[:1] + theirs[:1], (normed,))
+    inputs = [halo, norm_gain, *mine[:3], *theirs[:3]]
+    state = placed(place_b, 10, inputs, state)
+    state = placed(place_c, 10, mine[3:] + theirs[:3], state)
+    pieces = mine + theirs[3:]
+    return mixer(tokens[0], halo, norm_gain, pool_gain, pieces, state)[None]
 
 
 def solution(mesh):

time: 111 us -> 106 us (0.955)
  the two profiles are of different devices: /device:TPU:12 before, /device:TPU:24 now
where the time goes in v6:
time: 106 us
  blocking collectives  50.1 us (47%)
  waiting for transfers between devices  22.6 us (21%)
  starting transfers between devices  18.8 us (18%)
  Pallas kernels  12.2 us (12%)
  other arithmetic  1.49 us (1%)
    all_to_all x2, blocking collectives, shared(): lax.all_to_all(copies, AXES, 0, 0, axis_index_groups=list(groups.values()...  50.1 us
    ppermute x7, waiting for transfers between devices, send(): return lax.ppermute(block, AXES, route)  18.4 us
    ppermute x7, starting transfers between devices, send(): return lax.ppermute(block, AXES, route)  16.9 us
    pallas_call x1, Pallas kernels, mixer(): pl.pallas_call(mixer_kernel, out_shape=(jax.ShapeDtypeStruct(tokens.shape...  5.6 us
    pallas_call x3, Pallas kernels, placed(): pl.pallas_call(kernel, out_shape=(jax.ShapeDtypeStruct((rows, 2048), BF16...  4.36 us
    ppermute x1, waiting for transfers between devices, mixed(): halo = lax.ppermute(end, AXES, [(i, i + 32) for i in range(480)])  4.18 us
    pallas_call x1, Pallas kernels, head(): pl.pallas_call(head_kernel, out_shape=(jax.ShapeDtypeStruct((HALO + token...  2.25 us
  transfers between devices with their start and end apart: 8, of which 3 were waited for; matrix products, arithmetic and copies ran while one was open for 0% of the time, Pallas kernels for 6%

profile of v6, /device:TPU:24, one launch (start us, length us, event | category | flops | bytes accessed | tf_op | source)
XLA Modules:
  0.0 105.7 jit_solution(6249056345924177968)
XLA Ops:
  0.0 0.7 select_bitcast_fusion.1
  0.7 0.8 maximum_maximum_fusion
  1.5 0.0 copy-start
  1.5 33.5 %all_to_all.10 = bf16[16,64,128]{2,1,0:T(8,128)(2,1)S(1)} all-to-all(bf16[16,64,128]{2,1,0:T(8,128)(2,1)S(1)} %broadcast_in_dim.6), channel_id=1, replica_groups={{0,2,4,6,8,10,12,14,16,18,20,22,24,26,28,30},{1,3,5,7,9,11,13,15,17,19,..., dimensions={0} | all-to-all | bytes 524288 | tf_op jit(solution)/shard_map/all_to_all | solution.py:35
  35.1 0.2 broadcast_in_dim.7
  35.3 0.0 copy-start.1
  35.3 0.0 copy-start.2
  35.3 16.6 %all_to_all.11.refs_0_.refs_2_ = bf16[4,16,64,128]{3,2,1,0:T(8,128)(2,1)S(1)} all-to-all(bf16[4,16,64,128]{3,2,1,0:T(8,128)(2,1)S(1)} %broadcast_in_dim.7), channel_id=1, replica_groups={{0,32,64,96},{1,129,257,385},{2,34,66,98},{3,131,259,387},{4,36,68,100}..., dimensions={0} | all-to-all | bytes 2097152 | tf_op jit(solution)/shard_map/all_to_all | solution.py:35
  51.9 1.9 %collective-permute-start.1 = (bf16[4,16,64,128]{3,2,1,0:T(8,128)(2,1)S(1)}, bf16[4,16,64,128]{3,2,1,0:T(8,128)(2,1)S(1)}, u32[]{:S(2)}, u32[]{:S(2)}) collective-permute-start(bf16[4,16,64,128]{3,2,1,0:T(8,128)(2,1)S(1)} %all_to_all.11.refs_0_.refs_2_), channel_id=1, source_target_pairs={{0,128},{1,33},{2,130},{3,35},{4,132},{5,37},{6,134},{7,39},{8,136... | collective-permute-start | bytes 3145736 | tf_op jit(solution)/shard_map/ppermute | solution.py:28
  53.9 3.9 %collective-permute-start.2 = (bf16[4,16,64,128]{3,2,1,0:T(8,128)(2,1)S(1)}, bf16[4,16,64,128]{3,2,1,0:T(8,128)(2,1)S(1)}, u32[]{:S(2)}, u32[]{:S(2)}) collective-permute-start(bf16[4,16,64,128]{3,2,1,0:T(8,128)(2,1)S(1)} %all_to_all.11.refs_0_.refs_2_), channel_id=1, source_target_pairs={{0,384},{1,97},{2,386},{3,99},{4,388},{5,101},{6,390},{7,103},{8,3... | collective-permute-start | bytes 3145736 | tf_op jit(solution)/shard_map/ppermute | solution.py:28
  57.8 2.9 %collective-permute-start.3 = (bf16[4,16,64,128]{3,2,1,0:T(8,128)(2,1)S(1)}, bf16[4,16,64,128]{3,2,1,0:T(8,128)(2,1)S(1)}, u32[]{:S(2)}, u32[]{:S(2)}) collective-permute-start(bf16[4,16,64,128]{3,2,1,0:T(8,128)(2,1)S(1)} %all_to_all.11.refs_0_.refs_2_), channel_id=1, source_target_pairs={{0,256},{1,65},{2,258},{3,67},{4,260},{5,69},{6,262},{7,71},{8,264... | collective-permute-start | bytes 3145736 | tf_op jit(solution)/shard_map/ppermute | solution.py:28
  60.7 1.9 %collective-permute-start.5 = (bf16[4,16,64,128]{3,2,1,0:T(8,128)(2,1)S(1)}, bf16[4,16,64,128]{3,2,1,0:T(8,128)(2,1)S(1)}, u32[]{:S(2)}, u32[]{:S(2)}) collective-permute-start(bf16[4,16,64,128]{3,2,1,0:T(8,128)(2,1)S(1)} %all_to_all.11.refs_0_.refs_2_), channel_id=1, source_target_pairs={{0,1},{1,0},{2,3},{3,2},{4,5},{5,4},{6,7},{7,6},{8,9},{9,8},{10,11... | collective-permute-start | bytes 3145736 | tf_op jit(solution)/shard_map/ppermute | solution.py:28
  62.7 6.0 %collective-permute-done.1.refs_3_.refs_1_ = bf16[4,16,64,128]{3,2,1,0:T(8,128)(2,1)S(1)} collective-permute-done((bf16[4,16,64,128]{3,2,1,0:T(8,128)(2,1)S(1)}, bf16[4,16,64,128]{3,2,1,0:T(8,128)(2,1)S(1)}, u32[]{:S(2)}, u32[]{:S(2)}) %collective-permute-start.1) | collective-permute-done | bytes 1048608 | tf_op jit(solution)/shard_map/ppermute | solution.py:28
  68.6 1.9 %collective-permute-start.6 = (bf16[4,16,64,128]{3,2,1,0:T(8,128)(2,1)S(1)}, bf16[4,16,64,128]{3,2,1,0:T(8,128)(2,1)S(1)}, u32[]{:S(2)}, u32[]{:S(2)}) collective-permute-start(bf16[4,16,64,128]{3,2,1,0:T(8,128)(2,1)S(1)} %collective-permute-done.1.refs_3_.refs_1_), channel_id=1, source_target_pairs={{0,1},{1,0},{2,3},{3,2},{4,5},{5,4},{6,7},{7,6},{8,9},{9,8},{10,11... | collective-permute-start | bytes 3145736 | tf_op jit(solution)/shard_map/ppermute | solution.py:28
  70.5 12.5 %collective-permute-done.2.refs_4_.refs_2_ = bf16[4,16,64,128]{3,2,1,0:T(8,128)(2,1)S(1)} collective-permute-done((bf16[4,16,64,128]{3,2,1,0:T(8,128)(2,1)S(1)}, bf16[4,16,64,128]{3,2,1,0:T(8,128)(2,1)S(1)}, u32[]{:S(2)}, u32[]{:S(2)}) %collective-permute-start.2) | collective-permute-done | bytes 1048608 | tf_op jit(solution)/shard_map/ppermute | solution.py:28
  83.0 1.9 %collective-permute-start.7 = (bf16[4,16,64,128]{3,2,1,0:T(8,128)(2,1)S(1)}, bf16[4,16,64,128]{3,2,1,0:T(8,128)(2,1)S(1)}, u32[]{:S(2)}, u32[]{:S(2)}) collective-permute-start(bf16[4,16,64,128]{3,2,1,0:T(8,128)(2,1)S(1)} %collective-permute-done.2.refs_4_.refs_2_), channel_id=1, source_target_pairs={{0,1},{1,0},{2,3},{3,2},{4,5},{5,4},{6,7},{7,6},{8,9},{9,8},{10,11... | collective-permute-start | bytes 3145736 | tf_op jit(solution)/shard_map/ppermute | solution.py:28
  84.9 0.0 collective-permute-done.3.refs_0_.refs_3_
  84.9 2.4 %collective-permute-start.4 = (bf16[4,16,64,128]{3,2,1,0:T(8,128)(2,1)S(1)}, bf16[4,16,64,128]{3,2,1,0:T(8,128)(2,1)S(1)}, u32[]{:S(2)}, u32[]{:S(2)}) collective-permute-start(bf16[4,16,64,128]{3,2,1,0:T(8,128)(2,1)S(1)} %collective-permute-done.3.refs_0_.refs_3_), channel_id=1, source_target_pairs={{0,1},{1,0},{2,3},{3,2},{4,5},{5,4},{6,7},{7,6},{8,9},{9,8},{10,11... | collective-permute-start | bytes 3145736 | tf_op jit(solution)/shard_map/ppermute | solution.py:28
  87.3 0.0 copy-done
  87.4 1.9 %collective-permute-start = (bf16[32,2048]{1,0:T(8,128)(2,1)S(1)}, bf16[32,2048]{1,0:T(8,128)(2,1)S(1)}, u32[]{:S(2)}, u32[]{:S(2)}) collective-permute-start(bf16[32,2048]{1,0:T(8,128)(2,1)S(1)} %end.1), channel_id=1, source_target_pairs={{0,32},{1,33},{2,34},{3,35},{4,36},{5,37},{6,38},{7,39},{8,40},{9,... | collective-permute-start | bytes 393224 | tf_op jit(solution)/shard_map/ppermute | solution.py:354
  89.3 0.0 copy-done.1
  89.3 0.0 copy-done.2
  89.3 2.2 %head.1 = (bf16[416,2048]{1,0:T(8,128)(2,1)S(1)}, f32[2,512]{1,0:T(2,128)S(1)}) custom-call(bf16[384,2048]{1,0:T(8,128)(2,1)S(1)} %bitcast.10, f32[2,2048]{1,0:T(2,128)S(1)} %copy-done.1, f32[2,512]{1,0:T(2,128)S(1)} %copy-done.2), custom_call_target="tpu_custom_call" | custom-call | flops 1073741824 | bytes 1048576 | tf_op jit(solution)/shard_map/head/pallas_call | solution.py:161
  91.6 0.0 collective-permute-done.5.refs_1_.refs_5_
  91.6 1.0 shard_map.55
  92.6 4.2 %collective-permute-done.refs_0_.halo = bf16[32,2048]{1,0:T(8,128)(2,1)S(1)} collective-permute-done((bf16[32,2048]{1,0:T(8,128)(2,1)S(1)}, bf16[32,2048]{1,0:T(8,128)(2,1)S(1)}, u32[]{:S(2)}, u32[]{:S(2)}) %collective-permute-start) | collective-permute-done | bytes 131104 | tf_op jit(solution)/shard_map/ppermute | solution.py:354
  96.8 0.0 collective-permute-done.6.refs_6_.refs_2_
  96.8 0.0 collective-permute-done.7.refs_7_.refs_3_
  96.8 2.7 %shard_map.56 = (bf16[416,2048]{1,0:T(8,128)(2,1)S(1)}, f32[2,416,256]{2,1,0:T(8,128)S(1)}, bf16[2,16,16,2048]{3,2,1,0:T(8,128)(2,1)S(1)}, bf16[2,2,256,2048]{3,2,1,0:T(8,128)(2,1)S(1)}) custom-call(bf16[32,2048]{1,0:T(8,128)(2,1)S(1)} %collective-permute-done.refs_0_.halo, ...), custom_call_target="tpu_custom_call", output_to_operand_aliasing={{0}: (8, {}), {1}: (9, {}), {2}: (10, {}), {3}: (11, {})} | custom-call | flops 536870912 | bytes 1048576 | tf_op jit(solution)/shard_map/pallas_call | solution.py:189
  99.5 0.6 shard_map.57
  100.1 0.0 collective-permute-done.4.refs_4_
  100.1 5.6 %mixer.1 = (bf16[384,2048]{1,0:T(8,128)(2,1)}, f32[2,416,256]{2,1,0:T(8,128)S(1)}, bf16[2,16,16,2048]{3,2,1,0:T(8,128)(2,1)S(1)}, bf16[2,2,256,2048]{3,2,1,0:T(8,128)(2,1)S(1)}) custom-call(bf16[384,2048]{1,0:T(8,128)(2,1)S(1)} %bitcast.11, ...), custom_call_target="tpu_custom_call", output_to_operand_aliasing={{1}: (10, {}), {2}: (11, {}), {3}: (12, {})} | custom-call | flops 4294967296 | bytes 1048576 | tf_op jit(solution)/shard_map/mixer/pallas_call | solution.py:328
  (2 shorter events, 0.1 us)
Async XLA Ops:
  1.5 85.8 %copy-start = (bf16[1,384,2048]{2,1,0:T(8,128)(2,1)S(1)}, bf16[1,384,2048]{2,1,0:T(8,128)(2,1)}, u32[]{:S(2)}) copy-start(bf16[1,384,2048]{2,1,0:T(8,128)(2,1)} %param.5) | copy-start | bytes 4718596
  35.3 54.0 %copy-start.1 = (f32[2,2048]{1,0:T(2,128)S(1)}, f32[2,2048]{1,0:T(2,128)}, u32[]{:S(2)}) copy-start(f32[2,2048]{1,0:T(2,128)} %norm_gain.3) | copy-start | bytes 49156
  35.3 54.0 %copy-start.2 = (f32[2,512]{1,0:T(2,128)S(1)}, f32[2,512]{1,0:T(2,128)}, u32[]{:S(2)}) copy-start(f32[2,512]{1,0:T(2,128)} %pool_gain.1) | copy-start | bytes 12292
  51.9 16.7 %collective-permute-start.1 = (bf16[4,16,64,128]{3,2,1,0:T(8,128)(2,1)S(1)}, bf16[4,16,64,128]{3,2,1,0:T(8,128)(2,1)S(1)}, u32[]{:S(2)}, u32[]{:S(2)}) collective-permute-start(bf16[4,16,64,128]{3,2,1,0:T(8,128)(2,1)S(1)} %all_to_all.11.refs_0_.refs_2_), channel_id=1, source_target_pairs={{0,128},{1,33},{2,130},{3,35},{4,132},{5,37},{6,134},{7,39},{8,136... | collective-permute-start | bytes 3145736 | tf_op jit(solution)/shard_map/ppermute | solution.py:28
  53.9 29.1 %collective-permute-start.2 = (bf16[4,16,64,128]{3,2,1,0:T(8,128)(2,1)S(1)}, bf16[4,16,64,128]{3,2,1,0:T(8,128)(2,1)S(1)}, u32[]{:S(2)}, u32[]{:S(2)}) collective-permute-start(bf16[4,16,64,128]{3,2,1,0:T(8,128)(2,1)S(1)} %all_to_all.11.refs_0_.refs_2_), channel_id=1, source_target_pairs={{0,384},{1,97},{2,386},{3,99},{4,388},{5,101},{6,390},{7,103},{8,3... | collective-permute-start | bytes 3145736 | tf_op jit(solution)/shard_map/ppermute | solution.py:28
  57.8 27.1 %collective-permute-start.3 = (bf16[4,16,64,128]{3,2,1,0:T(8,128)(2,1)S(1)}, bf16[4,16,64,128]{3,2,1,0:T(8,128)(2,1)S(1)}, u32[]{:S(2)}, u32[]{:S(2)}) collective-permute-start(bf16[4,16,64,128]{3,2,1,0:T(8,128)(2,1)S(1)} %all_to_all.11.refs_0_.refs_2_), channel_id=1, source_target_pairs={{0,256},{1,65},{2,258},{3,67},{4,260},{5,69},{6,262},{7,71},{8,264... | collective-permute-start | bytes 3145736 | tf_op jit(solution)/shard_map/ppermute | solution.py:28
  60.7 30.8 %collective-permute-start.5 = (bf16[4,16,64,128]{3,2,1,0:T(8,128)(2,1)S(1)}, bf16[4,16,64,128]{3,2,1,0:T(8,128)(2,1)S(1)}, u32[]{:S(2)}, u32[]{:S(2)}) collective-permute-start(bf16[4,16,64,128]{3,2,1,0:T(8,128)(2,1)S(1)} %all_to_all.11.refs_0_.refs_2_), channel_id=1, source_target_pairs={{0,1},{1,0},{2,3},{3,2},{4,5},{5,4},{6,7},{7,6},{8,9},{9,8},{10,11... | collective-permute-start | bytes 3145736 | tf_op jit(solution)/shard_map/ppermute | solution.py:28
  68.6 28.2 %collective-permute-start.6 = (bf16[4,16,64,128]{3,2,1,0:T(8,128)(2,1)S(1)}, bf16[4,16,64,128]{3,2,1,0:T(8,128)(2,1)S(1)}, u32[]{:S(2)}, u32[]{:S(2)}) collective-permute-start(bf16[4,16,64,128]{3,2,1,0:T(8,128)(2,1)S(1)} %collective-permute-done.1.refs_3_.refs_1_), channel_id=1, source_target_pairs={{0,1},{1,0},{2,3},{3,2},{4,5},{5,4},{6,7},{7,6},{8,9},{9,8},{10,11... | collective-permute-start | bytes 3145736 | tf_op jit(solution)/shard_map/ppermute | solution.py:28
  83.0 13.8 %collective-permute-start.7 = (bf16[4,16,64,128]{3,2,1,0:T(8,128)(2,1)S(1)}, bf16[4,16,64,128]{3,2,1,0:T(8,128)(2,1)S(1)}, u32[]{:S(2)}, u32[]{:S(2)}) collective-permute-start(bf16[4,16,64,128]{3,2,1,0:T(8,128)(2,1)S(1)} %collective-permute-done.2.refs_4_.refs_2_), channel_id=1, source_target_pairs={{0,1},{1,0},{2,3},{3,2},{4,5},{5,4},{6,7},{7,6},{8,9},{9,8},{10,11... | collective-permute-start | bytes 3145736 | tf_op jit(solution)/shard_map/ppermute | solution.py:28
  84.9 15.2 %collective-permute-start.4 = (bf16[4,16,64,128]{3,2,1,0:T(8,128)(2,1)S(1)}, bf16[4,16,64,128]{3,2,1,0:T(8,128)(2,1)S(1)}, u32[]{:S(2)}, u32[]{:S(2)}) collective-permute-start(bf16[4,16,64,128]{3,2,1,0:T(8,128)(2,1)S(1)} %collective-permute-done.3.refs_0_.refs_3_), channel_id=1, source_target_pairs={{0,1},{1,0},{2,3},{3,2},{4,5},{5,4},{6,7},{7,6},{8,9},{9,8},{10,11... | collective-permute-start | bytes 3145736 | tf_op jit(solution)/shard_map/ppermute | solution.py:28
  87.4 9.4 %collective-permute-start = (bf16[32,2048]{1,0:T(8,128)(2,1)S(1)}, bf16[32,2048]{1,0:T(8,128)(2,1)S(1)}, u32[]{:S(2)}, u32[]{:S(2)}) collective-permute-start(bf16[32,2048]{1,0:T(8,128)(2,1)S(1)} %end.1), channel_id=1, source_target_pairs={{0,32},{1,33},{2,34},{3,35},{4,36},{5,37},{6,38},{7,39},{8,40},{9,... | collective-permute-start | bytes 393224 | tf_op jit(solution)/shard_map/ppermute | solution.py:354

commit v7 on v6

--- a/solution.py
+++ b/solution.py
@@ -60,10 +60,21 @@
     return (second + PIECES[k] + 4) % 4
 
 
+def of_first(piece, f):
+    return piece[f // 2].at[f % 2] if isinstance(piece, tuple) else piece.at[f]
+
+
+def down_tile(piece, f, z):
+    if not isinstance(piece, tuple):
+        return piece[f, z, 32:64]
+    low, high = (half[f % 2, z, 32:64] for half in piece)
+    return jnp.where(f < 2, low, high)
+
+
 def part(left, rows, piece, core, s):
     lhs = jnp.concatenate([left[rows, lanes_of(core, s, f)] for f in range(4)], axis=1)
     rhs = jnp.concatenate(
-        [piece[f, :, 0:16].reshape(256, 128) for f in range(4)], axis=1
+        [of_first(piece, f)[:, 0:16].reshape(256, 128) for f in range(4)], axis=1
     )
     return lax.dot_general(
         lhs, rhs, (((1,), (1,)), ((), ())), preferred_element_type=F32
@@ -71,11 +82,8 @@
 
 
 def put_in(piece, core, s, whole_in):
-    def step(f, carry):
-        whole_in[core, :, :, lanes_of(core, s, f)] = piece[f, :, 16:32]
-        return carry
-
-    lax.fori_loop(0, 4, step, 0)
+    for f in range(4):
+        whole_in[core, :, :, lanes_of(core, s, f)] = of_first(piece, f)[:, 16:32]
 
 
 def put_down(mine, theirs, pairs, whole_down):
@@ -86,8 +94,8 @@
         at = jnp.where(c == 0, a * 4 + b, b * 4 + a)
         rows = pl.ds(pl.multiple_of(at * 16, 16), 16)
         for z in range(16):
-            m = mine[k][b, z, 32:64]
-            t = theirs[j][a, z, 32:64]
+            m = down_tile(mine[k], b, z)
+            t = down_tile(theirs[j], a, z)
             lanes = slice(z * 128, (z + 1) * 128)
             first = jnp.where(left, m, t)
             last = jnp.where(left, t, m)
@@ -115,20 +123,18 @@
     return jnp.broadcast_to(block[None], (16, 64, 128))
 
 
-def end_kernel(tokens, end):
-    end[...] = tokens[tokens.shape[0] - HALO :]
-
-
-def end_of(tokens):
+def cut(array, low, high):
+    def kernel(array, out):
+        out[...] = array[low:high]
+
     return pl.pallas_call(
-        end_kernel,
-        out_shape=jax.ShapeDtypeStruct((HALO, tokens.shape[1]), BF16),
+        kernel,
+        out_shape=jax.ShapeDtypeStruct((high - low, *array.shape[1:]), BF16),
         in_specs=[VMEM],
         out_specs=VMEM,
         compiler_params=params(3),
         cost_estimate=cost(1 << 20),
-        name="end",
-    )(tokens)
+    )(array)
 
 
 def norm_rows(block, gain):
@@ -229,7 +235,7 @@
 
 
 def place_c(inputs, normed, total, whole_in, whole_down):
-    mine, theirs = (None, None, None, inputs[0]), inputs[1:]
+    mine, theirs = (None, None, None, tuple(inputs[:2])), inputs[2:]
     c, s_mine, _ = seconds()
     s = along(s_mine, 3)
     total[0] += part(normed, slice(None), mine[3], c, s)
@@ -238,7 +244,8 @@
 
 
 def mixer_kernel(tokens, halo, norm_gain, pool_gain, *refs):
-    mine, theirs, left = refs[:4], (None, None, None, refs[4]), refs[5]
+    mine = (*refs[:3], tuple(refs[3:5]))
+    theirs, left = (None, None, None, tuple(refs[5:7])), refs[7]
     out, total, whole_in, whole_down = refs[-10:-6]
     extended, pooled, middle, scaled, last, sems = refs[-6:]
     c, _, s_theirs = seconds()
@@ -350,7 +357,8 @@
 
 
 def mixed(tokens, norm_gain, in_weight, down_weight, pool_gain):
-    end = end_of(tokens[0])
+    rows = tokens.shape[1]
+    end = cut(tokens[0], rows - HALO, rows)
     halo = lax.ppermute(end, AXES, [(i, i + 32) for i in range(480)])
     normed, pool_gain = head(tokens[0], norm_gain, pool_gain)
     column = shared(packed(in_weight, down_weight), lambda y, x, z, c: (y, x, c))
@@ -358,8 +366,11 @@
         jnp.broadcast_to(column[None], (4, 16, 64, 128)),
         lambda y, x, z, c: (y, z, c) if c == 0 else (x, z, c),
     )
-    names = (1, -1, 2)
-    mine = [line] + [send(line, second_hop(d)) for d in names]
+    up = send(line, second_hop(1))
+    down = send(line, second_hop(-1))
+    up_on = send(cut(up, 0, 2), second_hop(1))
+    down_on = send(cut(down, 2, 4), second_hop(-1))
+    mine = [line, up, down, up_on, down_on]
     theirs = [send(piece, other_core) for piece in mine]
     state = placed(place_a, 10, mine[:1] + theirs[:1], (normed,))
     inputs = [halo, norm_gain, *mine[:3], *theirs[:3]]

time: 106 us -> 108 us (1.019)
  starting transfers between devices: 18.8 us -> 24.1 us
  Pallas kernels: 12.2 us -> 10.7 us
  waiting for transfers between devices: 22.6 us -> 21.4 us
    ppermute x7 -> x9, starting transfers between devices: 16.9 us -> 22.2 us  [send(): return lax.ppermute(block, AXES, route)]
    ppermute x7 -> x9, waiting for transfers between devices: 18.4 us -> 16.2 us  [send(): return lax.ppermute(block, AXES, route)]
    pallas_call x3, Pallas kernels: 4.36 us -> 2.76 us  [placed(): pl.pallas_call(kernel, out_shape=(jax.ShapeDtypeStruct((rows, 2048), BF16...]
  transfers between devices with their start and end apart: 8 -> 10, of which waited for: 3 -> 5; matrix products, arithmetic and copies ran while one was open for 0% -> 0% of each run, Pallas kernels for 6% -> 5%
where the time goes in v7:
time: 108 us
  blocking collectives  49.7 us (46%)
  starting transfers between devices  24.1 us (22%)
  waiting for transfers between devices  21.4 us (20%)
  Pallas kernels  10.7 us (10%)
  other arithmetic  1.49 us (1%)
    all_to_all x2, blocking collectives, shared(): lax.all_to_all(copies, AXES, 0, 0, axis_index_groups=list(groups.values()...  49.7 us
    ppermute x9, starting transfers between devices, send(): return lax.ppermute(block, AXES, route)  22.2 us
    ppermute x9, waiting for transfers between devices, send(): return lax.ppermute(block, AXES, route)  16.2 us
    pallas_call x1, Pallas kernels, mixer(): pl.pallas_call(mixer_kernel, out_shape=(jax.ShapeDtypeStruct(tokens.shape...  5.61 us
    ppermute x1, waiting for transfers between devices, mixed(): halo = lax.ppermute(end, AXES, [(i, i + 32) for i in range(480)])  5.15 us
    pallas_call x3, Pallas kernels, placed(): pl.pallas_call(kernel, out_shape=(jax.ShapeDtypeStruct((rows, 2048), BF16...  2.76 us
    pallas_call x1, Pallas kernels, head(): pl.pallas_call(head_kernel, out_shape=(jax.ShapeDtypeStruct((HALO + token...  2.25 us
  transfers between devices with their start and end apart: 10, of which 5 were waited for; matrix products, arithmetic and copies ran while one was open for 0% of the time, Pallas kernels for 5%

profile of v7, /device:TPU:24, one launch (start us, length us, event | category | flops | bytes accessed | tf_op | source)
XLA Modules:
  0.0 107.9 jit_solution(2061379717264214109)
XLA Ops:
  0.0 0.7 select_bitcast_fusion.1
  0.7 0.8 maximum_maximum_fusion
  1.5 33.4 %all_to_all.10 = bf16[16,64,128]{2,1,0:T(8,128)(2,1)S(1)} all-to-all(bf16[16,64,128]{2,1,0:T(8,128)(2,1)S(1)} %broadcast_in_dim.6), channel_id=1, replica_groups={{0,2,4,6,8,10,12,14,16,18,20,22,24,26,28,30},{1,3,5,7,9,11,13,15,17,19,..., dimensions={0} | all-to-all | bytes 524288 | tf_op jit(solution)/shard_map/all_to_all | solution.py:35
  34.9 0.2 broadcast_in_dim.7
  35.2 16.3 %all_to_all.11.refs_0_.refs_2_ = bf16[4,16,64,128]{3,2,1,0:T(8,128)(2,1)S(1)} all-to-all(bf16[4,16,64,128]{3,2,1,0:T(8,128)(2,1)S(1)} %broadcast_in_dim.7), channel_id=1, replica_groups={{0,32,64,96},{1,129,257,385},{2,34,66,98},{3,131,259,387},{4,36,68,100}..., dimensions={0} | all-to-all | bytes 2097152 | tf_op jit(solution)/shard_map/all_to_all | solution.py:35
  51.5 0.0 copy-start
  51.5 0.0 copy-start.1
  51.5 0.0 copy-start.2
  51.5 2.0 %collective-permute-start.1 = (bf16[4,16,64,128]{3,2,1,0:T(8,128)(2,1)S(1)}, bf16[4,16,64,128]{3,2,1,0:T(8,128)(2,1)S(1)}, u32[]{:S(2)}, u32[]{:S(2)}) collective-permute-start(bf16[4,16,64,128]{3,2,1,0:T(8,128)(2,1)S(1)} %all_to_all.11.refs_0_.refs_2_), channel_id=1, source_target_pairs={{0,128},{1,33},{2,130},{3,35},{4,132},{5,37},{6,134},{7,39},{8,136... | collective-permute-start | bytes 3145736 | tf_op jit(solution)/shard_map/ppermute | solution.py:28
  53.6 3.9 %collective-permute-start.2 = (bf16[4,16,64,128]{3,2,1,0:T(8,128)(2,1)S(1)}, bf16[4,16,64,128]{3,2,1,0:T(8,128)(2,1)S(1)}, u32[]{:S(2)}, u32[]{:S(2)}) collective-permute-start(bf16[4,16,64,128]{3,2,1,0:T(8,128)(2,1)S(1)} %all_to_all.11.refs_0_.refs_2_), channel_id=1, source_target_pairs={{0,384},{1,97},{2,386},{3,99},{4,388},{5,101},{6,390},{7,103},{8,3... | collective-permute-start | bytes 3145736 | tf_op jit(solution)/shard_map/ppermute | solution.py:28
  57.5 1.9 %collective-permute-start.7 = (bf16[4,16,64,128]{3,2,1,0:T(8,128)(2,1)S(1)}, bf16[4,16,64,128]{3,2,1,0:T(8,128)(2,1)S(1)}, u32[]{:S(2)}, u32[]{:S(2)}) collective-permute-start(bf16[4,16,64,128]{3,2,1,0:T(8,128)(2,1)S(1)} %all_to_all.11.refs_0_.refs_2_), channel_id=1, source_target_pairs={{0,1},{1,0},{2,3},{3,2},{4,5},{5,4},{6,7},{7,6},{8,9},{9,8},{10,11... | collective-permute-start | bytes 3145736 | tf_op jit(solution)/shard_map/ppermute | solution.py:28
  59.4 8.9 %collective-permute-done.1.array.refs_3_.refs_1_ = bf16[4,16,64,128]{3,2,1,0:T(8,128)(2,1)S(1)} collective-permute-done((bf16[4,16,64,128]{3,2,1,0:T(8,128)(2,1)S(1)}, bf16[4,16,64,128]{3,2,1,0:T(8,128)(2,1)S(1)}, u32[]{:S(2)}, u32[]{:S(2)}) %collective-permute-start.1) | collective-permute-done | bytes 1048608 | tf_op jit(solution)/shard_map/ppermute | solution.py:28
  68.3 1.9 %collective-permute-start.8 = (bf16[4,16,64,128]{3,2,1,0:T(8,128)(2,1)S(1)}, bf16[4,16,64,128]{3,2,1,0:T(8,128)(2,1)S(1)}, u32[]{:S(2)}, u32[]{:S(2)}) collective-permute-start(bf16[4,16,64,128]{3,2,1,0:T(8,128)(2,1)S(1)} %collective-permute-done.1.array.refs_3_.refs_1_), channel_id=1, source_target_pairs={{0,1},{1,0},{2,3},{3,2},{4,5},{5,4},{6,7},{7,6},{8,9},{9,8},{10,11... | collective-permute-start | bytes 3145736 | tf_op jit(solution)/shard_map/ppermute | solution.py:28
  70.3 1.2 %collective-permute-done.2.array.refs_4_.refs_2_ = bf16[4,16,64,128]{3,2,1,0:T(8,128)(2,1)S(1)} collective-permute-done((bf16[4,16,64,128]{3,2,1,0:T(8,128)(2,1)S(1)}, bf16[4,16,64,128]{3,2,1,0:T(8,128)(2,1)S(1)}, u32[]{:S(2)}, u32[]{:S(2)}) %collective-permute-start.2) | collective-permute-done | bytes 1048608 | tf_op jit(solution)/shard_map/ppermute | solution.py:28
  71.5 1.9 %collective-permute-start.9 = (bf16[4,16,64,128]{3,2,1,0:T(8,128)(2,1)S(1)}, bf16[4,16,64,128]{3,2,1,0:T(8,128)(2,1)S(1)}, u32[]{:S(2)}, u32[]{:S(2)}) collective-permute-start(bf16[4,16,64,128]{3,2,1,0:T(8,128)(2,1)S(1)} %collective-permute-done.2.array.refs_4_.refs_2_), channel_id=1, source_target_pairs={{0,1},{1,0},{2,3},{3,2},{4,5},{5,4},{6,7},{7,6},{8,9},{9,8},{10,11... | collective-permute-start | bytes 3145736 | tf_op jit(solution)/shard_map/ppermute | solution.py:28
  73.4 2.4 %collective-permute-start.3 = (bf16[2,16,64,128]{3,2,1,0:T(8,128)(2,1)S(1)}, bf16[2,16,64,128]{3,2,1,0:T(8,128)(2,1)S(1)}, u32[]{:S(2)}, u32[]{:S(2)}) collective-permute-start(bf16[2,16,64,128]{3,2,1,0:T(8,128)(2,1)S(1)} %shard_map.56), channel_id=1, source_target_pairs={{0,128},{1,33},{2,130},{3,35},{4,132},{5,37},{6,134},{7,39},{8,136... | collective-permute-start | bytes 1572872 | tf_op jit(solution)/shard_map/ppermute | solution.py:28
  75.9 3.4 %collective-permute-start.4 = (bf16[2,16,64,128]{3,2,1,0:T(8,128)(2,1)S(1)}, bf16[2,16,64,128]{3,2,1,0:T(8,128)(2,1)S(1)}, u32[]{:S(2)}, u32[]{:S(2)}) collective-permute-start(bf16[2,16,64,128]{3,2,1,0:T(8,128)(2,1)S(1)} %shard_map.57), channel_id=1, source_target_pairs={{0,384},{1,97},{2,386},{3,99},{4,388},{5,101},{6,390},{7,103},{8,3... | collective-permute-start | bytes 1572872 | tf_op jit(solution)/shard_map/ppermute | solution.py:28
  79.3 5.2 %collective-permute-done.3.refs_0_.refs_3_ = bf16[2,16,64,128]{3,2,1,0:T(8,128)(2,1)S(1)} collective-permute-done((bf16[2,16,64,128]{3,2,1,0:T(8,128)(2,1)S(1)}, bf16[2,16,64,128]{3,2,1,0:T(8,128)(2,1)S(1)}, u32[]{:S(2)}, u32[]{:S(2)}) %collective-permute-start.3) | collective-permute-done | bytes 524320 | tf_op jit(solution)/shard_map/ppermute | solution.py:28
  84.5 2.8 %collective-permute-start.5 = (bf16[2,16,64,128]{3,2,1,0:T(8,128)(2,1)S(1)}, bf16[2,16,64,128]{3,2,1,0:T(8,128)(2,1)S(1)}, u32[]{:S(2)}, u32[]{:S(2)}) collective-permute-start(bf16[2,16,64,128]{3,2,1,0:T(8,128)(2,1)S(1)} %collective-permute-done.3.refs_0_.refs_3_), channel_id=1, source_target_pairs={{0,1},{1,0},{2,3},{3,2},{4,5},{5,4},{6,7},{7,6},{8,9},{9,8},{10,11... | collective-permute-start | bytes 1572872 | tf_op jit(solution)/shard_map/ppermute | solution.py:28
  87.3 0.9 collective-permute-done.4.refs_1_.refs_4_
  88.2 1.9 %collective-permute-start.6 = (bf16[2,16,64,128]{3,2,1,0:T(8,128)(2,1)S(1)}, bf16[2,16,64,128]{3,2,1,0:T(8,128)(2,1)S(1)}, u32[]{:S(2)}, u32[]{:S(2)}) collective-permute-start(bf16[2,16,64,128]{3,2,1,0:T(8,128)(2,1)S(1)} %collective-permute-done.4.refs_1_.refs_4_), channel_id=1, source_target_pairs={{0,1},{1,0},{2,3},{3,2},{4,5},{5,4},{6,7},{7,6},{8,9},{9,8},{10,11... | collective-permute-start | bytes 1572872 | tf_op jit(solution)/shard_map/ppermute | solution.py:28
  90.1 0.0 copy-done
  90.1 0.0 collective-permute-done.7.refs_1_.refs_5_.refs_2_
  90.1 1.9 %collective-permute-start = (bf16[32,2048]{1,0:T(8,128)(2,1)S(1)}, bf16[32,2048]{1,0:T(8,128)(2,1)S(1)}, u32[]{:S(2)}, u32[]{:S(2)}) collective-permute-start(bf16[32,2048]{1,0:T(8,128)(2,1)S(1)} %shard_map.55), channel_id=1, source_target_pairs={{0,32},{1,33},{2,34},{3,35},{4,36},{5,37},{6,38},{7,39},{8,40},{9,... | collective-permute-start | bytes 393224 | tf_op jit(solution)/shard_map/ppermute | solution.py:362
  92.1 0.0 copy-done.1
  92.1 0.0 copy-done.2
  92.1 2.2 %head.1 = (bf16[416,2048]{1,0:T(8,128)(2,1)S(1)}, f32[2,512]{1,0:T(2,128)S(1)}) custom-call(bf16[384,2048]{1,0:T(8,128)(2,1)S(1)} %bitcast.10, f32[2,2048]{1,0:T(2,128)S(1)} %copy-done.1, f32[2,512]{1,0:T(2,128)S(1)} %copy-done.2), custom_call_target="tpu_custom_call" | custom-call | flops 1073741824 | bytes 1048576 | tf_op jit(solution)/shard_map/head/pallas_call | solution.py:167
  94.3 0.5 shard_map.58
  94.9 5.2 %collective-permute-done.refs_0_.halo = bf16[32,2048]{1,0:T(8,128)(2,1)S(1)} collective-permute-done((bf16[32,2048]{1,0:T(8,128)(2,1)S(1)}, bf16[32,2048]{1,0:T(8,128)(2,1)S(1)}, u32[]{:S(2)}, u32[]{:S(2)}) %collective-permute-start) | collective-permute-done | bytes 131104 | tf_op jit(solution)/shard_map/ppermute | solution.py:362
  100.0 0.0 collective-permute-done.8.refs_6_.refs_3_
  100.1 0.0 collective-permute-done.9.refs_7_.refs_4_
  100.1 1.7 %shard_map.59 = (bf16[416,2048]{1,0:T(8,128)(2,1)S(1)}, f32[2,416,256]{2,1,0:T(8,128)S(1)}, bf16[2,16,16,2048]{3,2,1,0:T(8,128)(2,1)S(1)}, bf16[2,2,256,2048]{3,2,1,0:T(8,128)(2,1)S(1)}) custom-call(bf16[32,2048]{1,0:T(8,128)(2,1)S(1)} %collective-permute-done.refs_0_.halo, ...), custom_call_target="tpu_custom_call", output_to_operand_aliasing={{0}: (8, {}), {1}: (9, {}), {2}: (10, {}), {3}: (11, {})} | custom-call | flops 536870912 | bytes 1048576 | tf_op jit(solution)/shard_map/pallas_call | solution.py:195
  101.8 0.5 shard_map.60
  102.3 0.0 collective-permute-done.5.refs_5_
  102.3 0.0 collective-permute-done.6.refs_6_
  102.3 5.6 %mixer.1 = (bf16[384,2048]{1,0:T(8,128)(2,1)}, f32[2,416,256]{2,1,0:T(8,128)S(1)}, bf16[2,16,16,2048]{3,2,1,0:T(8,128)(2,1)S(1)}, bf16[2,2,256,2048]{3,2,1,0:T(8,128)(2,1)S(1)}) custom-call(bf16[384,2048]{1,0:T(8,128)(2,1)S(1)} %bitcast.11, ...), custom_call_target="tpu_custom_call", output_to_operand_aliasing={{1}: (12, {}), {2}: (13, {}), {3}: (14, {})} | custom-call | flops 4294967296 | bytes 1048576 | tf_op jit(solution)/shard_map/mixer/pallas_call | solution.py:335
  (4 shorter events, 0.1 us)
Async XLA Ops:
  51.5 38.6 %copy-start = (bf16[1,384,2048]{2,1,0:T(8,128)(2,1)S(1)}, bf16[1,384,2048]{2,1,0:T(8,128)(2,1)}, u32[]{:S(2)}) copy-start(bf16[1,384,2048]{2,1,0:T(8,128)(2,1)} %param.5) | copy-start | bytes 4718596
  51.5 40.6 %copy-start.1 = (f32[2,2048]{1,0:T(2,128)S(1)}, f32[2,2048]{1,0:T(2,128)}, u32[]{:S(2)}) copy-start(f32[2,2048]{1,0:T(2,128)} %norm_gain.3) | copy-start | bytes 49156
  51.5 40.6 %copy-start.2 = (f32[2,512]{1,0:T(2,128)S(1)}, f32[2,512]{1,0:T(2,128)}, u32[]{:S(2)}) copy-start(f32[2,512]{1,0:T(2,128)} %pool_gain.1) | copy-start | bytes 12292
  51.5 16.8 %collective-permute-start.1 = (bf16[4,16,64,128]{3,2,1,0:T(8,128)(2,1)S(1)}, bf16[4,16,64,128]{3,2,1,0:T(8,128)(2,1)S(1)}, u32[]{:S(2)}, u32[]{:S(2)}) collective-permute-start(bf16[4,16,64,128]{3,2,1,0:T(8,128)(2,1)S(1)} %all_to_all.11.refs_0_.refs_2_), channel_id=1, source_target_pairs={{0,128},{1,33},{2,130},{3,35},{4,132},{5,37},{6,134},{7,39},{8,136... | collective-permute-start | bytes 3145736 | tf_op jit(solution)/shard_map/ppermute | solution.py:28
  53.6 17.9 %collective-permute-start.2 = (bf16[4,16,64,128]{3,2,1,0:T(8,128)(2,1)S(1)}, bf16[4,16,64,128]{3,2,1,0:T(8,128)(2,1)S(1)}, u32[]{:S(2)}, u32[]{:S(2)}) collective-permute-start(bf16[4,16,64,128]{3,2,1,0:T(8,128)(2,1)S(1)} %all_to_all.11.refs_0_.refs_2_), channel_id=1, source_target_pairs={{0,384},{1,97},{2,386},{3,99},{4,388},{5,101},{6,390},{7,103},{8,3... | collective-permute-start | bytes 3145736 | tf_op jit(solution)/shard_map/ppermute | solution.py:28
  57.5 32.6 %collective-permute-start.7 = (bf16[4,16,64,128]{3,2,1,0:T(8,128)(2,1)S(1)}, bf16[4,16,64,128]{3,2,1,0:T(8,128)(2,1)S(1)}, u32[]{:S(2)}, u32[]{:S(2)}) collective-permute-start(bf16[4,16,64,128]{3,2,1,0:T(8,128)(2,1)S(1)} %all_to_all.11.refs_0_.refs_2_), channel_id=1, source_target_pairs={{0,1},{1,0},{2,3},{3,2},{4,5},{5,4},{6,7},{7,6},{8,9},{9,8},{10,11... | collective-permute-start | bytes 3145736 | tf_op jit(solution)/shard_map/ppermute | solution.py:28
  68.3 31.7 %collective-permute-start.8 = (bf16[4,16,64,128]{3,2,1,0:T(8,128)(2,1)S(1)}, bf16[4,16,64,128]{3,2,1,0:T(8,128)(2,1)S(1)}, u32[]{:S(2)}, u32[]{:S(2)}) collective-permute-start(bf16[4,16,64,128]{3,2,1,0:T(8,128)(2,1)S(1)} %collective-permute-done.1.array.refs_3_.refs_1_), channel_id=1, source_target_pairs={{0,1},{1,0},{2,3},{3,2},{4,5},{5,4},{6,7},{7,6},{8,9},{9,8},{10,11... | collective-permute-start | bytes 3145736 | tf_op jit(solution)/shard_map/ppermute | solution.py:28
  71.5 28.6 %collective-permute-start.9 = (bf16[4,16,64,128]{3,2,1,0:T(8,128)(2,1)S(1)}, bf16[4,16,64,128]{3,2,1,0:T(8,128)(2,1)S(1)}, u32[]{:S(2)}, u32[]{:S(2)}) collective-permute-start(bf16[4,16,64,128]{3,2,1,0:T(8,128)(2,1)S(1)} %collective-permute-done.2.array.refs_4_.refs_2_), channel_id=1, source_target_pairs={{0,1},{1,0},{2,3},{3,2},{4,5},{5,4},{6,7},{7,6},{8,9},{9,8},{10,11... | collective-permute-start | bytes 3145736 | tf_op jit(solution)/shard_map/ppermute | solution.py:28
  73.4 11.1 %collective-permute-start.3 = (bf16[2,16,64,128]{3,2,1,0:T(8,128)(2,1)S(1)}, bf16[2,16,64,128]{3,2,1,0:T(8,128)(2,1)S(1)}, u32[]{:S(2)}, u32[]{:S(2)}) collective-permute-start(bf16[2,16,64,128]{3,2,1,0:T(8,128)(2,1)S(1)} %shard_map.56), channel_id=1, source_target_pairs={{0,128},{1,33},{2,130},{3,35},{4,132},{5,37},{6,134},{7,39},{8,136... | collective-permute-start | bytes 1572872 | tf_op jit(solution)/shard_map/ppermute | solution.py:28
  75.9 12.3 %collective-permute-start.4 = (bf16[2,16,64,128]{3,2,1,0:T(8,128)(2,1)S(1)}, bf16[2,16,64,128]{3,2,1,0:T(8,128)(2,1)S(1)}, u32[]{:S(2)}, u32[]{:S(2)}) collective-permute-start(bf16[2,16,64,128]{3,2,1,0:T(8,128)(2,1)S(1)} %shard_map.57), channel_id=1, source_target_pairs={{0,384},{1,97},{2,386},{3,99},{4,388},{5,101},{6,390},{7,103},{8,3... | collective-permute-start | bytes 1572872 | tf_op jit(solution)/shard_map/ppermute | solution.py:28
  84.5 17.8 %collective-permute-start.5 = (bf16[2,16,64,128]{3,2,1,0:T(8,128)(2,1)S(1)}, bf16[2,16,64,128]{3,2,1,0:T(8,128)(2,1)S(1)}, u32[]{:S(2)}, u32[]{:S(2)}) collective-permute-start(bf16[2,16,64,128]{3,2,1,0:T(8,128)(2,1)S(1)} %collective-permute-done.3.refs_0_.refs_3_), channel_id=1, source_target_pairs={{0,1},{1,0},{2,3},{3,2},{4,5},{5,4},{6,7},{7,6},{8,9},{9,8},{10,11... | collective-permute-start | bytes 1572872 | tf_op jit(solution)/shard_map/ppermute | solution.py:28
  88.2 14.1 %collective-permute-start.6 = (bf16[2,16,64,128]{3,2,1,0:T(8,128)(2,1)S(1)}, bf16[2,16,64,128]{3,2,1,0:T(8,128)(2,1)S(1)}, u32[]{:S(2)}, u32[]{:S(2)}) collective-permute-start(bf16[2,16,64,128]{3,2,1,0:T(8,128)(2,1)S(1)} %collective-permute-done.4.refs_1_.refs_4_), channel_id=1, source_target_pairs={{0,1},{1,0},{2,3},{3,2},{4,5},{5,4},{6,7},{7,6},{8,9},{9,8},{10,11... | collective-permute-start | bytes 1572872 | tf_op jit(solution)/shard_map/ppermute | solution.py:28
  90.1 9.9 %collective-permute-start = (bf16[32,2048]{1,0:T(8,128)(2,1)S(1)}, bf16[32,2048]{1,0:T(8,128)(2,1)S(1)}, u32[]{:S(2)}, u32[]{:S(2)}) collective-permute-start(bf16[32,2048]{1,0:T(8,128)(2,1)S(1)} %shard_map.55), channel_id=1, source_target_pairs={{0,32},{1,33},{2,34},{3,35},{4,36},{5,37},{6,38},{7,39},{8,40},{9,... | collective-permute-start | bytes 393224 | tf_op jit(solution)/shard_map/ppermute | solution.py:362

commit v8 on v7

--- a/solution.py
+++ b/solution.py
@@ -219,19 +219,33 @@
 
 
 def place_b(inputs, normed, total, whole_in, whole_down):
+    mine, theirs = inputs[:2], inputs[2:]
+    c, s_mine, s_theirs = seconds()
+    for slot, piece, core, second in (
+        (0, mine[1], c, s_mine),
+        (1, theirs[1], 1 - c, s_theirs),
+    ):
+        s = along(second, 1)
+        rows = slice(HALO, None)
+        total[slot, rows] += part(normed, rows, piece, core, s)
+        put_in(piece, core, s, whole_in)
+    put_down(mine, theirs, ((0, 1), (1, 0), (1, 1)), whole_down)
+
+
+def place_d(inputs, normed, total, whole_in, whole_down):
     halo, norm_gain, *pieces = inputs
     mine, theirs = pieces[:3], pieces[3:]
     normed[:HALO] = norm_rows(halo[...], norm_gain[0:1])
     c, s_mine, s_theirs = seconds()
     for slot, of, core, second in ((0, mine, c, s_mine), (1, theirs, 1 - c, s_theirs)):
         rows = slice(0, HALO)
-        total[slot, rows] = part(normed, rows, of[0], core, along(second, 0))
-        for k in (1, 2):
-            s = along(second, k)
-            total[slot] += part(normed, slice(None), of[k], core, s)
-            put_in(of[k], core, s, whole_in)
-    pairs = [(k, j) for k in range(3) for j in range(3) if k + j > 0]
-    put_down(mine, theirs, pairs, whole_down)
+        total[slot, rows] = part(normed, rows, of[0], core, along(second, 0)) + part(
+            normed, rows, of[1], core, along(second, 1)
+        )
+        s = along(second, 2)
+        total[slot] += part(normed, slice(None), of[2], core, s)
+        put_in(of[2], core, s, whole_in)
+    put_down(mine, theirs, ((0, 2), (1, 2), (2, 0), (2, 1), (2, 2)), whole_down)
 
 
 def place_c(inputs, normed, total, whole_in, whole_down):
@@ -261,7 +275,7 @@
     width = jnp.where(
         lane < 64, jnp.where(lane < 32, 2.0, 4.0), jnp.where(lane < 96, 8.0, 16.0)
     )
-    count = jnp.minimum(position, width)
+    share = 1.0 / jnp.minimum(position, width)
 
     def rounded(block):
         return block.astype(BF16).astype(F32)
@@ -279,7 +293,7 @@
                 jnp.where(lane < 32, two[PAD:], four[PAD:]),
                 jnp.where(lane < 96, eight[PAD:], sixteen[PAD:]),
             )
-            trailing = sums / count - own[PAD:]
+            trailing = sums * share - own[PAD:]
             pooled[:, lanes] = (trailing * pool_gain[l : l + 1, lanes]).astype(BF16)
 
     extended[PAD:, pl.ds(pl.multiple_of(c * 256, 256), 256)] = rounded(total[0])
@@ -374,7 +388,8 @@
     theirs = [send(piece, other_core) for piece in mine]
     state = placed(place_a, 10, mine[:1] + theirs[:1], (normed,))
     inputs = [halo, norm_gain, *mine[:3], *theirs[:3]]
-    state = placed(place_b, 10, inputs, state)
+    state = placed(place_b, 10, mine[:2] + theirs[:2], state)
+    state = placed(place_d, 10, inputs, state)
     state = placed(place_c, 10, mine[3:] + theirs[:3], state)
     pieces = mine + theirs[3:]
     return mixer(tokens[0], halo, norm_gain, pool_gain, pieces, state)[None]

time: 108 us -> 108 us (level)
    pallas_call x3 -> x4, Pallas kernels: 2.76 us -> 2.76 us  [placed(): pl.pallas_call(kernel, out_shape=(jax.ShapeDtypeStruct((rows, 2048), BF16...]
where the time goes in v8:
time: 108 us; the launch traced here: 107 us
  blocking collectives  49.7 us (46%)
  starting transfers between devices  24.1 us (22%)
  waiting for transfers between devices  20.7 us (19%)
  Pallas kernels  10.7 us (10%)
  other arithmetic  1.49 us (1%)
    all_to_all x2, blocking collectives, shared(): lax.all_to_all(copies, AXES, 0, 0, axis_index_groups=list(groups.values()...  49.7 us
    ppermute x9, starting transfers between devices, send(): return lax.ppermute(block, AXES, route)  22.2 us
    ppermute x9, waiting for transfers between devices, send(): return lax.ppermute(block, AXES, route)  16.2 us
    pallas_call x1, Pallas kernels, mixer(): pl.pallas_call(mixer_kernel, out_shape=(jax.ShapeDtypeStruct(tokens.shape...  5.65 us
    ppermute x1, waiting for transfers between devices, mixed(): halo = lax.ppermute(end, AXES, [(i, i + 32) for i in range(480)])  4.49 us
    pallas_call x4, Pallas kernels, placed(): pl.pallas_call(kernel, out_shape=(jax.ShapeDtypeStruct((rows, 2048), BF16...  2.76 us
    pallas_call x1, Pallas kernels, head(): pl.pallas_call(head_kernel, out_shape=(jax.ShapeDtypeStruct((HALO + token...  2.25 us
  transfers between devices with their start and end apart: 10, of which 5 were waited for; matrix products, arithmetic and copies ran while one was open for 0% of the time, Pallas kernels for 5%

profile of v8, /device:TPU:24, one launch (start us, length us, event | category | flops | bytes accessed | tf_op | source)
XLA Modules:
  0.0 107.3 jit_solution(4520189030033010905)
XLA Ops:
  0.0 0.7 select_bitcast_fusion.1
  0.7 0.8 maximum_maximum_fusion
  1.5 33.4 %all_to_all.10 = bf16[16,64,128]{2,1,0:T(8,128)(2,1)S(1)} all-to-all(bf16[16,64,128]{2,1,0:T(8,128)(2,1)S(1)} %broadcast_in_dim.6), channel_id=1, replica_groups={{0,2,4,6,8,10,12,14,16,18,20,22,24,26,28,30},{1,3,5,7,9,11,13,15,17,19,..., dimensions={0} | all-to-all | bytes 524288 | tf_op jit(solution)/shard_map/all_to_all | solution.py:35
  34.9 0.2 broadcast_in_dim.7
  35.2 16.3 %all_to_all.11.refs_0_.refs_2_ = bf16[4,16,64,128]{3,2,1,0:T(8,128)(2,1)S(1)} all-to-all(bf16[4,16,64,128]{3,2,1,0:T(8,128)(2,1)S(1)} %broadcast_in_dim.7), channel_id=1, replica_groups={{0,32,64,96},{1,129,257,385},{2,34,66,98},{3,131,259,387},{4,36,68,100}..., dimensions={0} | all-to-all | bytes 2097152 | tf_op jit(solution)/shard_map/all_to_all | solution.py:35
  51.5 0.0 copy-start
  51.5 0.0 copy-start.1
  51.5 0.0 copy-start.2
  51.5 2.0 %collective-permute-start.1 = (bf16[4,16,64,128]{3,2,1,0:T(8,128)(2,1)S(1)}, bf16[4,16,64,128]{3,2,1,0:T(8,128)(2,1)S(1)}, u32[]{:S(2)}, u32[]{:S(2)}) collective-permute-start(bf16[4,16,64,128]{3,2,1,0:T(8,128)(2,1)S(1)} %all_to_all.11.refs_0_.refs_2_), channel_id=1, source_target_pairs={{0,128},{1,33},{2,130},{3,35},{4,132},{5,37},{6,134},{7,39},{8,136... | collective-permute-start | bytes 3145736 | tf_op jit(solution)/shard_map/ppermute | solution.py:28
  53.6 3.9 %collective-permute-start.2 = (bf16[4,16,64,128]{3,2,1,0:T(8,128)(2,1)S(1)}, bf16[4,16,64,128]{3,2,1,0:T(8,128)(2,1)S(1)}, u32[]{:S(2)}, u32[]{:S(2)}) collective-permute-start(bf16[4,16,64,128]{3,2,1,0:T(8,128)(2,1)S(1)} %all_to_all.11.refs_0_.refs_2_), channel_id=1, source_target_pairs={{0,384},{1,97},{2,386},{3,99},{4,388},{5,101},{6,390},{7,103},{8,3... | collective-permute-start | bytes 3145736 | tf_op jit(solution)/shard_map/ppermute | solution.py:28
  57.5 1.9 %collective-permute-start.7 = (bf16[4,16,64,128]{3,2,1,0:T(8,128)(2,1)S(1)}, bf16[4,16,64,128]{3,2,1,0:T(8,128)(2,1)S(1)}, u32[]{:S(2)}, u32[]{:S(2)}) collective-permute-start(bf16[4,16,64,128]{3,2,1,0:T(8,128)(2,1)S(1)} %all_to_all.11.refs_0_.refs_2_), channel_id=1, source_target_pairs={{0,1},{1,0},{2,3},{3,2},{4,5},{5,4},{6,7},{7,6},{8,9},{9,8},{10,11... | collective-permute-start | bytes 3145736 | tf_op jit(solution)/shard_map/ppermute | solution.py:28
  59.4 8.9 %collective-permute-done.1.array.refs_1_.refs_3_ = bf16[4,16,64,128]{3,2,1,0:T(8,128)(2,1)S(1)} collective-permute-done((bf16[4,16,64,128]{3,2,1,0:T(8,128)(2,1)S(1)}, bf16[4,16,64,128]{3,2,1,0:T(8,128)(2,1)S(1)}, u32[]{:S(2)}, u32[]{:S(2)}) %collective-permute-start.1) | collective-permute-done | bytes 1048608 | tf_op jit(solution)/shard_map/ppermute | solution.py:28
  68.3 1.9 %collective-permute-start.8 = (bf16[4,16,64,128]{3,2,1,0:T(8,128)(2,1)S(1)}, bf16[4,16,64,128]{3,2,1,0:T(8,128)(2,1)S(1)}, u32[]{:S(2)}, u32[]{:S(2)}) collective-permute-start(bf16[4,16,64,128]{3,2,1,0:T(8,128)(2,1)S(1)} %collective-permute-done.1.array.refs_1_.refs_3_), channel_id=1, source_target_pairs={{0,1},{1,0},{2,3},{3,2},{4,5},{5,4},{6,7},{7,6},{8,9},{9,8},{10,11... | collective-permute-start | bytes 3145736 | tf_op jit(solution)/shard_map/ppermute | solution.py:28
  70.3 1.2 %collective-permute-done.2.array.refs_4_.refs_2_ = bf16[4,16,64,128]{3,2,1,0:T(8,128)(2,1)S(1)} collective-permute-done((bf16[4,16,64,128]{3,2,1,0:T(8,128)(2,1)S(1)}, bf16[4,16,64,128]{3,2,1,0:T(8,128)(2,1)S(1)}, u32[]{:S(2)}, u32[]{:S(2)}) %collective-permute-start.2) | collective-permute-done | bytes 1048608 | tf_op jit(solution)/shard_map/ppermute | solution.py:28
  71.5 1.9 %collective-permute-start.9 = (bf16[4,16,64,128]{3,2,1,0:T(8,128)(2,1)S(1)}, bf16[4,16,64,128]{3,2,1,0:T(8,128)(2,1)S(1)}, u32[]{:S(2)}, u32[]{:S(2)}) collective-permute-start(bf16[4,16,64,128]{3,2,1,0:T(8,128)(2,1)S(1)} %collective-permute-done.2.array.refs_4_.refs_2_), channel_id=1, source_target_pairs={{0,1},{1,0},{2,3},{3,2},{4,5},{5,4},{6,7},{7,6},{8,9},{9,8},{10,11... | collective-permute-start | bytes 3145736 | tf_op jit(solution)/shard_map/ppermute | solution.py:28
  73.4 2.4 %collective-permute-start.3 = (bf16[2,16,64,128]{3,2,1,0:T(8,128)(2,1)S(1)}, bf16[2,16,64,128]{3,2,1,0:T(8,128)(2,1)S(1)}, u32[]{:S(2)}, u32[]{:S(2)}) collective-permute-start(bf16[2,16,64,128]{3,2,1,0:T(8,128)(2,1)S(1)} %shard_map.56), channel_id=1, source_target_pairs={{0,128},{1,33},{2,130},{3,35},{4,132},{5,37},{6,134},{7,39},{8,136... | collective-permute-start | bytes 1572872 | tf_op jit(solution)/shard_map/ppermute | solution.py:28
  75.9 3.4 %collective-permute-start.4 = (bf16[2,16,64,128]{3,2,1,0:T(8,128)(2,1)S(1)}, bf16[2,16,64,128]{3,2,1,0:T(8,128)(2,1)S(1)}, u32[]{:S(2)}, u32[]{:S(2)}) collective-permute-start(bf16[2,16,64,128]{3,2,1,0:T(8,128)(2,1)S(1)} %shard_map.57), channel_id=1, source_target_pairs={{0,384},{1,97},{2,386},{3,99},{4,388},{5,101},{6,390},{7,103},{8,3... | collective-permute-start | bytes 1572872 | tf_op jit(solution)/shard_map/ppermute | solution.py:28
  79.3 5.2 %collective-permute-done.3.refs_0_.refs_3_ = bf16[2,16,64,128]{3,2,1,0:T(8,128)(2,1)S(1)} collective-permute-done((bf16[2,16,64,128]{3,2,1,0:T(8,128)(2,1)S(1)}, bf16[2,16,64,128]{3,2,1,0:T(8,128)(2,1)S(1)}, u32[]{:S(2)}, u32[]{:S(2)}) %collective-permute-start.3) | collective-permute-done | bytes 524320 | tf_op jit(solution)/shard_map/ppermute | solution.py:28
  84.5 2.8 %collective-permute-start.5 = (bf16[2,16,64,128]{3,2,1,0:T(8,128)(2,1)S(1)}, bf16[2,16,64,128]{3,2,1,0:T(8,128)(2,1)S(1)}, u32[]{:S(2)}, u32[]{:S(2)}) collective-permute-start(bf16[2,16,64,128]{3,2,1,0:T(8,128)(2,1)S(1)} %collective-permute-done.3.refs_0_.refs_3_), channel_id=1, source_target_pairs={{0,1},{1,0},{2,3},{3,2},{4,5},{5,4},{6,7},{7,6},{8,9},{9,8},{10,11... | collective-permute-start | bytes 1572872 | tf_op jit(solution)/shard_map/ppermute | solution.py:28
  87.3 0.9 collective-permute-done.4.refs_1_.refs_4_
  88.2 1.9 %collective-permute-start.6 = (bf16[2,16,64,128]{3,2,1,0:T(8,128)(2,1)S(1)}, bf16[2,16,64,128]{3,2,1,0:T(8,128)(2,1)S(1)}, u32[]{:S(2)}, u32[]{:S(2)}) collective-permute-start(bf16[2,16,64,128]{3,2,1,0:T(8,128)(2,1)S(1)} %collective-permute-done.4.refs_1_.refs_4_), channel_id=1, source_target_pairs={{0,1},{1,0},{2,3},{3,2},{4,5},{5,4},{6,7},{7,6},{8,9},{9,8},{10,11... | collective-permute-start | bytes 1572872 | tf_op jit(solution)/shard_map/ppermute | solution.py:28
  90.1 0.0 copy-done
  90.1 0.0 collective-permute-done.7.refs_1_.refs_2_.refs_5_
  90.1 1.9 %collective-permute-start = (bf16[32,2048]{1,0:T(8,128)(2,1)S(1)}, bf16[32,2048]{1,0:T(8,128)(2,1)S(1)}, u32[]{:S(2)}, u32[]{:S(2)}) collective-permute-start(bf16[32,2048]{1,0:T(8,128)(2,1)S(1)} %shard_map.55), channel_id=1, source_target_pairs={{0,32},{1,33},{2,34},{3,35},{4,36},{5,37},{6,38},{7,39},{8,40},{9,... | collective-permute-start | bytes 393224 | tf_op jit(solution)/shard_map/ppermute | solution.py:376
  92.1 0.0 copy-done.1
  92.1 0.0 copy-done.2
  92.1 2.2 %head.1 = (bf16[416,2048]{1,0:T(8,128)(2,1)S(1)}, f32[2,512]{1,0:T(2,128)S(1)}) custom-call(bf16[384,2048]{1,0:T(8,128)(2,1)S(1)} %bitcast.10, f32[2,2048]{1,0:T(2,128)S(1)} %copy-done.1, f32[2,512]{1,0:T(2,128)S(1)} %copy-done.2), custom_call_target="tpu_custom_call" | custom-call | flops 1073741824 | bytes 1048576 | tf_op jit(solution)/shard_map/head/pallas_call | solution.py:167
  94.3 0.5 shard_map.58
  94.9 0.0 collective-permute-done.8.refs_3_.refs_6_
  94.9 0.7 shard_map.59
  95.6 4.5 %collective-permute-done.refs_0_.halo = bf16[32,2048]{1,0:T(8,128)(2,1)S(1)} collective-permute-done((bf16[32,2048]{1,0:T(8,128)(2,1)S(1)}, bf16[32,2048]{1,0:T(8,128)(2,1)S(1)}, u32[]{:S(2)}, u32[]{:S(2)}) %collective-permute-start) | collective-permute-done | bytes 131104 | tf_op jit(solution)/shard_map/ppermute | solution.py:376
  100.0 0.0 collective-permute-done.9.refs_7_.refs_4_
  100.1 1.1 %shard_map.60 = (bf16[416,2048]{1,0:T(8,128)(2,1)S(1)}, f32[2,416,256]{2,1,0:T(8,128)S(1)}, bf16[2,16,16,2048]{3,2,1,0:T(8,128)(2,1)S(1)}, bf16[2,2,256,2048]{3,2,1,0:T(8,128)(2,1)S(1)}) custom-call(bf16[32,2048]{1,0:T(8,128)(2,1)S(1)} %collective-permute-done.refs_0_.halo, ...), custom_call_target="tpu_custom_call", output_to_operand_aliasing={{0}: (8, {}), {1}: (9, {}), {2}: (10, {}), {3}: (11, {})} | custom-call | flops 536870912 | bytes 1048576 | tf_op jit(solution)/shard_map/pallas_call | solution.py:195
  101.2 0.5 shard_map.61
  101.6 0.0 collective-permute-done.5.refs_5_
  101.7 0.0 collective-permute-done.6.refs_6_
  101.7 5.7 %mixer.1 = (bf16[384,2048]{1,0:T(8,128)(2,1)}, f32[2,416,256]{2,1,0:T(8,128)S(1)}, bf16[2,16,16,2048]{3,2,1,0:T(8,128)(2,1)S(1)}, bf16[2,2,256,2048]{3,2,1,0:T(8,128)(2,1)S(1)}) custom-call(bf16[384,2048]{1,0:T(8,128)(2,1)S(1)} %bitcast.11, ...), custom_call_target="tpu_custom_call", output_to_operand_aliasing={{1}: (12, {}), {2}: (13, {}), {3}: (14, {})} | custom-call | flops 4294967296 | bytes 1048576 | tf_op jit(solution)/shard_map/mixer/pallas_call | solution.py:349
  (4 shorter events, 0.1 us)
Async XLA Ops:
  51.5 38.6 %copy-start = (bf16[1,384,2048]{2,1,0:T(8,128)(2,1)S(1)}, bf16[1,384,2048]{2,1,0:T(8,128)(2,1)}, u32[]{:S(2)}) copy-start(bf16[1,384,2048]{2,1,0:T(8,128)(2,1)} %param.5) | copy-start | bytes 4718596
  51.5 40.6 %copy-start.1 = (f32[2,2048]{1,0:T(2,128)S(1)}, f32[2,2048]{1,0:T(2,128)}, u32[]{:S(2)}) copy-start(f32[2,2048]{1,0:T(2,128)} %norm_gain.3) | copy-start | bytes 49156
  51.5 40.6 %copy-start.2 = (f32[2,512]{1,0:T(2,128)S(1)}, f32[2,512]{1,0:T(2,128)}, u32[]{:S(2)}) copy-start(f32[2,512]{1,0:T(2,128)} %pool_gain.1) | copy-start | bytes 12292
  51.5 16.8 %collective-permute-start.1 = (bf16[4,16,64,128]{3,2,1,0:T(8,128)(2,1)S(1)}, bf16[4,16,64,128]{3,2,1,0:T(8,128)(2,1)S(1)}, u32[]{:S(2)}, u32[]{:S(2)}) collective-permute-start(bf16[4,16,64,128]{3,2,1,0:T(8,128)(2,1)S(1)} %all_to_all.11.refs_0_.refs_2_), channel_id=1, source_target_pairs={{0,128},{1,33},{2,130},{3,35},{4,132},{5,37},{6,134},{7,39},{8,136... | collective-permute-start | bytes 3145736 | tf_op jit(solution)/shard_map/ppermute | solution.py:28
  53.6 17.9 %collective-permute-start.2 = (bf16[4,16,64,128]{3,2,1,0:T(8,128)(2,1)S(1)}, bf16[4,16,64,128]{3,2,1,0:T(8,128)(2,1)S(1)}, u32[]{:S(2)}, u32[]{:S(2)}) collective-permute-start(bf16[4,16,64,128]{3,2,1,0:T(8,128)(2,1)S(1)} %all_to_all.11.refs_0_.refs_2_), channel_id=1, source_target_pairs={{0,384},{1,97},{2,386},{3,99},{4,388},{5,101},{6,390},{7,103},{8,3... | collective-permute-start | bytes 3145736 | tf_op jit(solution)/shard_map/ppermute | solution.py:28
  57.5 32.6 %collective-permute-start.7 = (bf16[4,16,64,128]{3,2,1,0:T(8,128)(2,1)S(1)}, bf16[4,16,64,128]{3,2,1,0:T(8,128)(2,1)S(1)}, u32[]{:S(2)}, u32[]{:S(2)}) collective-permute-start(bf16[4,16,64,128]{3,2,1,0:T(8,128)(2,1)S(1)} %all_to_all.11.refs_0_.refs_2_), channel_id=1, source_target_pairs={{0,1},{1,0},{2,3},{3,2},{4,5},{5,4},{6,7},{7,6},{8,9},{9,8},{10,11... | collective-permute-start | bytes 3145736 | tf_op jit(solution)/shard_map/ppermute | solution.py:28
  68.3 26.6 %collective-permute-start.8 = (bf16[4,16,64,128]{3,2,1,0:T(8,128)(2,1)S(1)}, bf16[4,16,64,128]{3,2,1,0:T(8,128)(2,1)S(1)}, u32[]{:S(2)}, u32[]{:S(2)}) collective-permute-start(bf16[4,16,64,128]{3,2,1,0:T(8,128)(2,1)S(1)} %collective-permute-done.1.array.refs_1_.refs_3_), channel_id=1, source_target_pairs={{0,1},{1,0},{2,3},{3,2},{4,5},{5,4},{6,7},{7,6},{8,9},{9,8},{10,11... | collective-permute-start | bytes 3145736 | tf_op jit(solution)/shard_map/ppermute | solution.py:28
  71.5 28.6 %collective-permute-start.9 = (bf16[4,16,64,128]{3,2,1,0:T(8,128)(2,1)S(1)}, bf16[4,16,64,128]{3,2,1,0:T(8,128)(2,1)S(1)}, u32[]{:S(2)}, u32[]{:S(2)}) collective-permute-start(bf16[4,16,64,128]{3,2,1,0:T(8,128)(2,1)S(1)} %collective-permute-done.2.array.refs_4_.refs_2_), channel_id=1, source_target_pairs={{0,1},{1,0},{2,3},{3,2},{4,5},{5,4},{6,7},{7,6},{8,9},{9,8},{10,11... | collective-permute-start | bytes 3145736 | tf_op jit(solution)/shard_map/ppermute | solution.py:28
  73.4 11.1 %collective-permute-start.3 = (bf16[2,16,64,128]{3,2,1,0:T(8,128)(2,1)S(1)}, bf16[2,16,64,128]{3,2,1,0:T(8,128)(2,1)S(1)}, u32[]{:S(2)}, u32[]{:S(2)}) collective-permute-start(bf16[2,16,64,128]{3,2,1,0:T(8,128)(2,1)S(1)} %shard_map.56), channel_id=1, source_target_pairs={{0,128},{1,33},{2,130},{3,35},{4,132},{5,37},{6,134},{7,39},{8,136... | collective-permute-start | bytes 1572872 | tf_op jit(solution)/shard_map/ppermute | solution.py:28
  75.9 12.3 %collective-permute-start.4 = (bf16[2,16,64,128]{3,2,1,0:T(8,128)(2,1)S(1)}, bf16[2,16,64,128]{3,2,1,0:T(8,128)(2,1)S(1)}, u32[]{:S(2)}, u32[]{:S(2)}) collective-permute-start(bf16[2,16,64,128]{3,2,1,0:T(8,128)(2,1)S(1)} %shard_map.57), channel_id=1, source_target_pairs={{0,384},{1,97},{2,386},{3,99},{4,388},{5,101},{6,390},{7,103},{8,3... | collective-permute-start | bytes 1572872 | tf_op jit(solution)/shard_map/ppermute | solution.py:28
  84.5 17.1 %collective-permute-start.5 = (bf16[2,16,64,128]{3,2,1,0:T(8,128)(2,1)S(1)}, bf16[2,16,64,128]{3,2,1,0:T(8,128)(2,1)S(1)}, u32[]{:S(2)}, u32[]{:S(2)}) collective-permute-start(bf16[2,16,64,128]{3,2,1,0:T(8,128)(2,1)S(1)} %collective-permute-done.3.refs_0_.refs_3_), channel_id=1, source_target_pairs={{0,1},{1,0},{2,3},{3,2},{4,5},{5,4},{6,7},{7,6},{8,9},{9,8},{10,11... | collective-permute-start | bytes 1572872 | tf_op jit(solution)/shard_map/ppermute | solution.py:28
  88.2 13.5 %collective-permute-start.6 = (bf16[2,16,64,128]{3,2,1,0:T(8,128)(2,1)S(1)}, bf16[2,16,64,128]{3,2,1,0:T(8,128)(2,1)S(1)}, u32[]{:S(2)}, u32[]{:S(2)}) collective-permute-start(bf16[2,16,64,128]{3,2,1,0:T(8,128)(2,1)S(1)} %collective-permute-done.4.refs_1_.refs_4_), channel_id=1, source_target_pairs={{0,1},{1,0},{2,3},{3,2},{4,5},{5,4},{6,7},{7,6},{8,9},{9,8},{10,11... | collective-permute-start | bytes 1572872 | tf_op jit(solution)/shard_map/ppermute | solution.py:28
  90.1 9.9 %collective-permute-start = (bf16[32,2048]{1,0:T(8,128)(2,1)S(1)}, bf16[32,2048]{1,0:T(8,128)(2,1)S(1)}, u32[]{:S(2)}, u32[]{:S(2)}) collective-permute-start(bf16[32,2048]{1,0:T(8,128)(2,1)S(1)} %shard_map.55), channel_id=1, source_target_pairs={{0,32},{1,33},{2,34},{3,35},{4,36},{5,37},{6,38},{7,39},{8,40},{9,... | collective-permute-start | bytes 393224 | tf_op jit(solution)/shard_map/ppermute | solution.py:376

commit v9 on v8

--- a/solution.py
+++ b/solution.py
@@ -113,14 +113,27 @@
     return pl.CostEstimate(flops=flops, bytes_accessed=1 << 20, transcendentals=0)
 
 
+def pack_kernel(turned, down, out):
+    c = lax.axis_index("tp") % 2
+    first = jnp.where(c == 0, down[0], down[1])
+    last = jnp.where(c == 0, down[1], down[0])
+    folded = jnp.concatenate([first, last], axis=1)
+    for z in range(16):
+        out[z, 0:16] = turned[0]
+        out[z, 16:32] = turned[1]
+        out[z, 32:64] = folded
+
+
 def packed(in_weight, down_weight):
-    core = lax.axis_index("tp") % 2
-    turned = jnp.swapaxes(in_weight, 1, 2).reshape(32, 128)
-    first = jnp.where(core == 0, down_weight[0], down_weight[1])
-    last = jnp.where(core == 0, down_weight[1], down_weight[0])
-    folded = jnp.concatenate([first, last], axis=1)
-    block = jnp.concatenate([turned, folded], axis=0)
-    return jnp.broadcast_to(block[None], (16, 64, 128))
+    return pl.pallas_call(
+        pack_kernel,
+        out_shape=jax.ShapeDtypeStruct((16, 64, 128), BF16),
+        in_specs=[VMEM] * 2,
+        out_specs=VMEM,
+        compiler_params=params(2),
+        cost_estimate=cost(1 << 20),
+        name="pack",
+    )(jnp.swapaxes(in_weight, 1, 2), down_weight)
 
 
 def cut(array, low, high):

time: 108 us -> 108 us (level)
  other arithmetic: 1.49 us -> 0 us
  local copies, waits for them, and re-layouts: 0.3 us -> 1.67 us
    unnamed x6 -> x10, local copies, waits for them, and re-layouts: 0.01 us -> 1.42 us
where the time goes in v9:
time: 108 us; the launch traced here: 107 us
  blocking collectives  49.7 us (46%)
  starting transfers between devices  24.1 us (22%)
  waiting for transfers between devices  20.7 us (19%)
  Pallas kernels  10.8 us (10%)
  local copies, waits for them, and re-layouts  1.67 us (2%)
    all_to_all x2, blocking collectives, shared(): lax.all_to_all(copies, AXES, 0, 0, axis_index_groups=list(groups.values()...  49.7 us
    ppermute x9, starting transfers between devices, send(): return lax.ppermute(block, AXES, route)  22.2 us
    ppermute x9, waiting for transfers between devices, send(): return lax.ppermute(block, AXES, route)  16.2 us
    pallas_call x1, Pallas kernels, mixer(): pl.pallas_call(mixer_kernel, out_shape=(jax.ShapeDtypeStruct(tokens.shape...  5.65 us
    ppermute x1, waiting for transfers between devices, mixed(): halo = lax.ppermute(end, AXES, [(i, i + 32) for i in range(480)])  4.49 us
    pallas_call x4, Pallas kernels, placed(): pl.pallas_call(kernel, out_shape=(jax.ShapeDtypeStruct((rows, 2048), BF16...  2.76 us
    pallas_call x1, Pallas kernels, head(): pl.pallas_call(head_kernel, out_shape=(jax.ShapeDtypeStruct((HALO + token...  2.25 us
  transfers between devices with their start and end apart: 10, of which 5 were waited for; matrix products, arithmetic and copies ran while one was open for 0% of the time, Pallas kernels for 5%

profile of v9, /device:TPU:24, one launch (start us, length us, event | category | flops | bytes accessed | tf_op | source)
XLA Modules:
  0.0 107.3 jit_solution(9464769841693751238)
XLA Ops:
  0.0 0.0 copy-start.2
  0.0 0.7 copy-done.2
  0.7 0.0 copy-start.3
  0.7 0.7 copy-done.3
  1.4 0.1 pack.1
  1.5 33.4 %all_to_all.10 = bf16[16,64,128]{2,1,0:T(8,128)(2,1)S(1)} all-to-all(bf16[16,64,128]{2,1,0:T(8,128)(2,1)S(1)} %pack.1), channel_id=1, replica_groups={{0,2,4,6,8,10,12,14,16,18,20,22,24,26,28,30},{1,3,5,7,9,11,13,15,17,19,..., dimensions={0} | all-to-all | bytes 524288 | tf_op jit(solution)/shard_map/all_to_all | solution.py:35
  34.9 0.2 broadcast_in_dim.4
  35.2 16.3 %all_to_all.11.refs_0_.refs_2_ = bf16[4,16,64,128]{3,2,1,0:T(8,128)(2,1)S(1)} all-to-all(bf16[4,16,64,128]{3,2,1,0:T(8,128)(2,1)S(1)} %broadcast_in_dim.4), channel_id=1, replica_groups={{0,32,64,96},{1,129,257,385},{2,34,66,98},{3,131,259,387},{4,36,68,100}..., dimensions={0} | all-to-all | bytes 2097152 | tf_op jit(solution)/shard_map/all_to_all | solution.py:35
  51.5 0.0 copy-start
  51.5 0.0 copy-start.1
  51.5 0.0 copy-start.4
  51.5 2.0 %collective-permute-start.1 = (bf16[4,16,64,128]{3,2,1,0:T(8,128)(2,1)S(1)}, bf16[4,16,64,128]{3,2,1,0:T(8,128)(2,1)S(1)}, u32[]{:S(2)}, u32[]{:S(2)}) collective-permute-start(bf16[4,16,64,128]{3,2,1,0:T(8,128)(2,1)S(1)} %all_to_all.11.refs_0_.refs_2_), channel_id=1, source_target_pairs={{0,128},{1,33},{2,130},{3,35},{4,132},{5,37},{6,134},{7,39},{8,136... | collective-permute-start | bytes 3145736 | tf_op jit(solution)/shard_map/ppermute | solution.py:28
  53.5 3.9 %collective-permute-start.2 = (bf16[4,16,64,128]{3,2,1,0:T(8,128)(2,1)S(1)}, bf16[4,16,64,128]{3,2,1,0:T(8,128)(2,1)S(1)}, u32[]{:S(2)}, u32[]{:S(2)}) collective-permute-start(bf16[4,16,64,128]{3,2,1,0:T(8,128)(2,1)S(1)} %all_to_all.11.refs_0_.refs_2_), channel_id=1, source_target_pairs={{0,384},{1,97},{2,386},{3,99},{4,388},{5,101},{6,390},{7,103},{8,3... | collective-permute-start | bytes 3145736 | tf_op jit(solution)/shard_map/ppermute | solution.py:28
  57.5 1.9 %collective-permute-start.7 = (bf16[4,16,64,128]{3,2,1,0:T(8,128)(2,1)S(1)}, bf16[4,16,64,128]{3,2,1,0:T(8,128)(2,1)S(1)}, u32[]{:S(2)}, u32[]{:S(2)}) collective-permute-start(bf16[4,16,64,128]{3,2,1,0:T(8,128)(2,1)S(1)} %all_to_all.11.refs_0_.refs_2_), channel_id=1, source_target_pairs={{0,1},{1,0},{2,3},{3,2},{4,5},{5,4},{6,7},{7,6},{8,9},{9,8},{10,11... | collective-permute-start | bytes 3145736 | tf_op jit(solution)/shard_map/ppermute | solution.py:28
  59.4 8.9 %collective-permute-done.1.array.refs_1_.refs_3_ = bf16[4,16,64,128]{3,2,1,0:T(8,128)(2,1)S(1)} collective-permute-done((bf16[4,16,64,128]{3,2,1,0:T(8,128)(2,1)S(1)}, bf16[4,16,64,128]{3,2,1,0:T(8,128)(2,1)S(1)}, u32[]{:S(2)}, u32[]{:S(2)}) %collective-permute-start.1) | collective-permute-done | bytes 1048608 | tf_op jit(solution)/shard_map/ppermute | solution.py:28
  68.3 1.9 %collective-permute-start.8 = (bf16[4,16,64,128]{3,2,1,0:T(8,128)(2,1)S(1)}, bf16[4,16,64,128]{3,2,1,0:T(8,128)(2,1)S(1)}, u32[]{:S(2)}, u32[]{:S(2)}) collective-permute-start(bf16[4,16,64,128]{3,2,1,0:T(8,128)(2,1)S(1)} %collective-permute-done.1.array.refs_1_.refs_3_), channel_id=1, source_target_pairs={{0,1},{1,0},{2,3},{3,2},{4,5},{5,4},{6,7},{7,6},{8,9},{9,8},{10,11... | collective-permute-start | bytes 3145736 | tf_op jit(solution)/shard_map/ppermute | solution.py:28
  70.2 1.2 %collective-permute-done.2.array.refs_4_.refs_2_ = bf16[4,16,64,128]{3,2,1,0:T(8,128)(2,1)S(1)} collective-permute-done((bf16[4,16,64,128]{3,2,1,0:T(8,128)(2,1)S(1)}, bf16[4,16,64,128]{3,2,1,0:T(8,128)(2,1)S(1)}, u32[]{:S(2)}, u32[]{:S(2)}) %collective-permute-start.2) | collective-permute-done | bytes 1048608 | tf_op jit(solution)/shard_map/ppermute | solution.py:28
  71.4 1.9 %collective-permute-start.9 = (bf16[4,16,64,128]{3,2,1,0:T(8,128)(2,1)S(1)}, bf16[4,16,64,128]{3,2,1,0:T(8,128)(2,1)S(1)}, u32[]{:S(2)}, u32[]{:S(2)}) collective-permute-start(bf16[4,16,64,128]{3,2,1,0:T(8,128)(2,1)S(1)} %collective-permute-done.2.array.refs_4_.refs_2_), channel_id=1, source_target_pairs={{0,1},{1,0},{2,3},{3,2},{4,5},{5,4},{6,7},{7,6},{8,9},{9,8},{10,11... | collective-permute-start | bytes 3145736 | tf_op jit(solution)/shard_map/ppermute | solution.py:28
  73.4 2.4 %collective-permute-start.3 = (bf16[2,16,64,128]{3,2,1,0:T(8,128)(2,1)S(1)}, bf16[2,16,64,128]{3,2,1,0:T(8,128)(2,1)S(1)}, u32[]{:S(2)}, u32[]{:S(2)}) collective-permute-start(bf16[2,16,64,128]{3,2,1,0:T(8,128)(2,1)S(1)} %shard_map.56), channel_id=1, source_target_pairs={{0,128},{1,33},{2,130},{3,35},{4,132},{5,37},{6,134},{7,39},{8,136... | collective-permute-start | bytes 1572872 | tf_op jit(solution)/shard_map/ppermute | solution.py:28
  75.9 3.4 %collective-permute-start.4 = (bf16[2,16,64,128]{3,2,1,0:T(8,128)(2,1)S(1)}, bf16[2,16,64,128]{3,2,1,0:T(8,128)(2,1)S(1)}, u32[]{:S(2)}, u32[]{:S(2)}) collective-permute-start(bf16[2,16,64,128]{3,2,1,0:T(8,128)(2,1)S(1)} %shard_map.57), channel_id=1, source_target_pairs={{0,384},{1,97},{2,386},{3,99},{4,388},{5,101},{6,390},{7,103},{8,3... | collective-permute-start | bytes 1572872 | tf_op jit(solution)/shard_map/ppermute | solution.py:28
  79.3 5.2 %collective-permute-done.3.refs_0_.refs_3_ = bf16[2,16,64,128]{3,2,1,0:T(8,128)(2,1)S(1)} collective-permute-done((bf16[2,16,64,128]{3,2,1,0:T(8,128)(2,1)S(1)}, bf16[2,16,64,128]{3,2,1,0:T(8,128)(2,1)S(1)}, u32[]{:S(2)}, u32[]{:S(2)}) %collective-permute-start.3) | collective-permute-done | bytes 524320 | tf_op jit(solution)/shard_map/ppermute | solution.py:28
  84.5 2.8 %collective-permute-start.5 = (bf16[2,16,64,128]{3,2,1,0:T(8,128)(2,1)S(1)}, bf16[2,16,64,128]{3,2,1,0:T(8,128)(2,1)S(1)}, u32[]{:S(2)}, u32[]{:S(2)}) collective-permute-start(bf16[2,16,64,128]{3,2,1,0:T(8,128)(2,1)S(1)} %collective-permute-done.3.refs_0_.refs_3_), channel_id=1, source_target_pairs={{0,1},{1,0},{2,3},{3,2},{4,5},{5,4},{6,7},{7,6},{8,9},{9,8},{10,11... | collective-permute-start | bytes 1572872 | tf_op jit(solution)/shard_map/ppermute | solution.py:28
  87.2 0.9 collective-permute-done.4.refs_1_.refs_4_
  88.2 1.9 %collective-permute-start.6 = (bf16[2,16,64,128]{3,2,1,0:T(8,128)(2,1)S(1)}, bf16[2,16,64,128]{3,2,1,0:T(8,128)(2,1)S(1)}, u32[]{:S(2)}, u32[]{:S(2)}) collective-permute-start(bf16[2,16,64,128]{3,2,1,0:T(8,128)(2,1)S(1)} %collective-permute-done.4.refs_1_.refs_4_), channel_id=1, source_target_pairs={{0,1},{1,0},{2,3},{3,2},{4,5},{5,4},{6,7},{7,6},{8,9},{9,8},{10,11... | collective-permute-start | bytes 1572872 | tf_op jit(solution)/shard_map/ppermute | solution.py:28
  90.1 0.0 copy-done
  90.1 0.0 collective-permute-done.7.refs_1_.refs_2_.refs_5_
  90.1 1.9 %collective-permute-start = (bf16[32,2048]{1,0:T(8,128)(2,1)S(1)}, bf16[32,2048]{1,0:T(8,128)(2,1)S(1)}, u32[]{:S(2)}, u32[]{:S(2)}) collective-permute-start(bf16[32,2048]{1,0:T(8,128)(2,1)S(1)} %shard_map.55), channel_id=1, source_target_pairs={{0,32},{1,33},{2,34},{3,35},{4,36},{5,37},{6,38},{7,39},{8,40},{9,... | collective-permute-start | bytes 393224 | tf_op jit(solution)/shard_map/ppermute | solution.py:389
  92.0 0.0 copy-done.1
  92.1 0.0 copy-done.4
  92.1 2.2 %head.1 = (bf16[416,2048]{1,0:T(8,128)(2,1)S(1)}, f32[2,512]{1,0:T(2,128)S(1)}) custom-call(bf16[384,2048]{1,0:T(8,128)(2,1)S(1)} %bitcast.4, f32[2,2048]{1,0:T(2,128)S(1)} %copy-done.1, f32[2,512]{1,0:T(2,128)S(1)} %copy-done.4), custom_call_target="tpu_custom_call" | custom-call | flops 1073741824 | bytes 1048576 | tf_op jit(solution)/shard_map/head/pallas_call | solution.py:180
  94.3 0.5 shard_map.58
  94.9 0.0 collective-permute-done.8.refs_3_.refs_6_
  94.9 0.7 shard_map.59
  95.5 4.5 %collective-permute-done.refs_0_.halo = bf16[32,2048]{1,0:T(8,128)(2,1)S(1)} collective-permute-done((bf16[32,2048]{1,0:T(8,128)(2,1)S(1)}, bf16[32,2048]{1,0:T(8,128)(2,1)S(1)}, u32[]{:S(2)}, u32[]{:S(2)}) %collective-permute-start) | collective-permute-done | bytes 131104 | tf_op jit(solution)/shard_map/ppermute | solution.py:389
  100.0 0.0 collective-permute-done.9.refs_7_.refs_4_
  100.0 1.1 %shard_map.60 = (bf16[416,2048]{1,0:T(8,128)(2,1)S(1)}, f32[2,416,256]{2,1,0:T(8,128)S(1)}, bf16[2,16,16,2048]{3,2,1,0:T(8,128)(2,1)S(1)}, bf16[2,2,256,2048]{3,2,1,0:T(8,128)(2,1)S(1)}) custom-call(bf16[32,2048]{1,0:T(8,128)(2,1)S(1)} %collective-permute-done.refs_0_.halo, ...), custom_call_target="tpu_custom_call", output_to_operand_aliasing={{0}: (8, {}), {1}: (9, {}), {2}: (10, {}), {3}: (11, {})} | custom-call | flops 536870912 | bytes 1048576 | tf_op jit(solution)/shard_map/pallas_call | solution.py:208
  101.1 0.5 shard_map.61
  101.6 0.0 collective-permute-done.5.refs_5_
  101.6 0.0 collective-permute-done.6.refs_6_
  101.6 5.7 %mixer.1 = (bf16[384,2048]{1,0:T(8,128)(2,1)}, f32[2,416,256]{2,1,0:T(8,128)S(1)}, bf16[2,16,16,2048]{3,2,1,0:T(8,128)(2,1)S(1)}, bf16[2,2,256,2048]{3,2,1,0:T(8,128)(2,1)S(1)}) custom-call(bf16[384,2048]{1,0:T(8,128)(2,1)S(1)} %bitcast.5, ...), custom_call_target="tpu_custom_call", output_to_operand_aliasing={{1}: (12, {}), {2}: (13, {}), {3}: (14, {})} | custom-call | flops 4294967296 | bytes 1048576 | tf_op jit(solution)/shard_map/mixer/pallas_call | solution.py:362
  (3 shorter events, 0.1 us)
Async XLA Ops:
  0.0 0.7 copy-start.2
  0.7 0.7 copy-start.3
  51.5 38.6 %copy-start = (bf16[1,384,2048]{2,1,0:T(8,128)(2,1)S(1)}, bf16[1,384,2048]{2,1,0:T(8,128)(2,1)}, u32[]{:S(2)}) copy-start(bf16[1,384,2048]{2,1,0:T(8,128)(2,1)} %param.5) | copy-start | bytes 4718596
  51.5 40.6 %copy-start.1 = (f32[2,2048]{1,0:T(2,128)S(1)}, f32[2,2048]{1,0:T(2,128)}, u32[]{:S(2)}) copy-start(f32[2,2048]{1,0:T(2,128)} %norm_gain.3) | copy-start | bytes 49156
  51.5 40.6 %copy-start.4 = (f32[2,512]{1,0:T(2,128)S(1)}, f32[2,512]{1,0:T(2,128)}, u32[]{:S(2)}) copy-start(f32[2,512]{1,0:T(2,128)} %pool_gain.1) | copy-start | bytes 12292
  51.5 16.8 %collective-permute-start.1 = (bf16[4,16,64,128]{3,2,1,0:T(8,128)(2,1)S(1)}, bf16[4,16,64,128]{3,2,1,0:T(8,128)(2,1)S(1)}, u32[]{:S(2)}, u32[]{:S(2)}) collective-permute-start(bf16[4,16,64,128]{3,2,1,0:T(8,128)(2,1)S(1)} %all_to_all.11.refs_0_.refs_2_), channel_id=1, source_target_pairs={{0,128},{1,33},{2,130},{3,35},{4,132},{5,37},{6,134},{7,39},{8,136... | collective-permute-start | bytes 3145736 | tf_op jit(solution)/shard_map/ppermute | solution.py:28
  53.5 17.9 %collective-permute-start.2 = (bf16[4,16,64,128]{3,2,1,0:T(8,128)(2,1)S(1)}, bf16[4,16,64,128]{3,2,1,0:T(8,128)(2,1)S(1)}, u32[]{:S(2)}, u32[]{:S(2)}) collective-permute-start(bf16[4,16,64,128]{3,2,1,0:T(8,128)(2,1)S(1)} %all_to_all.11.refs_0_.refs_2_), channel_id=1, source_target_pairs={{0,384},{1,97},{2,386},{3,99},{4,388},{5,101},{6,390},{7,103},{8,3... | collective-permute-start | bytes 3145736 | tf_op jit(solution)/shard_map/ppermute | solution.py:28
  57.5 32.6 %collective-permute-start.7 = (bf16[4,16,64,128]{3,2,1,0:T(8,128)(2,1)S(1)}, bf16[4,16,64,128]{3,2,1,0:T(8,128)(2,1)S(1)}, u32[]{:S(2)}, u32[]{:S(2)}) collective-permute-start(bf16[4,16,64,128]{3,2,1,0:T(8,128)(2,1)S(1)} %all_to_all.11.refs_0_.refs_2_), channel_id=1, source_target_pairs={{0,1},{1,0},{2,3},{3,2},{4,5},{5,4},{6,7},{7,6},{8,9},{9,8},{10,11... | collective-permute-start | bytes 3145736 | tf_op jit(solution)/shard_map/ppermute | solution.py:28
  68.3 26.6 %collective-permute-start.8 = (bf16[4,16,64,128]{3,2,1,0:T(8,128)(2,1)S(1)}, bf16[4,16,64,128]{3,2,1,0:T(8,128)(2,1)S(1)}, u32[]{:S(2)}, u32[]{:S(2)}) collective-permute-start(bf16[4,16,64,128]{3,2,1,0:T(8,128)(2,1)S(1)} %collective-permute-done.1.array.refs_1_.refs_3_), channel_id=1, source_target_pairs={{0,1},{1,0},{2,3},{3,2},{4,5},{5,4},{6,7},{7,6},{8,9},{9,8},{10,11... | collective-permute-start | bytes 3145736 | tf_op jit(solution)/shard_map/ppermute | solution.py:28
  71.4 28.6 %collective-permute-start.9 = (bf16[4,16,64,128]{3,2,1,0:T(8,128)(2,1)S(1)}, bf16[4,16,64,128]{3,2,1,0:T(8,128)(2,1)S(1)}, u32[]{:S(2)}, u32[]{:S(2)}) collective-permute-start(bf16[4,16,64,128]{3,2,1,0:T(8,128)(2,1)S(1)} %collective-permute-done.2.array.refs_4_.refs_2_), channel_id=1, source_target_pairs={{0,1},{1,0},{2,3},{3,2},{4,5},{5,4},{6,7},{7,6},{8,9},{9,8},{10,11... | collective-permute-start | bytes 3145736 | tf_op jit(solution)/shard_map/ppermute | solution.py:28
  73.4 11.1 %collective-permute-start.3 = (bf16[2,16,64,128]{3,2,1,0:T(8,128)(2,1)S(1)}, bf16[2,16,64,128]{3,2,1,0:T(8,128)(2,1)S(1)}, u32[]{:S(2)}, u32[]{:S(2)}) collective-permute-start(bf16[2,16,64,128]{3,2,1,0:T(8,128)(2,1)S(1)} %shard_map.56), channel_id=1, source_target_pairs={{0,128},{1,33},{2,130},{3,35},{4,132},{5,37},{6,134},{7,39},{8,136... | collective-permute-start | bytes 1572872 | tf_op jit(solution)/shard_map/ppermute | solution.py:28
  75.9 12.3 %collective-permute-start.4 = (bf16[2,16,64,128]{3,2,1,0:T(8,128)(2,1)S(1)}, bf16[2,16,64,128]{3,2,1,0:T(8,128)(2,1)S(1)}, u32[]{:S(2)}, u32[]{:S(2)}) collective-permute-start(bf16[2,16,64,128]{3,2,1,0:T(8,128)(2,1)S(1)} %shard_map.57), channel_id=1, source_target_pairs={{0,384},{1,97},{2,386},{3,99},{4,388},{5,101},{6,390},{7,103},{8,3... | collective-permute-start | bytes 1572872 | tf_op jit(solution)/shard_map/ppermute | solution.py:28
  84.5 17.1 %collective-permute-start.5 = (bf16[2,16,64,128]{3,2,1,0:T(8,128)(2,1)S(1)}, bf16[2,16,64,128]{3,2,1,0:T(8,128)(2,1)S(1)}, u32[]{:S(2)}, u32[]{:S(2)}) collective-permute-start(bf16[2,16,64,128]{3,2,1,0:T(8,128)(2,1)S(1)} %collective-permute-done.3.refs_0_.refs_3_), channel_id=1, source_target_pairs={{0,1},{1,0},{2,3},{3,2},{4,5},{5,4},{6,7},{7,6},{8,9},{9,8},{10,11... | collective-permute-start | bytes 1572872 | tf_op jit(solution)/shard_map/ppermute | solution.py:28
  88.2 13.5 %collective-permute-start.6 = (bf16[2,16,64,128]{3,2,1,0:T(8,128)(2,1)S(1)}, bf16[2,16,64,128]{3,2,1,0:T(8,128)(2,1)S(1)}, u32[]{:S(2)}, u32[]{:S(2)}) collective-permute-start(bf16[2,16,64,128]{3,2,1,0:T(8,128)(2,1)S(1)} %collective-permute-done.4.refs_1_.refs_4_), channel_id=1, source_target_pairs={{0,1},{1,0},{2,3},{3,2},{4,5},{5,4},{6,7},{7,6},{8,9},{9,8},{10,11... | collective-permute-start | bytes 1572872 | tf_op jit(solution)/shard_map/ppermute | solution.py:28
  90.1 9.9 %collective-permute-start = (bf16[32,2048]{1,0:T(8,128)(2,1)S(1)}, bf16[32,2048]{1,0:T(8,128)(2,1)S(1)}, u32[]{:S(2)}, u32[]{:S(2)}) collective-permute-start(bf16[32,2048]{1,0:T(8,128)(2,1)S(1)} %shard_map.55), channel_id=1, source_target_pairs={{0,32},{1,33},{2,34},{3,35},{4,36},{5,37},{6,38},{7,39},{8,40},{9,... | collective-permute-start | bytes 393224 | tf_op jit(solution)/shard_map/ppermute | solution.py:389
